TPU v7x, 256 devices: a whole 4x4x8 slice. The times are simulated.
256 devices in a mesh: ep: 64 (over z, x, core), tp: 4 (over y).
Axes of the slice: x: 4, y: 4, z: 8, core: 2. Of those that a mesh axis runs over, the one named last changes fastest.
Arguments:
- out_gate: bfloat16 [32768, 2048], P(('ep', 'tp')), may hold values from -6 to 6
- in_gate: bfloat16 [32768, 2048], P(('ep', 'tp')), may hold values from -6 to 6
- conv_input: bfloat16 [32768, 2048], P(('ep', 'tp')), may hold values from -6 to 6
- conv_taps: bfloat16 [3, 2048], replicated, may hold values from -3 to 3
- mixer_weight: bfloat16 [2048, 2048], P(None, 'tp'), may hold values from -0.125 to 0.125
- expert_input: bfloat16 [32768, 2048], P(('ep', 'tp')), may hold values from -6 to 6
- norm_gain: float32 [2048], replicated, may hold values from 0.1 to 1.9
- expert_gate: bfloat16 [64, 2048, 1024], P('ep', None, 'tp'), may hold values from -0.125 to 0.125
- expert_up: bfloat16 [64, 2048, 1024], P('ep', None, 'tp'), may hold values from -0.125 to 0.125
- expert_down: bfloat16 [64, 1024, 2048], P('ep', 'tp'), may hold values from -0.1875 to 0.1875
- expert_ids: int32 [32768, 2], P(('ep', 'tp')), may hold values from 0 to 63, all different within a row; in each aligned block of 128 rows (0 to 127, 128 to 255, ...) at most 8 rows name the same one
- route_weight: float32 [32768, 2], P(('ep', 'tp')), may hold values from 0.1 to 1
Outputs:
- mixer_out: bfloat16 [32768, 2048], P('ep', 'tp')
- experts_out: bfloat16 [32768, 2048], P(('ep', 'tp'))
Inputs may be any that keep to these rules, and one draw needn't show every extreme that they name: `expert_ids`: each row names 2 different experts. Within the 128 rows of one device no expert is named by more than 8 rows, and in some devices' rows some expert is named by exactly 8.
All inputs are finite; a program needn't handle non-finite values.
Results may differ from a plain program's by a relative error of at most 0.011.
Values may be sent and summed in bfloat16 or wider, within the bound.
No kernel may reach another device: no remote copies, remote signals or barrier semaphores. Data moves between devices by JAX's collectives and lax.ppermute only.
A program may use at most 128 MiB of HBM per device.

v0:
```python
import jax
import jax.numpy as jnp
from jax import lax
from jax.experimental import pallas as pl
from jax.experimental.pallas import tpu as pltpu
from jax.sharding import PartitionSpec as P


CONV = 3
NORM_EPS = 1e-06
PIECES = (256, 256, 1024, 512)
CHUNKS = ((0, 1), (2, 3))


def turn(value, steps):
    count = lax.axis_size("tp")
    pairs = [(source, (source + steps) % count) for source in range(count)]
    return lax.ppermute(value, "tp", pairs)


def from_sides(value):
    return turn(value, 1), turn(value, -1)


def from_opposite(left, right):
    half = left.shape[0] // 2
    return turn(left[:half], 1), turn(right[half:], -1)


def slot_table(ids, expert_count, slot_cap):
    tokens = ids.shape[1]
    expert = lax.broadcasted_iota(jnp.int32, (expert_count, tokens), 0)
    chosen = [ids[k : k + 1] == expert for k in range(ids.shape[0])]
    member = jnp.where(chosen[0] | chosen[1], 1.0, 0.0).astype(jnp.bfloat16)
    row = lax.broadcasted_iota(jnp.int32, (tokens, tokens), 0)
    column = lax.broadcasted_iota(jnp.int32, (tokens, tokens), 1)
    earlier = jnp.where(row < column, 1.0, 0.0).astype(jnp.bfloat16)
    before = jnp.dot(member, earlier, preferred_element_type=jnp.float32).astype(jnp.int32)
    shape = (expert_count, slot_cap, tokens)
    slot = lax.broadcasted_iota(jnp.int32, shape, 1)
    here = jnp.broadcast_to(before[:, None, :], shape) == slot
    return [
        jnp.where(here, jnp.broadcast_to(jnp.where(c, 1.0, 0.0)[:, None, :], shape), 0.0).reshape(
            expert_count * slot_cap, tokens
        )
        for c in chosen
    ]


def dispatch_kernel(ids_ref, input_ref, gain_ref, out_ref, *, expert_count, slot_cap):
    wide = input_ref[...].astype(jnp.float32)
    inv_norm = lax.rsqrt(jnp.mean(wide * wide, axis=1, keepdims=True) + NORM_EPS)
    normed = (wide * inv_norm * gain_ref[...]).astype(jnp.bfloat16)
    table = sum(slot_table(ids_ref[...], expert_count, slot_cap)).astype(jnp.bfloat16)
    out_ref[...] = jnp.dot(table, normed, preferred_element_type=jnp.float32).astype(jnp.bfloat16)


def mix_kernel(ids_ref, weight_ref, high_ref, low_ref, *, expert_count, slot_cap):
    weight = weight_ref[...]
    share = weight / (weight[0:1] + weight[1:2])
    tables = slot_table(ids_ref[...], expert_count, slot_cap)
    mix = (tables[0] * share[0:1] + tables[1] * share[1:2]).T
    high = mix.astype(jnp.bfloat16)
    high_ref[...] = high
    low_ref[...] = (mix - high.astype(jnp.float32)).astype(jnp.bfloat16)


def combine_kernel(high_ref, low_ref, *refs):
    out_ref, at = refs[-1], 0
    for ref in refs[:-1]:
        rows = ref[...]
        picked = dot32(high_ref[...], rows) + dot32(low_ref[...], rows)
        out_ref[:, at : at + rows.shape[1]] = picked.astype(jnp.bfloat16)
        at += rows.shape[1]


def down_kernel(*refs):
    out_ref, hidden, downs, at = refs[-1], refs[:4], refs[4:-1], 0
    for i in range(0, len(downs), 4):
        own = downs[i]
        total = sum(dot32(h[...], d[...]) for h, d in zip(hidden, downs[i : i + 4]))
        out_ref[:, at : at + own.shape[1]] = total.astype(jnp.bfloat16)
        at += own.shape[1]


def mixer_kernel(place_ref, own_ref, left_ref, right_ref, first_ref, second_ref, weight_ref, out_ref):
    rows = own_ref.shape[0]
    weight = weight_ref[...]

    def put(ref, steps, offset):
        block = jnp.dot(ref[...], weight, preferred_element_type=jnp.float32).astype(jnp.bfloat16)
        at = ((place_ref[0] + steps) & 3) * rows + offset
        out_ref[pl.ds(pl.multiple_of(at, rows // 2), block.shape[0]), :] = block

    put(own_ref, 0, 0)
    put(left_ref, 3, 0)
    put(right_ref, 1, 0)
    put(first_ref, 2, 0)
    put(second_ref, 2, rows // 2)


def dot32(a, b):
    return jnp.dot(a, b, preferred_element_type=jnp.float32)


def local(
    out_gate,
    in_gate,
    conv_input,
    conv_taps,
    mixer_weight,
    expert_input,
    norm_gain,
    expert_gate,
    expert_up,
    expert_down,
    expert_ids,
    route_weight,
):
    row_count, model_width = in_gate.shape
    token_count = expert_input.shape[0]
    expert_count = lax.axis_size("ep")
    slot_cap = 4 * token_count // expert_count
    slots = expert_count * slot_cap
    vmem = pl.BlockSpec(memory_space=pltpu.VMEM)
    ids_t = expert_ids.T
    weight_t = route_weight.T

    gate, up, down = expert_gate[0], expert_up[0], expert_down[0]
    gates = from_sides(gate)
    ups = from_sides(up)
    gate_far = turn(gates[0], 1)
    up_far = turn(ups[1], -1)
    downs, at = [], 0
    for i, width in enumerate(PIECES):
        part = down[:, at : at + width]
        at += width
        sides = from_sides(part)
        far = turn(sides[i % 2], 1 - 2 * (i % 2))
        downs.append((part, *sides, far))

    outgoing = pl.pallas_call(
        lambda *refs: dispatch_kernel(*refs, expert_count=expert_count, slot_cap=slot_cap),
        out_shape=jax.ShapeDtypeStruct((slots, model_width), jnp.bfloat16),
        in_specs=[vmem] * 3,
        out_specs=vmem,
        name="dispatch",
    )(ids_t, expert_input, norm_gain[None])
    arrived = lax.all_to_all(
        outgoing.reshape(expert_count, slot_cap, model_width), "ep", 0, 0, tiled=True
    ).reshape(slots, model_width)
    mix = pl.pallas_call(
        lambda *refs: mix_kernel(*refs, expert_count=expert_count, slot_cap=slot_cap),
        out_shape=[jax.ShapeDtypeStruct((token_count, slots), jnp.bfloat16)] * 2,
        in_specs=[vmem] * 2,
        out_specs=[vmem] * 2,
        name="mix",
    )(ids_t, weight_t)

    tap_span = CONV - 1
    product = in_gate.astype(jnp.float32) * conv_input.astype(jnp.float32)
    devices = expert_count * lax.axis_size("tp")
    earlier = lax.ppermute(
        product[row_count - tap_span :], ("ep", "tp"), [(i, i + 1) for i in range(devices - 1)]
    )
    padded = jnp.concatenate([earlier, product], axis=0)
    taps = conv_taps.astype(jnp.float32)
    smoothed = sum(padded[j : j + row_count] * taps[j] for j in range(CONV))
    gated = (out_gate.astype(jnp.float32) * smoothed).astype(jnp.bfloat16)

    hidden = [
        (jax.nn.silu(dot32(arrived, g)) * dot32(arrived, u)).astype(jnp.bfloat16)
        for g, u in zip((gate, *gates, gate_far), (up, *ups, up_far))
    ]

    returned = []
    for chunk in CHUNKS:
        operands = [d for piece in chunk for d in downs[piece]]
        width = sum(PIECES[piece] for piece in chunk)
        result = pl.pallas_call(
            down_kernel,
            out_shape=jax.ShapeDtypeStruct((slots, width), jnp.bfloat16),
            in_specs=[vmem] * (4 + len(operands)),
            out_specs=vmem,
        )(*hidden, *operands)
        back = lax.all_to_all(result.reshape(expert_count, slot_cap, width), "ep", 0, 0, tiled=True)
        returned.append(back.reshape(slots, width))

    gated_sides = from_sides(gated)
    gated_far = from_opposite(*gated_sides)
    mixer_out = pl.pallas_call(
        mixer_kernel,
        out_shape=jax.ShapeDtypeStruct((4 * row_count, mixer_weight.shape[1]), jnp.bfloat16),
        in_specs=[pl.BlockSpec(memory_space=pltpu.SMEM)] + [vmem] * 6,
        out_specs=vmem,
        name="mixer",
    )(lax.axis_index("tp").reshape(1), gated, *gated_sides, *gated_far, mixer_weight)

    experts_out = pl.pallas_call(
        combine_kernel,
        out_shape=jax.ShapeDtypeStruct((token_count, model_width), jnp.bfloat16),
        in_specs=[vmem] * (2 + len(returned)),
        out_specs=vmem,
        name="combine",
    )(*mix, *returned)
    return (mixer_out, experts_out)


def solution(mesh):
    return jax.shard_map(
        local,
        mesh=mesh,
        in_specs=(
            P(("ep", "tp"), None),
            P(("ep", "tp"), None),
            P(("ep", "tp"), None),
            P(),
            P(None, "tp"),
            P(("ep", "tp"), None),
            P(),
            P("ep", None, "tp"),
            P("ep", None, "tp"),
            P("ep", "tp", None),
            P(("ep", "tp"), None),
            P(("ep", "tp"), None),
        ),
        out_specs=(P("ep", "tp"), P(("ep", "tp"), None)),
        check_vma=False,
    )
```

profile of v0, /device:TPU:120, one launch (start us, length us, event | category | flops | bytes accessed | tf_op | source)
XLA Modules:
  0.0 240.8 jit_solution(4317270318576097326)
XLA Ops:
  0.6 3.3 %dispatch.1 = bf16[512,2048]{1,0:T(8,128)(2,1)} custom-call(s32[2,128]{1,0:T(2,128)} %bitcast.64, bf16[128,2048]{1,0:T(8,128)(2,1)} %refs_1_.1, f32[1,2048]{1,0:T(1,128)} %bitcast.63), custom_call_target="tpu_custom_call" | custom-call | tf_op jit(solution)/shard_map/dispatch/pallas_call | solution.py:142
  3.9 10.7 %all-to-all-start = ((bf16[64,8,2048]{2,1,0:T(8,128)(2,1)}), bf16[64,8,2048]{2,1,0:T(8,128)(2,1)S(1)}, u32[]{:S(2)}, u32[]{:S(2)}) async-start(bf16[64,8,2048]{2,1,0:T(8,128)(2,1)} %bitcast.52), calls=%async_computation | async-start | bytes 4194304 | tf_op jit(solution)/shard_map/all_to_all | solution.py:149
  15.0 1.8 collective-permute-start.8
  16.8 0.7 collective-permute-start.7
  17.5 2.5 %collective-permute-start.6 = (bf16[2048,256]{1,0:T(8,128)(2,1)}, bf16[2048,256]{1,0:T(8,128)(2,1)}, u32[]{:S(2)}, u32[]{:S(2)}) collective-permute-start(bf16[2048,256]{1,0:T(8,128)(2,1)} %bitcast.70), channel_id=1, source_target_pairs={{0,1},{1,2},{2,3},{3,0},{4,5},{5,6},{6,7},{7,4},{8,9},{9,10},{10,1... | collective-permute-start | bytes 3145736 | tf_op jit(solution)/shard_map/ppermute | solution.py:18
  20.0 21.1 %collective-permute-done.5 = bf16[2048,256]{1,0:T(8,128)(2,1)} collective-permute-done((bf16[2048,256]{1,0:T(8,128)(2,1)}, bf16[2048,256]{1,0:T(8,128)(2,1)}, u32[]{:S(2)}, u32[]{:S(2)}) %collective-permute-start.5) | collective-permute-done | bytes 1048608 | tf_op jit(solution)/shard_map/ppermute | solution.py:18
  41.1 1.4 collective-permute-start.9
  42.5 1.0 fusion.31
  44.0 1.1 slice.58.refs_4_
  45.1 19.0 %all-to-all-done = bf16[64,8,2048]{2,1,0:T(8,128)(2,1)S(1)} async-done(((bf16[64,8,2048]{2,1,0:T(8,128)(2,1)}), bf16[64,8,2048]{2,1,0:T(8,128)(2,1)S(1)}, u32[]{:S(2)}, u32[]{:S(2)}) %all-to-all-start) | async-done | bytes 2097184 | tf_op jit(solution)/shard_map/all_to_all | solution.py:149
  64.1 1.9 fusion.14
  66.0 0.8 collective-permute-start.12
  67.3 1.9 fusion.6
  69.2 2.6 %multiply_convert_fusion.1.refs_2_ = bf16[512,256]{1,0:T(8,128)(2,1)} fusion(f32[512,256]{1,0:T(8,128)S(1)} %fusion.6, bf16[2048,256]{1,0:T(8,128)(2,1)} %collective-permute-done.8, bf16[64,8,2048]{2,1,0:T(8,128)(2,1)S(1)} %all-to-all-done), kind=kOutput, calls=%fused_computation.30 | convolution fusion | flops 537657344 | bytes 3932160 | tf_op jit(solution)/shard_map/dot_general | solution.py:103
  71.9 14.1 %collective-permute-done.9 = bf16[2048,256]{1,0:T(8,128)(2,1)} collective-permute-done((bf16[2048,256]{1,0:T(8,128)(2,1)}, bf16[2048,256]{1,0:T(8,128)(2,1)}, u32[]{:S(2)}, u32[]{:S(2)}) %collective-permute-start.9) | collective-permute-done | bytes 1048608 | tf_op jit(solution)/shard_map/ppermute | solution.py:18
  86.8 1.9 fusion.2
  88.7 1.4 fusion.19.refs_0_
  90.1 5.2 %collective-permute-done.10 = bf16[2048,256]{1,0:T(8,128)(2,1)S(1)} collective-permute-done((bf16[2048,256]{1,0:T(8,128)(2,1)}, bf16[2048,256]{1,0:T(8,128)(2,1)S(1)}, u32[]{:S(2)}, u32[]{:S(2)}) %collective-permute-start.10) | collective-permute-done | bytes 1048608 | tf_op jit(solution)/shard_map/ppermute | solution.py:18
  95.3 1.4 multiply_convert_fusion.refs_3_
  96.7 1.9 fusion.10
  99.4 1.6 collective-permute-start.13
  101.4 2.7 %multiply_convert_fusion.2.refs_1_ = bf16[512,256]{1,0:T(8,128)(2,1)} fusion(f32[512,256]{1,0:T(8,128)S(1)} %fusion.10, bf16[2048,256]{1,0:T(8,128)(2,1)} %collective-permute-done.6, bf16[64,8,2048]{2,1,0:T(8,128)(2,1)S(1)} %all-to-all-done), kind=kOutput, calls=%fused_computation.31 | convolution fusion | flops 537657344 | bytes 3932160 | tf_op jit(solution)/shard_map/dot_general | solution.py:103
  104.1 9.2 %collective-permute-done.13.refs_7_ = bf16[256,256]{1,0:T(8,128)(2,1)S(1)} collective-permute-done((bf16[256,256]{1,0:T(8,128)(2,1)S(1)}, bf16[256,256]{1,0:T(8,128)(2,1)S(1)}, u32[]{:S(2)}, u32[]{:S(2)}) %collective-permute-start.13) | collective-permute-done | bytes 131104 | tf_op jit(solution)/shard_map/ppermute | solution.py:18
  114.0 3.0 %shard_map.131 = bf16[512,512]{1,0:T(8,128)(2,1)} custom-call(bf16[512,256]{1,0:T(8,128)(2,1)} %fusion.19.refs_0_, bf16[512,256]{1,0:T(8,128)(2,1)} %multiply_convert_fusion.2.refs_1_, bf16[512,256]{1,0:T(8,128)(2,1)} %multiply_convert_fusion.1.refs_2_, bf16[512,256]{1,0:T(8,128)(2,1)} %multiply_convert_fusion.refs_3_, bf16[256,256]{1,0:T(8,128)(2,1)} %copy-done.8, ...), custom_call_target="tpu_custom_call" | custom-call | tf_op jit(solution)/shard_map/pallas_call | solution.py:180
  117.0 9.2 %all-to-all-start.1 = ((bf16[64,8,512]{2,1,0:T(8,128)(2,1)}), bf16[64,8,512]{2,1,0:T(8,128)(2,1)S(1)}, u32[]{:S(2)}, u32[]{:S(2)}) async-start(bf16[64,8,512]{2,1,0:T(8,128)(2,1)} %bitcast.55), calls=%async_computation.1 | async-start | bytes 1048576 | tf_op jit(solution)/shard_map/all_to_all | solution.py:186
  126.1 1.0 slice.59.refs_8_
  127.1 1.8 collective-permute-start.21
  129.1 3.1 %collective-permute-start.19 = (bf16[256,1024]{1,0:T(8,128)(2,1)S(1)}, bf16[256,1024]{1,0:T(8,128)(2,1)S(1)}, u32[]{:S(2)}, u32[]{:S(2)}) collective-permute-start(bf16[256,1024]{1,0:T(8,128)(2,1)S(1)} %collective-permute-done.17.refs_5_), channel_id=1, source_target_pairs={{0,1},{1,2},{2,3},{3,0},{4,5},{5,6},{6,7},{7,4},{8,9},{9,10},{10,1... | collective-permute-start | bytes 1572872 | tf_op jit(solution)/shard_map/ppermute | solution.py:18
  132.5 5.1 %collective-permute-done.21.refs_10_ = bf16[256,512]{1,0:T(8,128)(2,1)S(1)} collective-permute-done((bf16[256,512]{1,0:T(8,128)(2,1)S(1)}, bf16[256,512]{1,0:T(8,128)(2,1)S(1)}, u32[]{:S(2)}, u32[]{:S(2)}) %collective-permute-start.21) | collective-permute-done | bytes 262176 | tf_op jit(solution)/shard_map/ppermute | solution.py:18
  138.1 10.6 %collective-permute-done.20.refs_9_ = bf16[256,512]{1,0:T(8,128)(2,1)S(1)} collective-permute-done((bf16[256,512]{1,0:T(8,128)(2,1)S(1)}, bf16[256,512]{1,0:T(8,128)(2,1)S(1)}, u32[]{:S(2)}, u32[]{:S(2)}) %collective-permute-start.20) | collective-permute-done | bytes 262176 | tf_op jit(solution)/shard_map/ppermute | solution.py:18
  148.7 4.9 %collective-permute-done.22.refs_11_ = bf16[256,512]{1,0:T(8,128)(2,1)S(1)} collective-permute-done((bf16[256,512]{1,0:T(8,128)(2,1)S(1)}, bf16[256,512]{1,0:T(8,128)(2,1)S(1)}, u32[]{:S(2)}, u32[]{:S(2)}) %collective-permute-start.22) | collective-permute-done | bytes 262176 | tf_op jit(solution)/shard_map/ppermute | solution.py:18
  154.3 0.8 copy-done.13
  155.1 0.8 copy-done.14
  155.9 5.1 %shard_map.132 = bf16[512,1536]{1,0:T(8,128)(2,1)} custom-call(bf16[512,256]{1,0:T(8,128)(2,1)} %fusion.19.refs_0_, bf16[512,256]{1,0:T(8,128)(2,1)} %multiply_convert_fusion.2.refs_1_, bf16[512,256]{1,0:T(8,128)(2,1)} %multiply_convert_fusion.1.refs_2_, bf16[512,256]{1,0:T(8,128)(2,1)} %multiply_convert_fusion.refs_3_, bf16[256,1024]{1,0:T(8,128)(2,1)} %copy-done.3, ...), custom_call_target="tpu_custom_call" | custom-call | tf_op jit(solution)/shard_map/pallas_call | solution.py:180
  161.0 10.4 %all-to-all-start.2 = ((bf16[64,8,1536]{2,1,0:T(8,128)(2,1)}), bf16[64,8,1536]{2,1,0:T(8,128)(2,1)S(1)}, u32[]{:S(2)}, u32[]{:S(2)}) async-start(bf16[64,8,1536]{2,1,0:T(8,128)(2,1)} %bitcast.53), calls=%async_computation.2 | async-start | bytes 3145728 | tf_op jit(solution)/shard_map/all_to_all | solution.py:186
  171.7 2.2 collective-permute-start
  173.9 3.4 %collective-permute-done = f32[2,2048]{1,0:T(2,128)S(1)} collective-permute-done((f32[2,2048]{1,0:T(2,128)S(1)}, f32[2,2048]{1,0:T(2,128)S(1)}, u32[]{:S(2)}, u32[]{:S(2)}) %collective-permute-start) | collective-permute-done | bytes 16416 | tf_op jit(solution)/shard_map/ppermute | solution.py:163
  177.7 34.1 %collective-permute-start.1 = (bf16[128,2048]{1,0:T(8,128)(2,1)S(1)}, bf16[128,2048]{1,0:T(8,128)(2,1)S(1)}, u32[]{:S(2)}, u32[]{:S(2)}) collective-permute-start(bf16[128,2048]{1,0:T(8,128)(2,1)S(1)} %fusion.27.own_ref), channel_id=1, source_target_pairs={{0,1},{1,2},{2,3},{3,0},{4,5},{5,6},{6,7},{7,4},{8,9},{9,10},{10,1... | collective-permute-start | bytes 1572872 | tf_op jit(solution)/shard_map/ppermute | solution.py:18
  211.8 6.7 %collective-permute-done.1.left_ref = bf16[128,2048]{1,0:T(8,128)(2,1)S(1)} collective-permute-done((bf16[128,2048]{1,0:T(8,128)(2,1)S(1)}, bf16[128,2048]{1,0:T(8,128)(2,1)S(1)}, u32[]{:S(2)}, u32[]{:S(2)}) %collective-permute-start.1) | collective-permute-done | bytes 524320 | tf_op jit(solution)/shard_map/ppermute | solution.py:18
  218.5 0.8 slice.54
  219.3 3.7 %collective-permute-start.3 = (bf16[64,2048]{1,0:T(8,128)(2,1)}, bf16[64,2048]{1,0:T(8,128)(2,1)S(1)}, u32[]{:S(2)}, u32[]{:S(2)}) collective-permute-start(bf16[64,2048]{1,0:T(8,128)(2,1)} %slice.54), channel_id=1, source_target_pairs={{0,1},{1,2},{2,3},{3,0},{4,5},{5,6},{6,7},{7,4},{8,9},{9,10},{10,1... | collective-permute-start | bytes 786440 | tf_op jit(solution)/shard_map/ppermute | solution.py:18
  223.0 0.8 slice.55
  223.8 1.7 mix.1
  225.5 1.7 collective-permute-done.3.first_ref
  227.2 4.5 %collective-permute-done.4.second_ref = bf16[64,2048]{1,0:T(8,128)(2,1)} collective-permute-done((bf16[64,2048]{1,0:T(8,128)(2,1)}, bf16[64,2048]{1,0:T(8,128)(2,1)}, u32[]{:S(2)}, u32[]{:S(2)}) %collective-permute-start.4) | collective-permute-done | bytes 262176 | tf_op jit(solution)/shard_map/ppermute | solution.py:18
  231.7 4.7 %mixer.1 = bf16[512,512]{1,0:T(8,128)(2,1)} custom-call(s32[1]{0:T(128)} %bitcast.place_ref, bf16[128,2048]{1,0:T(8,128)(2,1)} %copy-done.1, bf16[128,2048]{1,0:T(8,128)(2,1)} %copy-done.4, bf16[128,2048]{1,0:T(8,128)(2,1)} %copy-done.5, bf16[64,2048]{1,0:T(8,128)(2,1)} %copy-done.17, bf16[64,2048]{1,0:T(8,128)(2,1)} %collective-permute-done.4.second_ref, ...), custom_call_target="tpu_custom_call" | custom-call | tf_op jit(solution)/shard_map/mixer/pallas_call | solution.py:191
  236.4 1.2 copy-done
  237.6 3.2 %combine.1 = bf16[128,2048]{1,0:T(8,128)(2,1)} custom-call(bf16[128,512]{1,0:T(8,128)(2,1)} %get-tuple-element.4.high_ref, bf16[128,512]{1,0:T(8,128)(2,1)} %get-tuple-element.5.low_ref, bf16[512,512]{1,0:T(8,128)(2,1)} %bitcast.56, bf16[512,1536]{1,0:T(8,128)(2,1)} %bitcast.54), custom_call_target="tpu_custom_call" | custom-call | tf_op jit(solution)/shard_map/combine/pallas_call | solution.py:199
  (79 shorter events, 6.0 us)
Async XLA Ops:
  3.9 60.1 %all-to-all-start = ((bf16[64,8,2048]{2,1,0:T(8,128)(2,1)}), bf16[64,8,2048]{2,1,0:T(8,128)(2,1)S(1)}, u32[]{:S(2)}, u32[]{:S(2)}) async-start(bf16[64,8,2048]{2,1,0:T(8,128)(2,1)} %bitcast.52), calls=%async_computation | async-start | bytes 4194304 | tf_op jit(solution)/shard_map/all_to_all | solution.py:149
  14.7 26.4 %collective-permute-start.5 = (bf16[2048,256]{1,0:T(8,128)(2,1)}, bf16[2048,256]{1,0:T(8,128)(2,1)}, u32[]{:S(2)}, u32[]{:S(2)}) collective-permute-start(bf16[2048,256]{1,0:T(8,128)(2,1)} %bitcast.67), channel_id=1, source_target_pairs={{0,1},{1,2},{2,3},{3,0},{4,5},{5,6},{6,7},{7,4},{8,9},{9,10},{10,1... | collective-permute-start | bytes 3145736 | tf_op jit(solution)/shard_map/ppermute | solution.py:18
  15.0 51.0 %collective-permute-start.8 = (bf16[2048,256]{1,0:T(8,128)(2,1)}, bf16[2048,256]{1,0:T(8,128)(2,1)}, u32[]{:S(2)}, u32[]{:S(2)}) collective-permute-start(bf16[2048,256]{1,0:T(8,128)(2,1)} %bitcast.69), channel_id=1, source_target_pairs={{0,3},{1,0},{2,1},{3,2},{4,7},{5,4},{6,5},{7,6},{8,11},{9,8},{10,9... | collective-permute-start | bytes 3145736 | tf_op jit(solution)/shard_map/ppermute | solution.py:18
  16.8 50.1 %collective-permute-start.7 = (bf16[2048,256]{1,0:T(8,128)(2,1)}, bf16[2048,256]{1,0:T(8,128)(2,1)}, u32[]{:S(2)}, u32[]{:S(2)}) collective-permute-start(bf16[2048,256]{1,0:T(8,128)(2,1)} %bitcast.68), channel_id=1, source_target_pairs={{0,3},{1,0},{2,1},{3,2},{4,7},{5,4},{6,5},{7,6},{8,11},{9,8},{10,9... | collective-permute-start | bytes 3145736 | tf_op jit(solution)/shard_map/ppermute | solution.py:18
  17.5 83.4 %collective-permute-start.6 = (bf16[2048,256]{1,0:T(8,128)(2,1)}, bf16[2048,256]{1,0:T(8,128)(2,1)}, u32[]{:S(2)}, u32[]{:S(2)}) collective-permute-start(bf16[2048,256]{1,0:T(8,128)(2,1)} %bitcast.70), channel_id=1, source_target_pairs={{0,1},{1,2},{2,3},{3,0},{4,5},{5,6},{6,7},{7,4},{8,9},{9,10},{10,1... | collective-permute-start | bytes 3145736 | tf_op jit(solution)/shard_map/ppermute | solution.py:18
  41.1 44.9 %collective-permute-start.9 = (bf16[2048,256]{1,0:T(8,128)(2,1)}, bf16[2048,256]{1,0:T(8,128)(2,1)}, u32[]{:S(2)}, u32[]{:S(2)}) collective-permute-start(bf16[2048,256]{1,0:T(8,128)(2,1)} %collective-permute-done.5), channel_id=1, source_target_pairs={{0,1},{1,2},{2,3},{3,0},{4,5},{5,6},{6,7},{7,4},{8,9},{9,10},{10,1... | collective-permute-start | bytes 3145736 | tf_op jit(solution)/shard_map/ppermute | solution.py:18
  43.5 22.5 %copy-start.8 = (bf16[256,256]{1,0:T(8,128)(2,1)}, bf16[256,256]{1,0:T(8,128)(2,1)S(1)}, u32[]{:S(2)}) copy-start(bf16[256,256]{1,0:T(8,128)(2,1)S(1)} %get-tuple-element.7.refs_4_) | copy-start | bytes 393220
  43.5 51.8 %copy-start.7 = (bf16[256,256]{1,0:T(8,128)(2,1)}, bf16[256,256]{1,0:T(8,128)(2,1)S(1)}, u32[]{:S(2)}) copy-start(bf16[256,256]{1,0:T(8,128)(2,1)S(1)} %get-tuple-element.6.refs_8_) | copy-start | bytes 393220
  43.5 55.2 %collective-permute-start.11 = (bf16[256,256]{1,0:T(8,128)(2,1)S(1)}, bf16[256,256]{1,0:T(8,128)(2,1)S(1)}, u32[]{:S(2)}, u32[]{:S(2)}) collective-permute-start(bf16[256,256]{1,0:T(8,128)(2,1)S(1)} %get-tuple-element.7.refs_4_), channel_id=1, source_target_pairs={{0,1},{1,2},{2,3},{3,0},{4,5},{5,6},{6,7},{7,4},{8,9},{9,10},{10,1... | collective-permute-start | bytes 393224 | tf_op jit(solution)/shard_map/ppermute | solution.py:18
  45.0 83.9 %copy-start.3 = (bf16[256,1024]{1,0:T(8,128)(2,1)}, bf16[256,1024]{1,0:T(8,128)(2,1)S(1)}, u32[]{:S(2)}) copy-start(bf16[256,1024]{1,0:T(8,128)(2,1)S(1)} %slice.58.refs_4_) | copy-start | bytes 1572868
  66.0 38.0 %collective-permute-start.12 = (bf16[256,256]{1,0:T(8,128)(2,1)S(1)}, bf16[256,256]{1,0:T(8,128)(2,1)S(1)}, u32[]{:S(2)}, u32[]{:S(2)}) collective-permute-start(bf16[256,256]{1,0:T(8,128)(2,1)S(1)} %get-tuple-element.7.refs_4_), channel_id=1, source_target_pairs={{0,3},{1,0},{2,1},{3,2},{4,7},{5,4},{6,5},{7,6},{8,11},{9,8},{10,9... | collective-permute-start | bytes 393224 | tf_op jit(solution)/shard_map/ppermute | solution.py:18
  66.8 28.5 %collective-permute-start.10 = (bf16[2048,256]{1,0:T(8,128)(2,1)}, bf16[2048,256]{1,0:T(8,128)(2,1)S(1)}, u32[]{:S(2)}, u32[]{:S(2)}) collective-permute-start(bf16[2048,256]{1,0:T(8,128)(2,1)} %collective-permute-done.8), channel_id=1, source_target_pairs={{0,3},{1,0},{2,1},{3,2},{4,7},{5,4},{6,5},{7,6},{8,11},{9,8},{10,9... | collective-permute-start | bytes 3145736 | tf_op jit(solution)/shard_map/ppermute | solution.py:18
  71.9 16.8 %copy-start.25 = (bf16[1,2048,256]{2,1,0:T(8,128)(2,1)S(1)}, bf16[1,2048,256]{2,1,0:T(8,128)(2,1)}, u32[]{:S(2)}) copy-start(bf16[1,2048,256]{2,1,0:T(8,128)(2,1)} %param.20) | copy-start | bytes 3145732
  86.0 13.3 %collective-permute-start.15 = (bf16[256,256]{1,0:T(8,128)(2,1)S(1)}, bf16[256,256]{1,0:T(8,128)(2,1)S(1)}, u32[]{:S(2)}, u32[]{:S(2)}) collective-permute-start(bf16[256,256]{1,0:T(8,128)(2,1)S(1)} %get-tuple-element.6.refs_8_), channel_id=1, source_target_pairs={{0,3},{1,0},{2,1},{3,2},{4,7},{5,4},{6,5},{7,6},{8,11},{9,8},{10,9... | collective-permute-start | bytes 393224 | tf_op jit(solution)/shard_map/ppermute | solution.py:18
  95.3 8.7 %collective-permute-start.14 = (bf16[256,256]{1,0:T(8,128)(2,1)S(1)}, bf16[256,256]{1,0:T(8,128)(2,1)S(1)}, u32[]{:S(2)}, u32[]{:S(2)}) collective-permute-start(bf16[256,256]{1,0:T(8,128)(2,1)S(1)} %get-tuple-element.6.refs_8_), channel_id=1, source_target_pairs={{0,1},{1,2},{2,3},{3,0},{4,5},{5,6},{6,7},{7,4},{8,9},{9,10},{10,1... | collective-permute-start | bytes 393224 | tf_op jit(solution)/shard_map/ppermute | solution.py:18
  98.7 5.4 %copy-start.19 = (bf16[256,256]{1,0:T(8,128)(2,1)}, bf16[256,256]{1,0:T(8,128)(2,1)S(1)}, u32[]{:S(2)}) copy-start(bf16[256,256]{1,0:T(8,128)(2,1)S(1)} %collective-permute-done.11.refs_5_) | copy-start | bytes 393220
  98.7 30.3 %collective-permute-start.17 = (bf16[256,1024]{1,0:T(8,128)(2,1)S(1)}, bf16[256,1024]{1,0:T(8,128)(2,1)S(1)}, u32[]{:S(2)}, u32[]{:S(2)}) collective-permute-start(bf16[256,1024]{1,0:T(8,128)(2,1)S(1)} %slice.58.refs_4_), channel_id=1, source_target_pairs={{0,1},{1,2},{2,3},{3,0},{4,5},{5,6},{6,7},{7,4},{8,9},{9,10},{10,1... | collective-permute-start | bytes 1572872 | tf_op jit(solution)/shard_map/ppermute | solution.py:18
  99.4 4.7 %copy-start.21 = (bf16[256,256]{1,0:T(8,128)(2,1)}, bf16[256,256]{1,0:T(8,128)(2,1)S(1)}, u32[]{:S(2)}) copy-start(bf16[256,256]{1,0:T(8,128)(2,1)S(1)} %collective-permute-done.15.refs_10_) | copy-start | bytes 393220
  99.4 13.9 %collective-permute-start.13 = (bf16[256,256]{1,0:T(8,128)(2,1)S(1)}, bf16[256,256]{1,0:T(8,128)(2,1)S(1)}, u32[]{:S(2)}, u32[]{:S(2)}) collective-permute-start(bf16[256,256]{1,0:T(8,128)(2,1)S(1)} %collective-permute-done.11.refs_5_), channel_id=1, source_target_pairs={{0,1},{1,2},{2,3},{3,0},{4,5},{5,6},{6,7},{7,4},{8,9},{9,10},{10,1... | collective-permute-start | bytes 393224 | tf_op jit(solution)/shard_map/ppermute | solution.py:18
  100.9 13.0 %collective-permute-start.16 = (bf16[256,256]{1,0:T(8,128)(2,1)S(1)}, bf16[256,256]{1,0:T(8,128)(2,1)}, u32[]{:S(2)}, u32[]{:S(2)}) collective-permute-start(bf16[256,256]{1,0:T(8,128)(2,1)S(1)} %collective-permute-done.15.refs_10_), channel_id=1, source_target_pairs={{0,3},{1,0},{2,1},{3,2},{4,7},{5,4},{6,5},{7,6},{8,11},{9,8},{10,9... | collective-permute-start | bytes 393224 | tf_op jit(solution)/shard_map/ppermute | solution.py:18
  104.1 9.2 %copy-start.20 = (bf16[256,256]{1,0:T(8,128)(2,1)}, bf16[256,256]{1,0:T(8,128)(2,1)S(1)}, u32[]{:S(2)}) copy-start(bf16[256,256]{1,0:T(8,128)(2,1)S(1)} %collective-permute-done.12.refs_6_) | copy-start | bytes 393220
  104.1 9.2 %copy-start.22 = (bf16[256,256]{1,0:T(8,128)(2,1)}, bf16[256,256]{1,0:T(8,128)(2,1)S(1)}, u32[]{:S(2)}) copy-start(bf16[256,256]{1,0:T(8,128)(2,1)S(1)} %collective-permute-done.14.refs_9_) | copy-start | bytes 393220
  117.0 44.0 %all-to-all-start.1 = ((bf16[64,8,512]{2,1,0:T(8,128)(2,1)}), bf16[64,8,512]{2,1,0:T(8,128)(2,1)S(1)}, u32[]{:S(2)}, u32[]{:S(2)}) async-start(bf16[64,8,512]{2,1,0:T(8,128)(2,1)} %bitcast.55), calls=%async_computation.1 | async-start | bytes 1048576 | tf_op jit(solution)/shard_map/all_to_all | solution.py:186
  127.1 27.2 %copy-start.6 = (bf16[256,512]{1,0:T(8,128)(2,1)}, bf16[256,512]{1,0:T(8,128)(2,1)S(1)}, u32[]{:S(2)}) copy-start(bf16[256,512]{1,0:T(8,128)(2,1)S(1)} %slice.59.refs_8_) | copy-start | bytes 786436
  127.1 10.5 %collective-permute-start.21 = (bf16[256,512]{1,0:T(8,128)(2,1)S(1)}, bf16[256,512]{1,0:T(8,128)(2,1)S(1)}, u32[]{:S(2)}, u32[]{:S(2)}) collective-permute-start(bf16[256,512]{1,0:T(8,128)(2,1)S(1)} %slice.59.refs_8_), channel_id=1, source_target_pairs={{0,3},{1,0},{2,1},{3,2},{4,7},{5,4},{6,5},{7,6},{8,11},{9,8},{10,9... | collective-permute-start | bytes 786440 | tf_op jit(solution)/shard_map/ppermute | solution.py:18
  128.9 24.7 %collective-permute-start.18 = (bf16[256,1024]{1,0:T(8,128)(2,1)S(1)}, bf16[256,1024]{1,0:T(8,128)(2,1)S(1)}, u32[]{:S(2)}, u32[]{:S(2)}) collective-permute-start(bf16[256,1024]{1,0:T(8,128)(2,1)S(1)} %slice.58.refs_4_), channel_id=1, source_target_pairs={{0,3},{1,0},{2,1},{3,2},{4,7},{5,4},{6,5},{7,6},{8,11},{9,8},{10,9... | collective-permute-start | bytes 1572872 | tf_op jit(solution)/shard_map/ppermute | solution.py:18
  129.1 25.3 %copy-start.12 = (bf16[256,1024]{1,0:T(8,128)(2,1)}, bf16[256,1024]{1,0:T(8,128)(2,1)S(1)}, u32[]{:S(2)}) copy-start(bf16[256,1024]{1,0:T(8,128)(2,1)S(1)} %collective-permute-done.17.refs_5_) | copy-start | bytes 1572868
  129.1 25.3 %collective-permute-start.19 = (bf16[256,1024]{1,0:T(8,128)(2,1)S(1)}, bf16[256,1024]{1,0:T(8,128)(2,1)S(1)}, u32[]{:S(2)}, u32[]{:S(2)}) collective-permute-start(bf16[256,1024]{1,0:T(8,128)(2,1)S(1)} %collective-permute-done.17.refs_5_), channel_id=1, source_target_pairs={{0,1},{1,2},{2,3},{3,0},{4,5},{5,6},{6,7},{7,4},{8,9},{9,10},{10,1... | collective-permute-start | bytes 1572872 | tf_op jit(solution)/shard_map/ppermute | solution.py:18
  132.2 16.5 %collective-permute-start.20 = (bf16[256,512]{1,0:T(8,128)(2,1)S(1)}, bf16[256,512]{1,0:T(8,128)(2,1)S(1)}, u32[]{:S(2)}, u32[]{:S(2)}) collective-permute-start(bf16[256,512]{1,0:T(8,128)(2,1)S(1)} %slice.59.refs_8_), channel_id=1, source_target_pairs={{0,1},{1,2},{2,3},{3,0},{4,5},{5,6},{6,7},{7,4},{8,9},{9,10},{10,1... | collective-permute-start | bytes 786440 | tf_op jit(solution)/shard_map/ppermute | solution.py:18
  137.6 16.7 %copy-start.15 = (bf16[256,512]{1,0:T(8,128)(2,1)}, bf16[256,512]{1,0:T(8,128)(2,1)S(1)}, u32[]{:S(2)}) copy-start(bf16[256,512]{1,0:T(8,128)(2,1)S(1)} %collective-permute-done.21.refs_10_) | copy-start | bytes 786436
  137.6 16.0 %collective-permute-start.22 = (bf16[256,512]{1,0:T(8,128)(2,1)S(1)}, bf16[256,512]{1,0:T(8,128)(2,1)S(1)}, u32[]{:S(2)}, u32[]{:S(2)}) collective-permute-start(bf16[256,512]{1,0:T(8,128)(2,1)S(1)} %collective-permute-done.21.refs_10_), channel_id=1, source_target_pairs={{0,3},{1,0},{2,1},{3,2},{4,7},{5,4},{6,5},{7,6},{8,11},{9,8},{10,9... | collective-permute-start | bytes 786440 | tf_op jit(solution)/shard_map/ppermute | solution.py:18
  148.7 5.6 %copy-start.16 = (bf16[256,512]{1,0:T(8,128)(2,1)}, bf16[256,512]{1,0:T(8,128)(2,1)S(1)}, u32[]{:S(2)}) copy-start(bf16[256,512]{1,0:T(8,128)(2,1)S(1)} %collective-permute-done.20.refs_9_) | copy-start | bytes 786436
  161.0 10.5 %copy-start.9 = (bf16[128,2048]{1,0:T(8,128)(2,1)S(1)}, bf16[128,2048]{1,0:T(8,128)(2,1)}, u32[]{:S(2)}) copy-start(bf16[128,2048]{1,0:T(8,128)(2,1)} %param.14) | copy-start | bytes 1572868
  161.0 10.5 %copy-start.10 = (bf16[128,2048]{1,0:T(8,128)(2,1)S(1)}, bf16[128,2048]{1,0:T(8,128)(2,1)}, u32[]{:S(2)}) copy-start(bf16[128,2048]{1,0:T(8,128)(2,1)} %param.13) | copy-start | bytes 1572868
  161.0 10.6 %copy-start.2 = (bf16[64,8,512]{2,1,0:T(8,128)(2,1)}, bf16[64,8,512]{2,1,0:T(8,128)(2,1)S(1)}, u32[]{:S(2)}) copy-start(bf16[64,8,512]{2,1,0:T(8,128)(2,1)S(1)} %all-to-all-done.1) | copy-start | bytes 1572868
  161.0 12.8 %copy-start.24 = (bf16[3,2048]{1,0:T(4,128)(2,1)S(1)}, bf16[3,2048]{1,0:T(4,128)(2,1)}, u32[]{:S(2)}) copy-start(bf16[3,2048]{1,0:T(4,128)(2,1)} %param.15) | copy-start | bytes 36868
  161.0 75.4 %all-to-all-start.2 = ((bf16[64,8,1536]{2,1,0:T(8,128)(2,1)}), bf16[64,8,1536]{2,1,0:T(8,128)(2,1)S(1)}, u32[]{:S(2)}, u32[]{:S(2)}) async-start(bf16[64,8,1536]{2,1,0:T(8,128)(2,1)} %bitcast.53), calls=%async_computation.2 | async-start | bytes 3145728 | tf_op jit(solution)/shard_map/all_to_all | solution.py:186
  171.5 5.8 %copy-start.11 = (bf16[128,2048]{1,0:T(8,128)(2,1)S(1)}, bf16[128,2048]{1,0:T(8,128)(2,1)}, u32[]{:S(2)}) copy-start(bf16[128,2048]{1,0:T(8,128)(2,1)} %param.12) | copy-start | bytes 1572868
  171.7 5.6 %collective-permute-start = (f32[2,2048]{1,0:T(2,128)S(1)}, f32[2,2048]{1,0:T(2,128)S(1)}, u32[]{:S(2)}, u32[]{:S(2)}) collective-permute-start(f32[2,2048]{1,0:T(2,128)S(1)} %slice.48), channel_id=1, source_target_pairs={{0,1},{1,2},{2,3},{3,4},{4,5},{5,6},{6,7},{7,8},{8,9},{9,10},{10,1... | collective-permute-start | bytes 49160 | tf_op jit(solution)/shard_map/ppermute | solution.py:163
  177.7 54.0 %copy-start.1 = (bf16[128,2048]{1,0:T(8,128)(2,1)}, bf16[128,2048]{1,0:T(8,128)(2,1)S(1)}, u32[]{:S(2)}) copy-start(bf16[128,2048]{1,0:T(8,128)(2,1)S(1)} %fusion.27.own_ref) | copy-start | bytes 1572868
  177.7 40.8 %collective-permute-start.1 = (bf16[128,2048]{1,0:T(8,128)(2,1)S(1)}, bf16[128,2048]{1,0:T(8,128)(2,1)S(1)}, u32[]{:S(2)}, u32[]{:S(2)}) collective-permute-start(bf16[128,2048]{1,0:T(8,128)(2,1)S(1)} %fusion.27.own_ref), channel_id=1, source_target_pairs={{0,1},{1,2},{2,3},{3,0},{4,5},{5,6},{6,7},{7,4},{8,9},{9,10},{10,1... | collective-permute-start | bytes 1572872 | tf_op jit(solution)/shard_map/ppermute | solution.py:18
  211.8 11.2 %collective-permute-start.2 = (bf16[128,2048]{1,0:T(8,128)(2,1)S(1)}, bf16[128,2048]{1,0:T(8,128)(2,1)S(1)}, u32[]{:S(2)}, u32[]{:S(2)}) collective-permute-start(bf16[128,2048]{1,0:T(8,128)(2,1)S(1)} %fusion.27.own_ref), channel_id=1, source_target_pairs={{0,3},{1,0},{2,1},{3,2},{4,7},{5,4},{6,5},{7,6},{8,11},{9,8},{10,9... | collective-permute-start | bytes 1572872 | tf_op jit(solution)/shard_map/ppermute | solution.py:18
  218.5 13.1 %copy-start.4 = (bf16[128,2048]{1,0:T(8,128)(2,1)}, bf16[128,2048]{1,0:T(8,128)(2,1)S(1)}, u32[]{:S(2)}) copy-start(bf16[128,2048]{1,0:T(8,128)(2,1)S(1)} %collective-permute-done.1.left_ref) | copy-start | bytes 1572868
  219.3 7.9 %collective-permute-start.3 = (bf16[64,2048]{1,0:T(8,128)(2,1)}, bf16[64,2048]{1,0:T(8,128)(2,1)S(1)}, u32[]{:S(2)}, u32[]{:S(2)}) collective-permute-start(bf16[64,2048]{1,0:T(8,128)(2,1)} %slice.54), channel_id=1, source_target_pairs={{0,1},{1,2},{2,3},{3,0},{4,5},{5,6},{6,7},{7,4},{8,9},{9,10},{10,1... | collective-permute-start | bytes 786440 | tf_op jit(solution)/shard_map/ppermute | solution.py:18
  223.0 8.7 %copy-start.5 = (bf16[128,2048]{1,0:T(8,128)(2,1)}, bf16[128,2048]{1,0:T(8,128)(2,1)S(1)}, u32[]{:S(2)}) copy-start(bf16[128,2048]{1,0:T(8,128)(2,1)S(1)} %collective-permute-done.2.right_ref) | copy-start | bytes 1572868
  223.8 7.9 %collective-permute-start.4 = (bf16[64,2048]{1,0:T(8,128)(2,1)}, bf16[64,2048]{1,0:T(8,128)(2,1)}, u32[]{:S(2)}, u32[]{:S(2)}) collective-permute-start(bf16[64,2048]{1,0:T(8,128)(2,1)} %slice.55), channel_id=1, source_target_pairs={{0,3},{1,0},{2,1},{3,2},{4,7},{5,4},{6,5},{7,6},{8,11},{9,8},{10,9... | collective-permute-start | bytes 786440 | tf_op jit(solution)/shard_map/ppermute | solution.py:18
  227.2 4.5 %copy-start.17 = (bf16[64,2048]{1,0:T(8,128)(2,1)}, bf16[64,2048]{1,0:T(8,128)(2,1)S(1)}, u32[]{:S(2)}) copy-start(bf16[64,2048]{1,0:T(8,128)(2,1)S(1)} %collective-permute-done.3.first_ref) | copy-start | bytes 786436
  236.4 1.2 copy-start
  (4 other events, 2.9 us)
where the time goes:
time: 242 us; the launch traced here: 241 us
  waiting for transfers between devices  106 us (44%)
  starting transfers between devices  88.1 us (36%)
  Pallas kernels  21 us (9%)
  matrix products  15.8 us (7%)
  local copies, waits for them, and re-layouts  8.77 us (4%)
    ppermute x22, waiting for transfers between devices, turn(): return lax.ppermute(value, 'tp', pairs)  83.1 us
    ppermute x22, starting transfers between devices, turn(): return lax.ppermute(value, 'tp', pairs)  55.6 us
    all_to_all x2, starting transfers between devices, local(): lax.all_to_all(result.reshape(expert_count, slot_cap, width), 'ep', 0, 0,...  19.6 us
    all_to_all x1, waiting for transfers between devices, local(): lax.all_to_all(outgoing.reshape(expert_count, slot_cap, model_width), 'ep...  19 us
    dot_general x8, matrix products, dot32(): return jnp.dot(a, b, preferred_element_type=jnp.float32)  15.8 us
    all_to_all x1, starting transfers between devices, local(): lax.all_to_all(outgoing.reshape(expert_count, slot_cap, model_width), 'ep...  10.7 us
    pallas_call x2, Pallas kernels, local(): pl.pallas_call(down_kernel, out_shape=jax.ShapeDtypeStruct((slots, width)...  8.1 us
  transfers between devices with their start and end apart: 26, of which 12 were waited for; matrix products, arithmetic and copies ran while one was open for 9% of the time, Pallas kernels for 6%

commit v1 on v0

--- a/solution.py
+++ b/solution.py
@@ -8,8 +8,10 @@
 
 CONV = 3
 NORM_EPS = 1e-06
-PIECES = (256, 256, 1024, 512)
-CHUNKS = ((0, 1), (2, 3))
+PIECES = (384, 384, 768, 512)
+CHUNKS = (((0, 1), 384), ((2, 3), 256))
+DEPTH = 512
+COLUMNS = 256
 
 
 def turn(value, steps):
@@ -55,32 +57,110 @@
     out_ref[...] = jnp.dot(table, normed, preferred_element_type=jnp.float32).astype(jnp.bfloat16)
 
 
-def mix_kernel(ids_ref, weight_ref, high_ref, low_ref, *, expert_count, slot_cap):
+def mix_kernel(ids_ref, weight_ref, out_ref, *, expert_count, slot_cap):
     weight = weight_ref[...]
+    tokens = weight.shape[1]
     share = weight / (weight[0:1] + weight[1:2])
     tables = slot_table(ids_ref[...], expert_count, slot_cap)
     mix = (tables[0] * share[0:1] + tables[1] * share[1:2]).T
     high = mix.astype(jnp.bfloat16)
-    high_ref[...] = high
-    low_ref[...] = (mix - high.astype(jnp.float32)).astype(jnp.bfloat16)
-
-
-def combine_kernel(high_ref, low_ref, *refs):
-    out_ref, at = refs[-1], 0
-    for ref in refs[:-1]:
-        rows = ref[...]
-        picked = dot32(high_ref[...], rows) + dot32(low_ref[...], rows)
-        out_ref[:, at : at + rows.shape[1]] = picked.astype(jnp.bfloat16)
-        at += rows.shape[1]
-
-
-def down_kernel(*refs):
-    out_ref, hidden, downs, at = refs[-1], refs[:4], refs[4:-1], 0
-    for i in range(0, len(downs), 4):
-        own = downs[i]
-        total = sum(dot32(h[...], d[...]) for h, d in zip(hidden, downs[i : i + 4]))
-        out_ref[:, at : at + own.shape[1]] = total.astype(jnp.bfloat16)
-        at += own.shape[1]
+    out_ref[:tokens] = high
+    out_ref[tokens:] = (mix - high.astype(jnp.float32)).astype(jnp.bfloat16)
+
+
+def combine_kernel(mix_ref, rows_ref, *refs):
+    out_ref = refs[-1]
+    both = dot32(mix_ref[...], rows_ref[...])
+    tokens = out_ref.shape[0]
+    out_ref[...] = (both[:tokens] + both[tokens:]).astype(jnp.bfloat16)
+
+
+def combine(mix, rows, at, width, before):
+    tokens, slots = mix.shape[0] // 2, mix.shape[1]
+    first = at // COLUMNS
+    return pl.pallas_call(
+        combine_kernel,
+        out_shape=jax.ShapeDtypeStruct((tokens, width), jnp.bfloat16),
+        grid=(rows.shape[1] // COLUMNS,),
+        in_specs=[
+            pl.BlockSpec(mix.shape, lambda j: (0, 0)),
+            pl.BlockSpec((slots, COLUMNS), lambda j: (0, j)),
+        ]
+        + [pl.BlockSpec(memory_space=pl.ANY)] * len(before),
+        out_specs=pl.BlockSpec((tokens, COLUMNS), lambda j: (0, j + first)),
+        input_output_aliases={2: 0} if before else {},
+    )(mix, rows, *before)
+
+
+def hidden_kernel(*refs, count):
+    rows = refs[0][...]
+    weights, outs, sums = refs[1 : 1 + 2 * count], refs[1 + 2 * count : 1 + 3 * count], refs[1 + 3 * count :]
+    step = pl.program_id(0)
+    products = [dot32(rows, w[...]) for w in weights]
+
+    @pl.when(step == 0)
+    def _():
+        for total, product in zip(sums, products):
+            total[...] = product
+
+    @pl.when(step > 0)
+    def _():
+        for total, product in zip(sums, products):
+            total[...] += product
+
+    @pl.when(step == pl.num_programs(0) - 1)
+    def _():
+        for i, out in enumerate(outs):
+            gate = sums[2 * i][...]
+            out[...] = (gate / (1.0 + jnp.exp(-gate)) * sums[2 * i + 1][...]).astype(jnp.bfloat16)
+
+
+def hidden_of(rows, pairs):
+    slots, width = rows.shape
+    units = pairs[0][0].shape[1]
+    weights = [w for pair in pairs for w in pair]
+    return pl.pallas_call(
+        lambda *refs: hidden_kernel(*refs, count=len(pairs)),
+        out_shape=[jax.ShapeDtypeStruct((slots, units), jnp.bfloat16)] * len(pairs),
+        grid=(width // DEPTH,),
+        in_specs=[pl.BlockSpec((slots, DEPTH), lambda k: (0, k))]
+        + [pl.BlockSpec((DEPTH, units), lambda k: (k, 0))] * len(weights),
+        out_specs=[pl.BlockSpec((slots, units), lambda k: (0, 0))] * len(pairs),
+        scratch_shapes=[pltpu.VMEM((slots, units), jnp.float32)] * len(weights),
+    )(rows, *weights)
+
+
+def down_kernel(*refs, counts):
+    hidden, downs, out_ref = refs[:4], refs[4:-1], refs[-1]
+    step, first = pl.program_id(0), 0
+    for i, count in enumerate(counts):
+
+        @pl.when((step >= first) & (step < first + count))
+        def _():
+            total = sum(dot32(h[...], d[...]) for h, d in zip(hidden, downs[4 * i : 4 * i + 4]))
+            out_ref[...] = total.astype(jnp.bfloat16)
+
+        first += count
+
+
+def down_of(hidden, pieces, block):
+    slots, units = hidden[0].shape
+    counts = [piece[0].shape[1] // block for piece in pieces]
+    specs, first = [pl.BlockSpec((slots, units), lambda j: (0, 0))] * 4, 0
+    for count in counts:
+        specs += [
+            pl.BlockSpec(
+                (units, block), lambda j, first=first, count=count: (0, jnp.clip(j - first, 0, count - 1))
+            )
+        ] * 4
+        first += count
+    return pl.pallas_call(
+        lambda *refs: down_kernel(*refs, counts=counts),
+        out_shape=jax.ShapeDtypeStruct((slots, first * block), jnp.bfloat16),
+        grid=(first,),
+        in_specs=specs,
+        out_specs=pl.BlockSpec((slots, block), lambda j: (0, j)),
+    )(*hidden, *[d for piece in pieces for d in piece])
 
 
 def mixer_kernel(place_ref, own_ref, left_ref, right_ref, first_ref, second_ref, weight_ref, out_ref):
@@ -151,9 +231,9 @@
     ).reshape(slots, model_width)
     mix = pl.pallas_call(
         lambda *refs: mix_kernel(*refs, expert_count=expert_count, slot_cap=slot_cap),
-        out_shape=[jax.ShapeDtypeStruct((token_count, slots), jnp.bfloat16)] * 2,
+        out_shape=jax.ShapeDtypeStruct((2 * token_count, slots), jnp.bfloat16),
         in_specs=[vmem] * 2,
-        out_specs=[vmem] * 2,
+        out_specs=vmem,
         name="mix",
     )(ids_t, weight_t)
 
@@ -168,23 +248,16 @@
     smoothed = sum(padded[j : j + row_count] * taps[j] for j in range(CONV))
     gated = (out_gate.astype(jnp.float32) * smoothed).astype(jnp.bfloat16)
 
-    hidden = [
-        (jax.nn.silu(dot32(arrived, g)) * dot32(arrived, u)).astype(jnp.bfloat16)
-        for g, u in zip((gate, *gates, gate_far), (up, *ups, up_far))
-    ]
-
-    returned = []
-    for chunk in CHUNKS:
-        operands = [d for piece in chunk for d in downs[piece]]
-        width = sum(PIECES[piece] for piece in chunk)
-        result = pl.pallas_call(
-            down_kernel,
-            out_shape=jax.ShapeDtypeStruct((slots, width), jnp.bfloat16),
-            in_specs=[vmem] * (4 + len(operands)),
-            out_specs=vmem,
-        )(*hidden, *operands)
+    hidden = hidden_of(arrived, list(zip((gate, *gates), (up, *ups))))
+    hidden += hidden_of(arrived, [(gate_far, up_far)])
+
+    results, at = [], 0
+    for chunk, block in CHUNKS:
+        result = down_of(hidden, [downs[piece] for piece in chunk], block)
+        width = result.shape[1]
         back = lax.all_to_all(result.reshape(expert_count, slot_cap, width), "ep", 0, 0, tiled=True)
-        returned.append(back.reshape(slots, width))
+        results = [combine(mix, back.reshape(slots, width), at, model_width, results)]
+        at += width
 
     gated_sides = from_sides(gated)
     gated_far = from_opposite(*gated_sides)
@@ -196,14 +269,7 @@
         name="mixer",
     )(lax.axis_index("tp").reshape(1), gated, *gated_sides, *gated_far, mixer_weight)
 
-    experts_out = pl.pallas_call(
-        combine_kernel,
-        out_shape=jax.ShapeDtypeStruct((token_count, model_width), jnp.bfloat16),
-        in_specs=[vmem] * (2 + len(returned)),
-        out_specs=vmem,
-        name="combine",
-    )(*mix, *returned)
-    return (mixer_out, experts_out)
+    return (mixer_out, results[0])
 
 
 def solution(mesh):

time: 242 us -> 249 us (1.029)
  Pallas kernels: 21 us -> 40.6 us
  matrix products: 15.8 us -> 0 us
    ppermute x22, waiting for transfers between devices: 83.1 us -> 106 us  [turn(): return lax.ppermute(value, 'tp', pairs)]
    pallas_call x3 -> x6, Pallas kernels: 11.3 us -> 30.9 us  [the longest x2 13.1 us: hidden_of(): pl.pallas_call(lambda *refs: hidden_kernel(*refs, count=len(pairs)), out_...]
    all_to_all x1, waiting for transfers between devices: 19 us -> 0.01 us  [local(): lax.all_to_all(outgoing.reshape(expert_count, slot_cap, model_width), 'ep...]
    dot_general x8 -> x0, matrix products: 15.8 us -> none  [dot32(): return jnp.dot(a, b, preferred_element_type=jnp.float32)]
    ppermute x1, starting transfers between devices: 2.17 us -> 5.33 us  [local(): lax.ppermute(product[row_count - tap_span:], ('ep', 'tp'), [(i, i + 1) fo...]
    ppermute x22, starting transfers between devices: 55.6 us -> 52.8 us  [turn(): return lax.ppermute(value, 'tp', pairs)]
    unnamed x52 -> x54, local copies, waits for them, and re-layouts: 4.16 us -> 6.22 us
  transfers between devices with their start and end apart: 26 -> 26, of which waited for: 12 -> 9; matrix products, arithmetic and copies ran while one was open for 9% -> 1% of each run, Pallas kernels for 6% -> 12%
where the time goes in v1:
time: 249 us; the launch traced here: 248 us
  waiting for transfers between devices  107 us (43%)
  starting transfers between devices  89.6 us (36%)
  Pallas kernels  40.6 us (16%)
  local copies, waits for them, and re-layouts  8.91 us (4%)
    ppermute x22, waiting for transfers between devices, turn(): return lax.ppermute(value, 'tp', pairs)  106 us
    ppermute x22, starting transfers between devices, turn(): return lax.ppermute(value, 'tp', pairs)  52.8 us
    all_to_all x2, starting transfers between devices, local(): lax.all_to_all(result.reshape(expert_count, slot_cap, width), 'ep', 0, 0,...  20.7 us
    pallas_call x2, Pallas kernels, hidden_of(): pl.pallas_call(lambda *refs: hidden_kernel(*refs, count=len(pairs)), out_...  13.1 us
    all_to_all x1, starting transfers between devices, local(): lax.all_to_all(outgoing.reshape(expert_count, slot_cap, model_width), 'ep...  10.7 us
    pallas_call x2, Pallas kernels, down_of(): pl.pallas_call(lambda *refs: down_kernel(*refs, counts=counts), out_shape...  10.4 us
    pallas_call x2, Pallas kernels, combine(): pl.pallas_call(combine_kernel, out_shape=jax.ShapeDtypeStruct((tokens, wi...  7.45 us
    unnamed x54, local copies, waits for them, and re-layouts  6.22 us
  transfers between devices with their start and end apart: 26, of which 9 were waited for; matrix products, arithmetic and copies ran while one was open for 1% of the time, Pallas kernels for 12%

profile of v1, /device:TPU:120, one launch (start us, length us, event | category | flops | bytes accessed | tf_op | source)
XLA Modules:
  0.0 247.9 jit_solution(11057361221824021442)
XLA Ops:
  0.6 3.3 %dispatch.1 = bf16[512,2048]{1,0:T(8,128)(2,1)} custom-call(s32[2,128]{1,0:T(2,128)} %bitcast.30, bf16[128,2048]{1,0:T(8,128)(2,1)} %refs_1_.1, f32[1,2048]{1,0:T(1,128)} %bitcast.29), custom_call_target="tpu_custom_call" | custom-call | tf_op jit(solution)/shard_map/dispatch/pallas_call | solution.py:222
  3.9 10.7 %all-to-all-start = ((bf16[64,8,2048]{2,1,0:T(8,128)(2,1)}), bf16[64,8,2048]{2,1,0:T(8,128)(2,1)S(1)}, u32[]{:S(2)}, u32[]{:S(2)}) async-start(bf16[64,8,2048]{2,1,0:T(8,128)(2,1)} %bitcast.18), calls=%async_computation | async-start | bytes 4194304 | tf_op jit(solution)/shard_map/all_to_all | solution.py:229
  14.7 0.8 collective-permute-start.8
  15.5 2.5 %collective-permute-start.5 = (bf16[2048,256]{1,0:T(8,128)(2,1)}, bf16[2048,256]{1,0:T(8,128)(2,1)}, u32[]{:S(2)}, u32[]{:S(2)}) collective-permute-start(bf16[2048,256]{1,0:T(8,128)(2,1)} %bitcast.9.refs_1_), channel_id=1, source_target_pairs={{0,1},{1,2},{2,3},{3,0},{4,5},{5,6},{6,7},{7,4},{8,9},{9,10},{10,1... | collective-permute-start | bytes 3145736 | tf_op jit(solution)/shard_map/ppermute | solution.py:20
  18.0 2.0 collective-permute-start.7
  20.0 22.2 %collective-permute-done.8.refs_6_ = bf16[2048,256]{1,0:T(8,128)(2,1)S(1)} collective-permute-done((bf16[2048,256]{1,0:T(8,128)(2,1)}, bf16[2048,256]{1,0:T(8,128)(2,1)S(1)}, u32[]{:S(2)}, u32[]{:S(2)}) %collective-permute-start.8) | collective-permute-done | bytes 1048608 | tf_op jit(solution)/shard_map/ppermute | solution.py:20
  42.2 3.3 %collective-permute-start.9 = (bf16[2048,256]{1,0:T(8,128)(2,1)}, bf16[2048,256]{1,0:T(8,128)(2,1)}, u32[]{:S(2)}, u32[]{:S(2)}) collective-permute-start(bf16[2048,256]{1,0:T(8,128)(2,1)} %collective-permute-done.5.refs_3_), channel_id=1, source_target_pairs={{0,1},{1,2},{2,3},{3,0},{4,5},{5,6},{6,7},{7,4},{8,9},{9,10},{10,1... | collective-permute-start | bytes 3145736 | tf_op jit(solution)/shard_map/ppermute | solution.py:20
  45.5 1.1 fusion.7
  46.7 43.1 %collective-permute-done.17.refs_5_ = bf16[256,384]{1,0:T(8,128)(2,1)} collective-permute-done((bf16[256,384]{1,0:T(8,128)(2,1)S(1)}, bf16[256,384]{1,0:T(8,128)(2,1)}, u32[]{:S(2)}, u32[]{:S(2)}) %collective-permute-start.17) | collective-permute-done | bytes 196640 | tf_op jit(solution)/shard_map/ppermute | solution.py:20
  89.9 0.5 collective-permute-start.21
  90.3 7.4 %collective-permute-done.21.refs_10_ = bf16[256,384]{1,0:T(8,128)(2,1)} collective-permute-done((bf16[256,384]{1,0:T(8,128)(2,1)S(1)}, bf16[256,384]{1,0:T(8,128)(2,1)}, u32[]{:S(2)}, u32[]{:S(2)}) %collective-permute-start.21) | collective-permute-done | bytes 196640 | tf_op jit(solution)/shard_map/ppermute | solution.py:20
  97.7 3.2 %collective-permute-start.20 = (bf16[256,384]{1,0:T(8,128)(2,1)S(1)}, bf16[256,384]{1,0:T(8,128)(2,1)}, u32[]{:S(2)}, u32[]{:S(2)}) collective-permute-start(bf16[256,384]{1,0:T(8,128)(2,1)S(1)} %get-tuple-element.8.refs_8_), channel_id=1, source_target_pairs={{0,1},{1,2},{2,3},{3,0},{4,5},{5,6},{6,7},{7,4},{8,9},{9,10},{10,1... | collective-permute-start | bytes 589832 | tf_op jit(solution)/shard_map/ppermute | solution.py:20
  101.0 0.5 collective-permute-start.19
  101.5 0.5 copy-done.12
  102.0 1.3 collective-permute-start.22
  103.3 1.3 copy-done
  104.6 8.2 %shard_map.131 = (bf16[512,256]{1,0:T(8,128)(2,1)}, bf16[512,256]{1,0:T(8,128)(2,1)}, bf16[512,256]{1,0:T(8,128)(2,1)}) custom-call(bf16[512,2048]{1,0:T(8,128)(2,1)} %bitcast.16, bf16[2048,256]{1,0:T(8,128)(2,1)} %bitcast.9.refs_1_, bf16[2048,256]{1,0:T(8,128)(2,1)} %bitcast.10.refs_2_, bf16[2048,256]{1,0:T(8,128)(2,1)} %collective-permute-done.5.refs_3_, ...), custom_call_target="tpu_custom_call" | custom-call | tf_op jit(solution)/shard_map/pallas_call | solution.py:122
  112.8 4.9 %shard_map.132.refs_3_ = bf16[512,256]{1,0:T(8,128)(2,1)} custom-call(bf16[512,2048]{1,0:T(8,128)(2,1)} %bitcast.17, bf16[2048,256]{1,0:T(8,128)(2,1)} %collective-permute-done.9.refs_1_, bf16[2048,256]{1,0:T(8,128)(2,1)} %copy-done.7), custom_call_target="tpu_custom_call" | custom-call | tf_op jit(solution)/shard_map/pallas_call | solution.py:122
  117.8 4.1 %shard_map.134 = bf16[512,768]{1,0:T(8,128)(2,1)} custom-call(bf16[512,256]{1,0:T(8,128)(2,1)} %get-tuple-element.5.refs_0_, bf16[512,256]{1,0:T(8,128)(2,1)} %get-tuple-element.6.refs_1_, bf16[512,256]{1,0:T(8,128)(2,1)} %get-tuple-element.7.refs_2_, bf16[512,256]{1,0:T(8,128)(2,1)} %shard_map.132.refs_3_, bf16[256,384]{1,0:T(8,128)(2,1)} %copy-done.14, ...), custom_call_target="tpu_custom_call" | custom-call | tf_op jit(solution)/shard_map/pallas_call | solution.py:157
  121.9 10.4 %all-to-all-start.2 = ((bf16[64,8,768]{2,1,0:T(8,128)(2,1)}), bf16[64,8,768]{2,1,0:T(8,128)(2,1)S(1)}, u32[]{:S(2)}, u32[]{:S(2)}) async-start(bf16[64,8,768]{2,1,0:T(8,128)(2,1)} %bitcast.22), calls=%async_computation.2 | async-start | bytes 1572864 | tf_op jit(solution)/shard_map/all_to_all | solution.py:258
  132.4 2.0 collective-permute-start.11
  134.5 0.1 collective-permute-start.15
  134.7 8.9 %collective-permute-done.11.refs_5_ = bf16[256,768]{1,0:T(8,128)(2,1)S(1)} collective-permute-done((bf16[256,768]{1,0:T(8,128)(2,1)S(1)}, bf16[256,768]{1,0:T(8,128)(2,1)S(1)}, u32[]{:S(2)}, u32[]{:S(2)}) %collective-permute-start.11) | collective-permute-done | bytes 393248 | tf_op jit(solution)/shard_map/ppermute | solution.py:20
  143.6 3.2 %collective-permute-start.13 = (bf16[256,768]{1,0:T(8,128)(2,1)S(1)}, bf16[256,768]{1,0:T(8,128)(2,1)S(1)}, u32[]{:S(2)}, u32[]{:S(2)}) collective-permute-start(bf16[256,768]{1,0:T(8,128)(2,1)S(1)} %collective-permute-done.11.refs_5_), channel_id=1, source_target_pairs={{0,1},{1,2},{2,3},{3,0},{4,5},{5,6},{6,7},{7,4},{8,9},{9,10},{10,1... | collective-permute-start | bytes 1179656 | tf_op jit(solution)/shard_map/ppermute | solution.py:20
  146.8 2.0 collective-permute-start.16
  148.9 11.4 %collective-permute-done.14.refs_9_ = bf16[256,512]{1,0:T(8,128)(2,1)S(1)} collective-permute-done((bf16[256,512]{1,0:T(8,128)(2,1)S(1)}, bf16[256,512]{1,0:T(8,128)(2,1)S(1)}, u32[]{:S(2)}, u32[]{:S(2)}) %collective-permute-start.14) | collective-permute-done | bytes 262176 | tf_op jit(solution)/shard_map/ppermute | solution.py:20
  160.3 0.6 copy-done.22
  160.9 0.1 copy-done.19
  161.2 0.8 copy-done.20
  162.0 6.2 %shard_map.133 = bf16[512,1280]{1,0:T(8,128)(2,1)} custom-call(bf16[512,256]{1,0:T(8,128)(2,1)} %get-tuple-element.5.refs_0_, bf16[512,256]{1,0:T(8,128)(2,1)} %get-tuple-element.6.refs_1_, bf16[512,256]{1,0:T(8,128)(2,1)} %get-tuple-element.7.refs_2_, bf16[512,256]{1,0:T(8,128)(2,1)} %shard_map.132.refs_3_, bf16[256,768]{1,0:T(8,128)(2,1)} %copy-done.4, ...), custom_call_target="tpu_custom_call" | custom-call | tf_op jit(solution)/shard_map/pallas_call | solution.py:157
  168.2 0.9 copy-done.2
  169.1 10.3 %all-to-all-start.1 = ((bf16[64,8,1280]{2,1,0:T(8,128)(2,1)}), bf16[64,8,1280]{2,1,0:T(8,128)(2,1)S(1)}, u32[]{:S(2)}, u32[]{:S(2)}) async-start(bf16[64,8,1280]{2,1,0:T(8,128)(2,1)} %bitcast.20), calls=%async_computation.1 | async-start | bytes 2621440 | tf_op jit(solution)/shard_map/all_to_all | solution.py:258
  179.6 5.3 %collective-permute-start = (f32[2,2048]{1,0:T(2,128)S(1)}, f32[2,2048]{1,0:T(2,128)S(1)}, u32[]{:S(2)}, u32[]{:S(2)}) collective-permute-start(f32[2,2048]{1,0:T(2,128)S(1)} %slice.48), channel_id=1, source_target_pairs={{0,1},{1,2},{2,3},{3,4},{4,5},{5,6},{6,7},{7,8},{8,9},{9,10},{10,1... | collective-permute-start | bytes 49160 | tf_op jit(solution)/shard_map/ppermute | solution.py:243
  185.0 1.4 collective-permute-done
  186.3 0.4 fusion.5.own_ref
  186.8 27.4 %collective-permute-start.1 = (bf16[128,2048]{1,0:T(8,128)(2,1)S(1)}, bf16[128,2048]{1,0:T(8,128)(2,1)S(1)}, u32[]{:S(2)}, u32[]{:S(2)}) collective-permute-start(bf16[128,2048]{1,0:T(8,128)(2,1)S(1)} %fusion.5.own_ref), channel_id=1, source_target_pairs={{0,1},{1,2},{2,3},{3,0},{4,5},{5,6},{6,7},{7,4},{8,9},{9,10},{10,1... | collective-permute-start | bytes 1572872 | tf_op jit(solution)/shard_map/ppermute | solution.py:20
  214.2 6.7 %collective-permute-done.1.left_ref = bf16[128,2048]{1,0:T(8,128)(2,1)S(1)} collective-permute-done((bf16[128,2048]{1,0:T(8,128)(2,1)S(1)}, bf16[128,2048]{1,0:T(8,128)(2,1)S(1)}, u32[]{:S(2)}, u32[]{:S(2)}) %collective-permute-start.1) | collective-permute-done | bytes 524320 | tf_op jit(solution)/shard_map/ppermute | solution.py:20
  220.9 0.8 slice.54
  221.7 3.7 %collective-permute-start.3 = (bf16[64,2048]{1,0:T(8,128)(2,1)}, bf16[64,2048]{1,0:T(8,128)(2,1)S(1)}, u32[]{:S(2)}, u32[]{:S(2)}) collective-permute-start(bf16[64,2048]{1,0:T(8,128)(2,1)} %slice.54), channel_id=1, source_target_pairs={{0,1},{1,2},{2,3},{3,0},{4,5},{5,6},{6,7},{7,4},{8,9},{9,10},{10,1... | collective-permute-start | bytes 786440 | tf_op jit(solution)/shard_map/ppermute | solution.py:20
  225.4 0.8 slice.55
  226.1 1.7 mix.1.mix_ref
  227.8 1.7 collective-permute-done.3.first_ref
  229.6 4.4 %collective-permute-done.4.second_ref = bf16[64,2048]{1,0:T(8,128)(2,1)S(1)} collective-permute-done((bf16[64,2048]{1,0:T(8,128)(2,1)}, bf16[64,2048]{1,0:T(8,128)(2,1)S(1)}, u32[]{:S(2)}, u32[]{:S(2)}) %collective-permute-start.4) | collective-permute-done | bytes 262176 | tf_op jit(solution)/shard_map/ppermute | solution.py:20
  234.0 0.7 copy-done.25
  234.6 4.7 %mixer.1 = bf16[512,512]{1,0:T(8,128)(2,1)} custom-call(s32[1]{0:T(128)} %bitcast.place_ref, bf16[128,2048]{1,0:T(8,128)(2,1)} %copy-done.3, bf16[128,2048]{1,0:T(8,128)(2,1)} %copy-done.5, bf16[128,2048]{1,0:T(8,128)(2,1)} %copy-done.6, bf16[64,2048]{1,0:T(8,128)(2,1)} %copy-done.23, bf16[64,2048]{1,0:T(8,128)(2,1)} %copy-done.25, bf16[2048,512]{1,0:T(8,128)(2,1)} %weight_ref.1), custom_call_target="tpu_custom_call" | custom-call | tf_op jit(solution)/shard_map/mixer/pallas_call | solution.py:264
  239.4 3.1 %shard_map.135.refs_0_ = bf16[128,2048]{1,0:T(8,128)(2,1)} custom-call(bf16[256,512]{1,0:T(8,128)(2,1)} %mix.1.mix_ref, bf16[512,768]{1,0:T(8,128)(2,1)} %bitcast.21), custom_call_target="tpu_custom_call" | custom-call | tf_op jit(solution)/shard_map/pallas_call | solution.py:81
  242.5 1.1 copy-done.1
  243.6 4.3 %shard_map.136 = bf16[128,2048]{1,0:T(8,128)(2,1)} custom-call(bf16[256,512]{1,0:T(8,128)(2,1)} %mix.1.mix_ref, bf16[512,1280]{1,0:T(8,128)(2,1)} %bitcast.19, bf16[128,2048]{1,0:T(8,128)(2,1)} %shard_map.135.refs_0_), custom_call_target="tpu_custom_call", output_to_operand_aliasing={{}: (2, {})} | custom-call | tf_op jit(solution)/shard_map/pallas_call | solution.py:81
  (76 shorter events, 0.7 us)
Async XLA Ops:
  3.9 99.4 %all-to-all-start = ((bf16[64,8,2048]{2,1,0:T(8,128)(2,1)}), bf16[64,8,2048]{2,1,0:T(8,128)(2,1)S(1)}, u32[]{:S(2)}, u32[]{:S(2)}) async-start(bf16[64,8,2048]{2,1,0:T(8,128)(2,1)} %bitcast.18), calls=%async_computation | async-start | bytes 4194304 | tf_op jit(solution)/shard_map/all_to_all | solution.py:229
  14.7 27.5 %collective-permute-start.8 = (bf16[2048,256]{1,0:T(8,128)(2,1)}, bf16[2048,256]{1,0:T(8,128)(2,1)S(1)}, u32[]{:S(2)}, u32[]{:S(2)}) collective-permute-start(bf16[2048,256]{1,0:T(8,128)(2,1)} %bitcast.10.refs_2_), channel_id=1, source_target_pairs={{0,3},{1,0},{2,1},{3,2},{4,7},{5,4},{6,5},{7,6},{8,11},{9,8},{10,9... | collective-permute-start | bytes 3145736 | tf_op jit(solution)/shard_map/ppermute | solution.py:20
  15.5 26.7 %collective-permute-start.5 = (bf16[2048,256]{1,0:T(8,128)(2,1)}, bf16[2048,256]{1,0:T(8,128)(2,1)}, u32[]{:S(2)}, u32[]{:S(2)}) collective-permute-start(bf16[2048,256]{1,0:T(8,128)(2,1)} %bitcast.9.refs_1_), channel_id=1, source_target_pairs={{0,1},{1,2},{2,3},{3,0},{4,5},{5,6},{6,7},{7,4},{8,9},{9,10},{10,1... | collective-permute-start | bytes 3145736 | tf_op jit(solution)/shard_map/ppermute | solution.py:20
  18.0 79.7 %collective-permute-start.6 = (bf16[2048,256]{1,0:T(8,128)(2,1)}, bf16[2048,256]{1,0:T(8,128)(2,1)S(1)}, u32[]{:S(2)}, u32[]{:S(2)}) collective-permute-start(bf16[2048,256]{1,0:T(8,128)(2,1)} %bitcast.10.refs_2_), channel_id=1, source_target_pairs={{0,1},{1,2},{2,3},{3,0},{4,5},{5,6},{6,7},{7,4},{8,9},{9,10},{10,1... | collective-permute-start | bytes 3145736 | tf_op jit(solution)/shard_map/ppermute | solution.py:20
  18.0 83.0 %collective-permute-start.7 = (bf16[2048,256]{1,0:T(8,128)(2,1)}, bf16[2048,256]{1,0:T(8,128)(2,1)S(1)}, u32[]{:S(2)}, u32[]{:S(2)}) collective-permute-start(bf16[2048,256]{1,0:T(8,128)(2,1)} %bitcast.9.refs_1_), channel_id=1, source_target_pairs={{0,3},{1,0},{2,1},{3,2},{4,7},{5,4},{6,5},{7,6},{8,11},{9,8},{10,9... | collective-permute-start | bytes 3145736 | tf_op jit(solution)/shard_map/ppermute | solution.py:20
  42.2 59.3 %copy-start.10 = (bf16[2048,256]{1,0:T(8,128)(2,1)}, bf16[2048,256]{1,0:T(8,128)(2,1)S(1)}, u32[]{:S(2)}) copy-start(bf16[2048,256]{1,0:T(8,128)(2,1)S(1)} %collective-permute-done.8.refs_6_) | copy-start | bytes 3145732
  42.2 59.3 %collective-permute-start.10 = (bf16[2048,256]{1,0:T(8,128)(2,1)S(1)}, bf16[2048,256]{1,0:T(8,128)(2,1)S(1)}, u32[]{:S(2)}, u32[]{:S(2)}) collective-permute-start(bf16[2048,256]{1,0:T(8,128)(2,1)S(1)} %collective-permute-done.8.refs_6_), channel_id=1, source_target_pairs={{0,3},{1,0},{2,1},{3,2},{4,7},{5,4},{6,5},{7,6},{8,11},{9,8},{10,9... | collective-permute-start | bytes 3145736 | tf_op jit(solution)/shard_map/ppermute | solution.py:20
  42.2 70.6 %collective-permute-start.9 = (bf16[2048,256]{1,0:T(8,128)(2,1)}, bf16[2048,256]{1,0:T(8,128)(2,1)}, u32[]{:S(2)}, u32[]{:S(2)}) collective-permute-start(bf16[2048,256]{1,0:T(8,128)(2,1)} %collective-permute-done.5.refs_3_), channel_id=1, source_target_pairs={{0,1},{1,2},{2,3},{3,0},{4,5},{5,6},{6,7},{7,4},{8,9},{9,10},{10,1... | collective-permute-start | bytes 3145736 | tf_op jit(solution)/shard_map/ppermute | solution.py:20
  46.6 66.2 %copy-start.13 = (bf16[256,384]{1,0:T(8,128)(2,1)}, bf16[256,384]{1,0:T(8,128)(2,1)S(1)}, u32[]{:S(2)}) copy-start(bf16[256,384]{1,0:T(8,128)(2,1)S(1)} %get-tuple-element.8.refs_8_) | copy-start | bytes 589828
  46.6 66.2 %copy-start.14 = (bf16[256,384]{1,0:T(8,128)(2,1)}, bf16[256,384]{1,0:T(8,128)(2,1)S(1)}, u32[]{:S(2)}) copy-start(bf16[256,384]{1,0:T(8,128)(2,1)S(1)} %get-tuple-element.9.refs_4_) | copy-start | bytes 589828
  46.6 43.2 %collective-permute-start.17 = (bf16[256,384]{1,0:T(8,128)(2,1)S(1)}, bf16[256,384]{1,0:T(8,128)(2,1)}, u32[]{:S(2)}, u32[]{:S(2)}) collective-permute-start(bf16[256,384]{1,0:T(8,128)(2,1)S(1)} %get-tuple-element.9.refs_4_), channel_id=1, source_target_pairs={{0,1},{1,2},{2,3},{3,0},{4,5},{5,6},{6,7},{7,4},{8,9},{9,10},{10,1... | collective-permute-start | bytes 589832 | tf_op jit(solution)/shard_map/ppermute | solution.py:20
  89.9 7.9 %collective-permute-start.21 = (bf16[256,384]{1,0:T(8,128)(2,1)S(1)}, bf16[256,384]{1,0:T(8,128)(2,1)}, u32[]{:S(2)}, u32[]{:S(2)}) collective-permute-start(bf16[256,384]{1,0:T(8,128)(2,1)S(1)} %get-tuple-element.8.refs_8_), channel_id=1, source_target_pairs={{0,3},{1,0},{2,1},{3,2},{4,7},{5,4},{6,5},{7,6},{8,11},{9,8},{10,9... | collective-permute-start | bytes 589832 | tf_op jit(solution)/shard_map/ppermute | solution.py:20
  97.7 20.0 %collective-permute-start.18 = (bf16[256,384]{1,0:T(8,128)(2,1)S(1)}, bf16[256,384]{1,0:T(8,128)(2,1)}, u32[]{:S(2)}, u32[]{:S(2)}) collective-permute-start(bf16[256,384]{1,0:T(8,128)(2,1)S(1)} %get-tuple-element.9.refs_4_), channel_id=1, source_target_pairs={{0,3},{1,0},{2,1},{3,2},{4,7},{5,4},{6,5},{7,6},{8,11},{9,8},{10,9... | collective-permute-start | bytes 589832 | tf_op jit(solution)/shard_map/ppermute | solution.py:20
  97.7 3.8 %copy-start.11 = (bf16[2048,256]{1,0:T(8,128)(2,1)}, bf16[2048,256]{1,0:T(8,128)(2,1)S(1)}, u32[]{:S(2)}) copy-start(bf16[2048,256]{1,0:T(8,128)(2,1)S(1)} %collective-permute-done.6.refs_4_) | copy-start | bytes 3145732
  97.7 20.0 %collective-permute-start.20 = (bf16[256,384]{1,0:T(8,128)(2,1)S(1)}, bf16[256,384]{1,0:T(8,128)(2,1)}, u32[]{:S(2)}, u32[]{:S(2)}) collective-permute-start(bf16[256,384]{1,0:T(8,128)(2,1)S(1)} %get-tuple-element.8.refs_8_), channel_id=1, source_target_pairs={{0,1},{1,2},{2,3},{3,0},{4,5},{5,6},{6,7},{7,4},{8,9},{9,10},{10,1... | collective-permute-start | bytes 589832 | tf_op jit(solution)/shard_map/ppermute | solution.py:20
  101.0 1.0 copy-start.12
  101.0 16.8 %collective-permute-start.19 = (bf16[256,384]{1,0:T(8,128)(2,1)}, bf16[256,384]{1,0:T(8,128)(2,1)}, u32[]{:S(2)}, u32[]{:S(2)}) collective-permute-start(bf16[256,384]{1,0:T(8,128)(2,1)} %collective-permute-done.17.refs_5_), channel_id=1, source_target_pairs={{0,1},{1,2},{2,3},{3,0},{4,5},{5,6},{6,7},{7,4},{8,9},{9,10},{10,1... | collective-permute-start | bytes 589832 | tf_op jit(solution)/shard_map/ppermute | solution.py:20
  102.0 10.8 %copy-start.7 = (bf16[2048,256]{1,0:T(8,128)(2,1)}, bf16[2048,256]{1,0:T(8,128)(2,1)S(1)}, u32[]{:S(2)}) copy-start(bf16[2048,256]{1,0:T(8,128)(2,1)S(1)} %collective-permute-done.10.refs_2_) | copy-start | bytes 3145732
  102.0 15.8 %collective-permute-start.22 = (bf16[256,384]{1,0:T(8,128)(2,1)}, bf16[256,384]{1,0:T(8,128)(2,1)}, u32[]{:S(2)}, u32[]{:S(2)}) collective-permute-start(bf16[256,384]{1,0:T(8,128)(2,1)} %collective-permute-done.21.refs_10_), channel_id=1, source_target_pairs={{0,3},{1,0},{2,1},{3,2},{4,7},{5,4},{6,5},{7,6},{8,11},{9,8},{10,9... | collective-permute-start | bytes 589832 | tf_op jit(solution)/shard_map/ppermute | solution.py:20
  103.3 1.3 copy-start
  121.9 10.5 %copy-start.9 = (bf16[1,256,2048]{2,1,0:T(8,128)(2,1)S(1)}, bf16[1,256,2048]{2,1,0:T(8,128)(2,1)}, u32[]{:S(2)}) copy-start(bf16[1,256,2048]{2,1,0:T(8,128)(2,1)} %param.21) | copy-start | bytes 3145732
  121.9 46.3 %all-to-all-start.2 = ((bf16[64,8,768]{2,1,0:T(8,128)(2,1)}), bf16[64,8,768]{2,1,0:T(8,128)(2,1)S(1)}, u32[]{:S(2)}, u32[]{:S(2)}) async-start(bf16[64,8,768]{2,1,0:T(8,128)(2,1)} %bitcast.22), calls=%async_computation.2 | async-start | bytes 1572864 | tf_op jit(solution)/shard_map/all_to_all | solution.py:258
  132.4 27.9 %copy-start.4 = (bf16[256,768]{1,0:T(8,128)(2,1)}, bf16[256,768]{1,0:T(8,128)(2,1)S(1)}, u32[]{:S(2)}) copy-start(bf16[256,768]{1,0:T(8,128)(2,1)S(1)} %slice.56.refs_4_) | copy-start | bytes 1179652
  132.4 11.2 %collective-permute-start.11 = (bf16[256,768]{1,0:T(8,128)(2,1)S(1)}, bf16[256,768]{1,0:T(8,128)(2,1)S(1)}, u32[]{:S(2)}, u32[]{:S(2)}) collective-permute-start(bf16[256,768]{1,0:T(8,128)(2,1)S(1)} %slice.56.refs_4_), channel_id=1, source_target_pairs={{0,1},{1,2},{2,3},{3,0},{4,5},{5,6},{6,7},{7,4},{8,9},{9,10},{10,1... | collective-permute-start | bytes 1179656 | tf_op jit(solution)/shard_map/ppermute | solution.py:20
  134.5 25.8 %copy-start.8 = (bf16[256,512]{1,0:T(8,128)(2,1)}, bf16[256,512]{1,0:T(8,128)(2,1)S(1)}, u32[]{:S(2)}) copy-start(bf16[256,512]{1,0:T(8,128)(2,1)S(1)} %slice.57.refs_8_) | copy-start | bytes 786436
  134.5 12.4 %collective-permute-start.15 = (bf16[256,512]{1,0:T(8,128)(2,1)S(1)}, bf16[256,512]{1,0:T(8,128)(2,1)S(1)}, u32[]{:S(2)}, u32[]{:S(2)}) collective-permute-start(bf16[256,512]{1,0:T(8,128)(2,1)S(1)} %slice.57.refs_8_), channel_id=1, source_target_pairs={{0,3},{1,0},{2,1},{3,2},{4,7},{5,4},{6,5},{7,6},{8,11},{9,8},{10,9... | collective-permute-start | bytes 786440 | tf_op jit(solution)/shard_map/ppermute | solution.py:20
  134.6 25.6 %collective-permute-start.12 = (bf16[256,768]{1,0:T(8,128)(2,1)S(1)}, bf16[256,768]{1,0:T(8,128)(2,1)S(1)}, u32[]{:S(2)}, u32[]{:S(2)}) collective-permute-start(bf16[256,768]{1,0:T(8,128)(2,1)S(1)} %slice.56.refs_4_), channel_id=1, source_target_pairs={{0,3},{1,0},{2,1},{3,2},{4,7},{5,4},{6,5},{7,6},{8,11},{9,8},{10,9... | collective-permute-start | bytes 1179656 | tf_op jit(solution)/shard_map/ppermute | solution.py:20
  143.6 16.7 %copy-start.18 = (bf16[256,768]{1,0:T(8,128)(2,1)}, bf16[256,768]{1,0:T(8,128)(2,1)S(1)}, u32[]{:S(2)}) copy-start(bf16[256,768]{1,0:T(8,128)(2,1)S(1)} %collective-permute-done.11.refs_5_) | copy-start | bytes 1179652
  143.6 16.6 %collective-permute-start.13 = (bf16[256,768]{1,0:T(8,128)(2,1)S(1)}, bf16[256,768]{1,0:T(8,128)(2,1)S(1)}, u32[]{:S(2)}, u32[]{:S(2)}) collective-permute-start(bf16[256,768]{1,0:T(8,128)(2,1)S(1)} %collective-permute-done.11.refs_5_), channel_id=1, source_target_pairs={{0,1},{1,2},{2,3},{3,0},{4,5},{5,6},{6,7},{7,4},{8,9},{9,10},{10,1... | collective-permute-start | bytes 1179656 | tf_op jit(solution)/shard_map/ppermute | solution.py:20
  146.8 13.4 %collective-permute-start.14 = (bf16[256,512]{1,0:T(8,128)(2,1)S(1)}, bf16[256,512]{1,0:T(8,128)(2,1)S(1)}, u32[]{:S(2)}, u32[]{:S(2)}) collective-permute-start(bf16[256,512]{1,0:T(8,128)(2,1)S(1)} %slice.57.refs_8_), channel_id=1, source_target_pairs={{0,1},{1,2},{2,3},{3,0},{4,5},{5,6},{6,7},{7,4},{8,9},{9,10},{10,1... | collective-permute-start | bytes 786440 | tf_op jit(solution)/shard_map/ppermute | solution.py:20
  146.8 13.5 %copy-start.21 = (bf16[256,512]{1,0:T(8,128)(2,1)}, bf16[256,512]{1,0:T(8,128)(2,1)S(1)}, u32[]{:S(2)}) copy-start(bf16[256,512]{1,0:T(8,128)(2,1)S(1)} %collective-permute-done.15.refs_10_) | copy-start | bytes 786436
  146.8 13.4 %collective-permute-start.16 = (bf16[256,512]{1,0:T(8,128)(2,1)S(1)}, bf16[256,512]{1,0:T(8,128)(2,1)S(1)}, u32[]{:S(2)}, u32[]{:S(2)}) collective-permute-start(bf16[256,512]{1,0:T(8,128)(2,1)S(1)} %collective-permute-done.15.refs_10_), channel_id=1, source_target_pairs={{0,3},{1,0},{2,1},{3,2},{4,7},{5,4},{6,5},{7,6},{8,11},{9,8},{10,9... | collective-permute-start | bytes 786440 | tf_op jit(solution)/shard_map/ppermute | solution.py:20
  160.3 0.9 copy-start.24
  168.2 11.2 %copy-start.15 = (bf16[128,2048]{1,0:T(8,128)(2,1)S(1)}, bf16[128,2048]{1,0:T(8,128)(2,1)}, u32[]{:S(2)}) copy-start(bf16[128,2048]{1,0:T(8,128)(2,1)} %param.14) | copy-start | bytes 1572868
  168.2 11.2 %copy-start.16 = (bf16[128,2048]{1,0:T(8,128)(2,1)S(1)}, bf16[128,2048]{1,0:T(8,128)(2,1)}, u32[]{:S(2)}) copy-start(bf16[128,2048]{1,0:T(8,128)(2,1)} %param.13) | copy-start | bytes 1572868
  169.1 73.4 %all-to-all-start.1 = ((bf16[64,8,1280]{2,1,0:T(8,128)(2,1)}), bf16[64,8,1280]{2,1,0:T(8,128)(2,1)S(1)}, u32[]{:S(2)}, u32[]{:S(2)}) async-start(bf16[64,8,1280]{2,1,0:T(8,128)(2,1)} %bitcast.20), calls=%async_computation.1 | async-start | bytes 2621440 | tf_op jit(solution)/shard_map/all_to_all | solution.py:258
  179.4 5.5 %copy-start.26 = (bf16[3,2048]{1,0:T(4,128)(2,1)S(1)}, bf16[3,2048]{1,0:T(4,128)(2,1)}, u32[]{:S(2)}) copy-start(bf16[3,2048]{1,0:T(4,128)(2,1)} %param.15) | copy-start | bytes 36868
  179.4 6.9 %copy-start.17 = (bf16[128,2048]{1,0:T(8,128)(2,1)S(1)}, bf16[128,2048]{1,0:T(8,128)(2,1)}, u32[]{:S(2)}) copy-start(bf16[128,2048]{1,0:T(8,128)(2,1)} %param.12) | copy-start | bytes 1572868
  179.6 6.8 %collective-permute-start = (f32[2,2048]{1,0:T(2,128)S(1)}, f32[2,2048]{1,0:T(2,128)S(1)}, u32[]{:S(2)}, u32[]{:S(2)}) collective-permute-start(f32[2,2048]{1,0:T(2,128)S(1)} %slice.48), channel_id=1, source_target_pairs={{0,1},{1,2},{2,3},{3,4},{4,5},{5,6},{6,7},{7,8},{8,9},{9,10},{10,1... | collective-permute-start | bytes 49160 | tf_op jit(solution)/shard_map/ppermute | solution.py:243
  186.8 47.2 %copy-start.3 = (bf16[128,2048]{1,0:T(8,128)(2,1)}, bf16[128,2048]{1,0:T(8,128)(2,1)S(1)}, u32[]{:S(2)}) copy-start(bf16[128,2048]{1,0:T(8,128)(2,1)S(1)} %fusion.5.own_ref) | copy-start | bytes 1572868
  186.8 34.1 %collective-permute-start.1 = (bf16[128,2048]{1,0:T(8,128)(2,1)S(1)}, bf16[128,2048]{1,0:T(8,128)(2,1)S(1)}, u32[]{:S(2)}, u32[]{:S(2)}) collective-permute-start(bf16[128,2048]{1,0:T(8,128)(2,1)S(1)} %fusion.5.own_ref), channel_id=1, source_target_pairs={{0,1},{1,2},{2,3},{3,0},{4,5},{5,6},{6,7},{7,4},{8,9},{9,10},{10,1... | collective-permute-start | bytes 1572872 | tf_op jit(solution)/shard_map/ppermute | solution.py:20
  214.2 11.2 %collective-permute-start.2 = (bf16[128,2048]{1,0:T(8,128)(2,1)S(1)}, bf16[128,2048]{1,0:T(8,128)(2,1)S(1)}, u32[]{:S(2)}, u32[]{:S(2)}) collective-permute-start(bf16[128,2048]{1,0:T(8,128)(2,1)S(1)} %fusion.5.own_ref), channel_id=1, source_target_pairs={{0,3},{1,0},{2,1},{3,2},{4,7},{5,4},{6,5},{7,6},{8,11},{9,8},{10,9... | collective-permute-start | bytes 1572872 | tf_op jit(solution)/shard_map/ppermute | solution.py:20
  220.9 13.0 %copy-start.5 = (bf16[128,2048]{1,0:T(8,128)(2,1)}, bf16[128,2048]{1,0:T(8,128)(2,1)S(1)}, u32[]{:S(2)}) copy-start(bf16[128,2048]{1,0:T(8,128)(2,1)S(1)} %collective-permute-done.1.left_ref) | copy-start | bytes 1572868
  221.7 7.9 %collective-permute-start.3 = (bf16[64,2048]{1,0:T(8,128)(2,1)}, bf16[64,2048]{1,0:T(8,128)(2,1)S(1)}, u32[]{:S(2)}, u32[]{:S(2)}) collective-permute-start(bf16[64,2048]{1,0:T(8,128)(2,1)} %slice.54), channel_id=1, source_target_pairs={{0,1},{1,2},{2,3},{3,0},{4,5},{5,6},{6,7},{7,4},{8,9},{9,10},{10,1... | collective-permute-start | bytes 786440 | tf_op jit(solution)/shard_map/ppermute | solution.py:20
  225.4 8.6 %copy-start.6 = (bf16[128,2048]{1,0:T(8,128)(2,1)}, bf16[128,2048]{1,0:T(8,128)(2,1)S(1)}, u32[]{:S(2)}) copy-start(bf16[128,2048]{1,0:T(8,128)(2,1)S(1)} %collective-permute-done.2.right_ref) | copy-start | bytes 1572868
  226.1 7.8 %collective-permute-start.4 = (bf16[64,2048]{1,0:T(8,128)(2,1)}, bf16[64,2048]{1,0:T(8,128)(2,1)S(1)}, u32[]{:S(2)}, u32[]{:S(2)}) collective-permute-start(bf16[64,2048]{1,0:T(8,128)(2,1)} %slice.55), channel_id=1, source_target_pairs={{0,3},{1,0},{2,1},{3,2},{4,7},{5,4},{6,5},{7,6},{8,11},{9,8},{10,9... | collective-permute-start | bytes 786440 | tf_op jit(solution)/shard_map/ppermute | solution.py:20
  229.6 4.4 %copy-start.23 = (bf16[64,2048]{1,0:T(8,128)(2,1)}, bf16[64,2048]{1,0:T(8,128)(2,1)S(1)}, u32[]{:S(2)}) copy-start(bf16[64,2048]{1,0:T(8,128)(2,1)S(1)} %collective-permute-done.3.first_ref) | copy-start | bytes 786436
  242.5 1.1 copy-start.1
  (5 other events, 3.9 us)

commit v2 on v0

--- a/solution.py
+++ b/solution.py
@@ -8,8 +8,10 @@
 
 CONV = 3
 NORM_EPS = 1e-06
-PIECES = (256, 256, 1024, 512)
+PIECES = (384, 384, 768, 512)
 CHUNKS = ((0, 1), (2, 3))
+COLUMNS = 256
+MIB = 1 << 20
 
 
 def turn(value, steps):
@@ -55,32 +57,63 @@
     out_ref[...] = jnp.dot(table, normed, preferred_element_type=jnp.float32).astype(jnp.bfloat16)
 
 
-def mix_kernel(ids_ref, weight_ref, high_ref, low_ref, *, expert_count, slot_cap):
+def mix_kernel(ids_ref, weight_ref, out_ref, *, expert_count, slot_cap):
     weight = weight_ref[...]
+    tokens = weight.shape[1]
     share = weight / (weight[0:1] + weight[1:2])
     tables = slot_table(ids_ref[...], expert_count, slot_cap)
     mix = (tables[0] * share[0:1] + tables[1] * share[1:2]).T
     high = mix.astype(jnp.bfloat16)
-    high_ref[...] = high
-    low_ref[...] = (mix - high.astype(jnp.float32)).astype(jnp.bfloat16)
-
-
-def combine_kernel(high_ref, low_ref, *refs):
-    out_ref, at = refs[-1], 0
-    for ref in refs[:-1]:
-        rows = ref[...]
-        picked = dot32(high_ref[...], rows) + dot32(low_ref[...], rows)
-        out_ref[:, at : at + rows.shape[1]] = picked.astype(jnp.bfloat16)
-        at += rows.shape[1]
-
-
-def down_kernel(*refs):
-    out_ref, hidden, downs, at = refs[-1], refs[:4], refs[4:-1], 0
+    out_ref[:tokens] = high
+    out_ref[tokens:] = (mix - high.astype(jnp.float32)).astype(jnp.bfloat16)
+
+
+def combine_kernel(mix_ref, *refs):
+    chunks, out_ref, made, sent = refs[:-3], refs[-3], refs[-2], refs[-1]
+    tokens, at, copies = made.shape[0], 0, []
+    for chunk in chunks:
+        for first in range(0, chunk.shape[1], COLUMNS):
+            both = dot32(mix_ref[...], chunk[:, first : first + COLUMNS])
+            made[:, at : at + COLUMNS] = (both[:tokens] + both[tokens:]).astype(jnp.bfloat16)
+            place = pl.ds(at, COLUMNS)
+            copies.append(pltpu.make_async_copy(made.at[:, place], out_ref.at[:, place], sent.at[len(copies)]))
+            copies[-1].start()
+            at += COLUMNS
+    for copy in copies:
+        copy.wait()
+
+
+def hidden_kernel(rows_ref, *refs):
+    weights, out_ref = refs[:-1], refs[-1]
+    units = weights[0].shape[1]
+    for i in range(len(weights) // 2):
+        gate = dot32(rows_ref[...], weights[2 * i][...])
+        up = dot32(rows_ref[...], weights[2 * i + 1][...])
+        out_ref[:, i * units : (i + 1) * units] = (gate / (1.0 + jnp.exp(-gate)) * up).astype(jnp.bfloat16)
+
+
+def down_kernel(near_ref, far_ref, *refs):
+    downs, (out_ref, hidden, weight) = refs[:-3], refs[-3:]
+    middle, units, at = near_ref.shape[1], far_ref.shape[1], 0
+    hidden[:, :middle] = near_ref[...]
+    hidden[:, middle:] = far_ref[...]
     for i in range(0, len(downs), 4):
-        own = downs[i]
-        total = sum(dot32(h[...], d[...]) for h, d in zip(hidden, downs[i : i + 4]))
-        out_ref[:, at : at + own.shape[1]] = total.astype(jnp.bfloat16)
-        at += own.shape[1]
+        width = downs[i].shape[1]
+        for k in range(4):
+            weight[k * units : (k + 1) * units, at : at + width] = downs[i + k][...]
+        at += width
+    out_ref[...] = dot32(hidden[...], weight[...]).astype(jnp.bfloat16)
+
+
+def on_core(kernel, shape, operands, mib, scratch=(), out=pltpu.VMEM):
+    return pl.pallas_call(
+        kernel,
+        out_shape=jax.ShapeDtypeStruct(shape, jnp.bfloat16),
+        in_specs=[pl.BlockSpec(memory_space=pltpu.VMEM)] * len(operands),
+        out_specs=pl.BlockSpec(memory_space=out),
+        scratch_shapes=list(scratch),
+        compiler_params=pltpu.CompilerParams(vmem_limit_bytes=mib * MIB),
+    )(*operands)
 
 
 def mixer_kernel(place_ref, own_ref, left_ref, right_ref, first_ref, second_ref, weight_ref, out_ref):
@@ -139,23 +172,21 @@
         far = turn(sides[i % 2], 1 - 2 * (i % 2))
         downs.append((part, *sides, far))
 
-    outgoing = pl.pallas_call(
+    outgoing = on_core(
         lambda *refs: dispatch_kernel(*refs, expert_count=expert_count, slot_cap=slot_cap),
-        out_shape=jax.ShapeDtypeStruct((slots, model_width), jnp.bfloat16),
-        in_specs=[vmem] * 3,
-        out_specs=vmem,
-        name="dispatch",
-    )(ids_t, expert_input, norm_gain[None])
+        (slots, model_width),
+        (ids_t, expert_input, norm_gain[None]),
+        12,
+    )
     arrived = lax.all_to_all(
         outgoing.reshape(expert_count, slot_cap, model_width), "ep", 0, 0, tiled=True
     ).reshape(slots, model_width)
-    mix = pl.pallas_call(
+    mix = on_core(
         lambda *refs: mix_kernel(*refs, expert_count=expert_count, slot_cap=slot_cap),
-        out_shape=[jax.ShapeDtypeStruct((token_count, slots), jnp.bfloat16)] * 2,
-        in_specs=[vmem] * 2,
-        out_specs=[vmem] * 2,
-        name="mix",
-    )(ids_t, weight_t)
+        (2 * token_count, slots),
+        (ids_t, weight_t),
+        8,
+    )
 
     tap_span = CONV - 1
     product = in_gate.astype(jnp.float32) * conv_input.astype(jnp.float32)
@@ -168,21 +199,17 @@
     smoothed = sum(padded[j : j + row_count] * taps[j] for j in range(CONV))
     gated = (out_gate.astype(jnp.float32) * smoothed).astype(jnp.bfloat16)
 
-    hidden = [
-        (jax.nn.silu(dot32(arrived, g)) * dot32(arrived, u)).astype(jnp.bfloat16)
-        for g, u in zip((gate, *gates, gate_far), (up, *ups, up_far))
-    ]
+    units = gate.shape[1]
+    near_weights = (gate, up, gates[0], ups[0], gates[1], ups[1])
+    near = on_core(hidden_kernel, (slots, 3 * units), (arrived, *near_weights), 12)
+    far = on_core(hidden_kernel, (slots, units), (arrived, gate_far, up_far), 8)
 
     returned = []
     for chunk in CHUNKS:
-        operands = [d for piece in chunk for d in downs[piece]]
         width = sum(PIECES[piece] for piece in chunk)
-        result = pl.pallas_call(
-            down_kernel,
-            out_shape=jax.ShapeDtypeStruct((slots, width), jnp.bfloat16),
-            in_specs=[vmem] * (4 + len(operands)),
-            out_specs=vmem,
-        )(*hidden, *operands)
+        operands = (near, far, *[d for piece in chunk for d in downs[piece]])
+        scratch = (pltpu.VMEM((slots, 4 * units), jnp.bfloat16), pltpu.VMEM((4 * units, width), jnp.bfloat16))
+        result = on_core(down_kernel, (slots, width), operands, 14, scratch)
         back = lax.all_to_all(result.reshape(expert_count, slot_cap, width), "ep", 0, 0, tiled=True)
         returned.append(back.reshape(slots, width))
 
@@ -193,16 +220,15 @@
         out_shape=jax.ShapeDtypeStruct((4 * row_count, mixer_weight.shape[1]), jnp.bfloat16),
         in_specs=[pl.BlockSpec(memory_space=pltpu.SMEM)] + [vmem] * 6,
         out_specs=vmem,
+        compiler_params=pltpu.CompilerParams(vmem_limit_bytes=8 * MIB),
         name="mixer",
     )(lax.axis_index("tp").reshape(1), gated, *gated_sides, *gated_far, mixer_weight)
 
-    experts_out = pl.pallas_call(
-        combine_kernel,
-        out_shape=jax.ShapeDtypeStruct((token_count, model_width), jnp.bfloat16),
-        in_specs=[vmem] * (2 + len(returned)),
-        out_specs=vmem,
-        name="combine",
-    )(*mix, *returned)
+    scratch = (
+        pltpu.VMEM((token_count, model_width), jnp.bfloat16),
+        pltpu.SemaphoreType.DMA((model_width // COLUMNS,)),
+    )
+    experts_out = on_core(combine_kernel, (token_count, model_width), (mix, *returned), 8, scratch, pl.ANY)
     return (mixer_out, experts_out)
 
 

time: 242 us -> 240 us (level)
  matrix products: 15.8 us -> 0 us
  local copies, waits for them, and re-layouts: 8.77 us -> 22.9 us
  Pallas kernels: 21 us -> 18.2 us
    ppermute x22, waiting for transfers between devices: 83.1 us -> 105 us  [turn(): return lax.ppermute(value, 'tp', pairs)]
    all_to_all x1, waiting for transfers between devices: 19 us -> 0.01 us  [local(): lax.all_to_all(outgoing.reshape(expert_count, slot_cap, model_width), 'ep...]
    dot_general x8 -> x0, matrix products: 15.8 us -> none  [dot32(): return jnp.dot(a, b, preferred_element_type=jnp.float32)]
    unnamed x52 -> x50, local copies, waits for them, and re-layouts: 4.16 us -> 18.4 us
    ppermute x1, starting transfers between devices: 2.17 us -> 5.33 us  [local(): lax.ppermute(product[row_count - tap_span:], ('ep', 'tp'), [(i, i + 1) fo...]
    ppermute x22, starting transfers between devices: 55.6 us -> 53 us  [turn(): return lax.ppermute(value, 'tp', pairs)]
    pallas_call x5 -> x7, Pallas kernels: 16.3 us -> 14.7 us  [on_core(): pl.pallas_call(kernel, out_shape=jax.ShapeDtypeStruct(shape, jnp.bfloat16...]
  transfers between devices with their start and end apart: 26 -> 26, of which waited for: 12 -> 9; matrix products, arithmetic and copies ran while one was open for 9% -> 2% of each run, Pallas kernels for 6% -> 5%
where the time goes in v2:
time: 240 us; the launch traced here: 239 us
  waiting for transfers between devices  107 us (45%)
  starting transfers between devices  89.9 us (37%)
  local copies, waits for them, and re-layouts  22.9 us (10%)
  Pallas kernels  18.2 us (8%)
    ppermute x22, waiting for transfers between devices, turn(): return lax.ppermute(value, 'tp', pairs)  105 us
    ppermute x22, starting transfers between devices, turn(): return lax.ppermute(value, 'tp', pairs)  53 us
    all_to_all x2, starting transfers between devices, local(): lax.all_to_all(result.reshape(expert_count, slot_cap, width), 'ep', 0, 0,...  20.7 us
    unnamed x50, local copies, waits for them, and re-layouts  18.4 us
    pallas_call x7, Pallas kernels, on_core(): pl.pallas_call(kernel, out_shape=jax.ShapeDtypeStruct(shape, jnp.bfloat16...  14.7 us
    all_to_all x1, starting transfers between devices, local(): lax.all_to_all(outgoing.reshape(expert_count, slot_cap, model_width), 'ep...  10.9 us
    ppermute x1, starting transfers between devices, local(): lax.ppermute(product[row_count - tap_span:], ('ep', 'tp'), [(i, i + 1) fo...  5.33 us
  transfers between devices with their start and end apart: 26, of which 9 were waited for; matrix products, arithmetic and copies ran while one was open for 2% of the time, Pallas kernels for 5%

profile of v2, /device:TPU:120, one launch (start us, length us, event | category | flops | bytes accessed | tf_op | source)
XLA Modules:
  0.0 239.3 jit_solution(14731389324648414699)
XLA Ops:
  0.6 1.0 copy-done.16
  3.0 0.9 shard_map.132
  4.0 1.3 copy-done
  5.3 10.9 %all-to-all-start = ((bf16[64,8,2048]{2,1,0:T(8,128)(2,1)}), bf16[64,8,2048]{2,1,0:T(8,128)(2,1)S(1)}, u32[]{:S(2)}, u32[]{:S(2)}) async-start(bf16[64,8,2048]{2,1,0:T(8,128)(2,1)} %bitcast.18), calls=%async_computation | async-start | bytes 4194304 | tf_op jit(solution)/shard_map/all_to_all | solution.py:181
  16.2 0.8 collective-permute-start.8
  17.0 2.5 %collective-permute-start.5 = (bf16[2048,256]{1,0:T(8,128)(2,1)S(1)}, bf16[2048,256]{1,0:T(8,128)(2,1)}, u32[]{:S(2)}, u32[]{:S(2)}) collective-permute-start(bf16[2048,256]{1,0:T(8,128)(2,1)S(1)} %bitcast.22), channel_id=1, source_target_pairs={{0,1},{1,2},{2,3},{3,0},{4,5},{5,6},{6,7},{7,4},{8,9},{9,10},{10,1... | collective-permute-start | bytes 3145736 | tf_op jit(solution)/shard_map/ppermute | solution.py:20
  19.5 2.0 collective-permute-start.7
  21.5 22.2 %collective-permute-done.8.refs_5_ = bf16[2048,256]{1,0:T(8,128)(2,1)S(1)} collective-permute-done((bf16[2048,256]{1,0:T(8,128)(2,1)}, bf16[2048,256]{1,0:T(8,128)(2,1)S(1)}, u32[]{:S(2)}, u32[]{:S(2)}) %collective-permute-start.8) | collective-permute-done | bytes 1048608 | tf_op jit(solution)/shard_map/ppermute | solution.py:20
  43.7 1.0 copy-done.8
  44.7 3.2 %collective-permute-start.9 = (bf16[2048,256]{1,0:T(8,128)(2,1)}, bf16[2048,256]{1,0:T(8,128)(2,1)}, u32[]{:S(2)}, u32[]{:S(2)}) collective-permute-start(bf16[2048,256]{1,0:T(8,128)(2,1)} %collective-permute-done.5.refs_2_), channel_id=1, source_target_pairs={{0,1},{1,2},{2,3},{3,0},{4,5},{5,6},{6,7},{7,4},{8,9},{9,10},{10,1... | collective-permute-start | bytes 3145736 | tf_op jit(solution)/shard_map/ppermute | solution.py:20
  47.9 1.1 fusion.7
  49.1 42.1 %collective-permute-done.11.refs_1_ = bf16[256,384]{1,0:T(8,128)(2,1)} collective-permute-done((bf16[256,384]{1,0:T(8,128)(2,1)S(1)}, bf16[256,384]{1,0:T(8,128)(2,1)}, u32[]{:S(2)}, u32[]{:S(2)}) %collective-permute-start.11) | collective-permute-done | bytes 196640 | tf_op jit(solution)/shard_map/ppermute | solution.py:20
  91.6 7.4 %collective-permute-done.15.refs_6_ = bf16[256,384]{1,0:T(8,128)(2,1)} collective-permute-done((bf16[256,384]{1,0:T(8,128)(2,1)S(1)}, bf16[256,384]{1,0:T(8,128)(2,1)}, u32[]{:S(2)}, u32[]{:S(2)}) %collective-permute-start.15) | collective-permute-done | bytes 196640 | tf_op jit(solution)/shard_map/ppermute | solution.py:20
  99.0 1.0 copy-done.10
  100.0 3.2 %collective-permute-start.14 = (bf16[256,384]{1,0:T(8,128)(2,1)S(1)}, bf16[256,384]{1,0:T(8,128)(2,1)}, u32[]{:S(2)}, u32[]{:S(2)}) collective-permute-start(bf16[256,384]{1,0:T(8,128)(2,1)S(1)} %get-tuple-element.2.refs_4_), channel_id=1, source_target_pairs={{0,1},{1,2},{2,3},{3,0},{4,5},{5,6},{6,7},{7,4},{8,9},{9,10},{10,1... | collective-permute-start | bytes 589832 | tf_op jit(solution)/shard_map/ppermute | solution.py:20
  103.2 1.0 copy-done.12
  104.8 1.0 copy-done.14
  105.8 1.5 collective-permute-start.16
  107.3 1.2 copy-done.6
  108.5 1.2 copy-done.7
  109.7 1.2 copy-done.9
  111.0 1.2 copy-done.11
  112.2 1.2 copy-done.13
  113.4 4.7 %shard_map.133.near_ref = bf16[512,768]{1,0:T(8,128)(2,1)S(1)} custom-call(bf16[512,2048]{1,0:T(8,128)(2,1)S(1)} %bitcast.16, bf16[2048,256]{1,0:T(8,128)(2,1)S(1)} %bitcast.24, bf16[2048,256]{1,0:T(8,128)(2,1)S(1)} %bitcast.27, bf16[2048,256]{1,0:T(8,128)(2,1)} %collective-permute-done.5.refs_2_, bf16[2048,256]{1,0:T(8,128)(2,1)S(1)} %copy-done.11, ...), custom_call_target="tpu_custom_call" | custom-call | tf_op jit(solution)/shard_map/pallas_call | solution.py:109
  118.2 2.5 %shard_map.134.far_ref = bf16[512,256]{1,0:T(8,128)(2,1)S(1)} custom-call(bf16[512,2048]{1,0:T(8,128)(2,1)S(1)} %bitcast.17, bf16[2048,256]{1,0:T(8,128)(2,1)} %collective-permute-done.9.refs_0_, bf16[2048,256]{1,0:T(8,128)(2,1)S(1)} %copy-done.15), custom_call_target="tpu_custom_call" | custom-call | tf_op jit(solution)/shard_map/pallas_call | solution.py:109
  120.7 3.3 %shard_map.135 = bf16[512,768]{1,0:T(8,128)(2,1)} custom-call(bf16[512,768]{1,0:T(8,128)(2,1)S(1)} %shard_map.133.near_ref, bf16[512,256]{1,0:T(8,128)(2,1)S(1)} %shard_map.134.far_ref, bf16[256,384]{1,0:T(8,128)(2,1)S(1)} %get-tuple-element.3.refs_0_, bf16[256,384]{1,0:T(8,128)(2,1)} %collective-permute-done.11.refs_1_, ...), custom_call_target="tpu_custom_call" | custom-call | tf_op jit(solution)/shard_map/pallas_call | solution.py:109
  124.0 10.3 %all-to-all-start.1 = ((bf16[64,8,768]{2,1,0:T(8,128)(2,1)}), bf16[64,8,768]{2,1,0:T(8,128)(2,1)S(1)}, u32[]{:S(2)}, u32[]{:S(2)}) async-start(bf16[64,8,768]{2,1,0:T(8,128)(2,1)} %bitcast.12), calls=%async_computation.1 | async-start | bytes 1572864 | tf_op jit(solution)/shard_map/all_to_all | solution.py:213
  134.3 1.0 slice.58.refs_0_
  135.3 1.8 collective-permute-start.17
  137.1 1.0 slice.59.refs_4_
  138.5 8.0 %collective-permute-done.17.refs_1_ = bf16[256,768]{1,0:T(8,128)(2,1)S(1)} collective-permute-done((bf16[256,768]{1,0:T(8,128)(2,1)S(1)}, bf16[256,768]{1,0:T(8,128)(2,1)S(1)}, u32[]{:S(2)}, u32[]{:S(2)}) %collective-permute-start.17) | collective-permute-done | bytes 393248 | tf_op jit(solution)/shard_map/ppermute | solution.py:20
  146.5 3.0 %collective-permute-start.19 = (bf16[256,768]{1,0:T(8,128)(2,1)S(1)}, bf16[256,768]{1,0:T(8,128)(2,1)S(1)}, u32[]{:S(2)}, u32[]{:S(2)}) collective-permute-start(bf16[256,768]{1,0:T(8,128)(2,1)S(1)} %collective-permute-done.17.refs_1_), channel_id=1, source_target_pairs={{0,1},{1,2},{2,3},{3,0},{4,5},{5,6},{6,7},{7,4},{8,9},{9,10},{10,1... | collective-permute-start | bytes 1179656 | tf_op jit(solution)/shard_map/ppermute | solution.py:20
  149.5 2.0 collective-permute-start.22
  151.5 11.4 %collective-permute-done.20.refs_5_ = bf16[256,512]{1,0:T(8,128)(2,1)S(1)} collective-permute-done((bf16[256,512]{1,0:T(8,128)(2,1)S(1)}, bf16[256,512]{1,0:T(8,128)(2,1)S(1)}, u32[]{:S(2)}, u32[]{:S(2)}) %collective-permute-start.20) | collective-permute-done | bytes 262176 | tf_op jit(solution)/shard_map/ppermute | solution.py:20
  162.9 1.5 shard_map.136
  164.5 1.1 copy-done.1
  165.6 10.4 %all-to-all-start.2 = ((bf16[64,8,1280]{2,1,0:T(8,128)(2,1)}), bf16[64,8,1280]{2,1,0:T(8,128)(2,1)S(1)}, u32[]{:S(2)}, u32[]{:S(2)}) async-start(bf16[64,8,1280]{2,1,0:T(8,128)(2,1)} %bitcast.20), calls=%async_computation.2 | async-start | bytes 2621440 | tf_op jit(solution)/shard_map/all_to_all | solution.py:213
  176.2 5.3 %collective-permute-start = (f32[2,2048]{1,0:T(2,128)S(1)}, f32[2,2048]{1,0:T(2,128)S(1)}, u32[]{:S(2)}, u32[]{:S(2)}) collective-permute-start(f32[2,2048]{1,0:T(2,128)S(1)} %slice.48), channel_id=1, source_target_pairs={{0,1},{1,2},{2,3},{3,4},{4,5},{5,6},{6,7},{7,8},{8,9},{9,10},{10,1... | collective-permute-start | bytes 49160 | tf_op jit(solution)/shard_map/ppermute | solution.py:194
  181.6 1.4 collective-permute-done
  183.4 27.6 %collective-permute-start.1 = (bf16[128,2048]{1,0:T(8,128)(2,1)S(1)}, bf16[128,2048]{1,0:T(8,128)(2,1)S(1)}, u32[]{:S(2)}, u32[]{:S(2)}) collective-permute-start(bf16[128,2048]{1,0:T(8,128)(2,1)S(1)} %fusion.5.own_ref), channel_id=1, source_target_pairs={{0,1},{1,2},{2,3},{3,0},{4,5},{5,6},{6,7},{7,4},{8,9},{9,10},{10,1... | collective-permute-start | bytes 1572872 | tf_op jit(solution)/shard_map/ppermute | solution.py:20
  211.0 6.7 %collective-permute-done.1.left_ref = bf16[128,2048]{1,0:T(8,128)(2,1)S(1)} collective-permute-done((bf16[128,2048]{1,0:T(8,128)(2,1)S(1)}, bf16[128,2048]{1,0:T(8,128)(2,1)S(1)}, u32[]{:S(2)}, u32[]{:S(2)}) %collective-permute-start.1) | collective-permute-done | bytes 524320 | tf_op jit(solution)/shard_map/ppermute | solution.py:20
  218.4 3.7 %collective-permute-start.3 = (bf16[64,2048]{1,0:T(8,128)(2,1)}, bf16[64,2048]{1,0:T(8,128)(2,1)}, u32[]{:S(2)}, u32[]{:S(2)}) collective-permute-start(bf16[64,2048]{1,0:T(8,128)(2,1)} %slice.54), channel_id=1, source_target_pairs={{0,1},{1,2},{2,3},{3,0},{4,5},{5,6},{6,7},{7,4},{8,9},{9,10},{10,1... | collective-permute-start | bytes 786440 | tf_op jit(solution)/shard_map/ppermute | solution.py:20
  224.0 2.4 collective-permute-done.3.first_ref
  226.3 5.2 %collective-permute-done.4.second_ref = bf16[64,2048]{1,0:T(8,128)(2,1)} collective-permute-done((bf16[64,2048]{1,0:T(8,128)(2,1)}, bf16[64,2048]{1,0:T(8,128)(2,1)}, u32[]{:S(2)}, u32[]{:S(2)}) %collective-permute-start.4) | collective-permute-done | bytes 262176 | tf_op jit(solution)/shard_map/ppermute | solution.py:20
  231.6 1.6 copy-done.2
  233.1 1.0 copy-done.4
  234.2 3.5 %mixer.1 = bf16[512,512]{1,0:T(8,128)(2,1)} custom-call(s32[1]{0:T(128)} %bitcast.place_ref, bf16[128,2048]{1,0:T(8,128)(2,1)S(1)} %fusion.5.own_ref, bf16[128,2048]{1,0:T(8,128)(2,1)S(1)} %collective-permute-done.1.left_ref, bf16[128,2048]{1,0:T(8,128)(2,1)S(1)} %copy-done.4, bf16[64,2048]{1,0:T(8,128)(2,1)} %collective-permute-done.3.first_ref, ...), custom_call_target="tpu_custom_call" | custom-call | tf_op jit(solution)/shard_map/mixer/pallas_call | solution.py:218
  237.7 1.4 shard_map.137
  (71 shorter events, 6.2 us)
Async XLA Ops:
  0.6 1.0 copy-start.16
  4.0 1.3 copy-start
  5.3 11.7 %copy-start.5 = (bf16[1,2048,256]{2,1,0:T(8,128)(2,1)S(1)}, bf16[1,2048,256]{2,1,0:T(8,128)(2,1)}, u32[]{:S(2)}) copy-start(bf16[1,2048,256]{2,1,0:T(8,128)(2,1)} %param.19) | copy-start | bytes 3145732
  5.3 102.0 %all-to-all-start = ((bf16[64,8,2048]{2,1,0:T(8,128)(2,1)}), bf16[64,8,2048]{2,1,0:T(8,128)(2,1)S(1)}, u32[]{:S(2)}, u32[]{:S(2)}) async-start(bf16[64,8,2048]{2,1,0:T(8,128)(2,1)} %bitcast.18), calls=%async_computation | async-start | bytes 4194304 | tf_op jit(solution)/shard_map/all_to_all | solution.py:181
  16.2 27.5 %collective-permute-start.8 = (bf16[2048,256]{1,0:T(8,128)(2,1)}, bf16[2048,256]{1,0:T(8,128)(2,1)S(1)}, u32[]{:S(2)}, u32[]{:S(2)}) collective-permute-start(bf16[2048,256]{1,0:T(8,128)(2,1)} %bitcast.25), channel_id=1, source_target_pairs={{0,3},{1,0},{2,1},{3,2},{4,7},{5,4},{6,5},{7,6},{8,11},{9,8},{10,9... | collective-permute-start | bytes 3145736 | tf_op jit(solution)/shard_map/ppermute | solution.py:20
  17.0 27.7 %collective-permute-start.5 = (bf16[2048,256]{1,0:T(8,128)(2,1)S(1)}, bf16[2048,256]{1,0:T(8,128)(2,1)}, u32[]{:S(2)}, u32[]{:S(2)}) collective-permute-start(bf16[2048,256]{1,0:T(8,128)(2,1)S(1)} %bitcast.22), channel_id=1, source_target_pairs={{0,1},{1,2},{2,3},{3,0},{4,5},{5,6},{6,7},{7,4},{8,9},{9,10},{10,1... | collective-permute-start | bytes 3145736 | tf_op jit(solution)/shard_map/ppermute | solution.py:20
  19.5 79.5 %collective-permute-start.6 = (bf16[2048,256]{1,0:T(8,128)(2,1)}, bf16[2048,256]{1,0:T(8,128)(2,1)S(1)}, u32[]{:S(2)}, u32[]{:S(2)}) collective-permute-start(bf16[2048,256]{1,0:T(8,128)(2,1)} %bitcast.26), channel_id=1, source_target_pairs={{0,1},{1,2},{2,3},{3,0},{4,5},{5,6},{6,7},{7,4},{8,9},{9,10},{10,1... | collective-permute-start | bytes 3145736 | tf_op jit(solution)/shard_map/ppermute | solution.py:20
  19.5 83.7 %collective-permute-start.7 = (bf16[2048,256]{1,0:T(8,128)(2,1)S(1)}, bf16[2048,256]{1,0:T(8,128)(2,1)S(1)}, u32[]{:S(2)}, u32[]{:S(2)}) collective-permute-start(bf16[2048,256]{1,0:T(8,128)(2,1)S(1)} %bitcast.23), channel_id=1, source_target_pairs={{0,3},{1,0},{2,1},{3,2},{4,7},{5,4},{6,5},{7,6},{8,11},{9,8},{10,9... | collective-permute-start | bytes 3145736 | tf_op jit(solution)/shard_map/ppermute | solution.py:20
  43.7 61.0 %collective-permute-start.10 = (bf16[2048,256]{1,0:T(8,128)(2,1)S(1)}, bf16[2048,256]{1,0:T(8,128)(2,1)S(1)}, u32[]{:S(2)}, u32[]{:S(2)}) collective-permute-start(bf16[2048,256]{1,0:T(8,128)(2,1)S(1)} %collective-permute-done.8.refs_5_), channel_id=1, source_target_pairs={{0,3},{1,0},{2,1},{3,2},{4,7},{5,4},{6,5},{7,6},{8,11},{9,8},{10,9... | collective-permute-start | bytes 3145736 | tf_op jit(solution)/shard_map/ppermute | solution.py:20
  43.7 1.0 copy-start.8
  44.7 73.5 %collective-permute-start.9 = (bf16[2048,256]{1,0:T(8,128)(2,1)}, bf16[2048,256]{1,0:T(8,128)(2,1)}, u32[]{:S(2)}, u32[]{:S(2)}) collective-permute-start(bf16[2048,256]{1,0:T(8,128)(2,1)} %collective-permute-done.5.refs_2_), channel_id=1, source_target_pairs={{0,1},{1,2},{2,3},{3,0},{4,5},{5,6},{6,7},{7,4},{8,9},{9,10},{10,1... | collective-permute-start | bytes 3145736 | tf_op jit(solution)/shard_map/ppermute | solution.py:20
  49.0 42.2 %collective-permute-start.11 = (bf16[256,384]{1,0:T(8,128)(2,1)S(1)}, bf16[256,384]{1,0:T(8,128)(2,1)}, u32[]{:S(2)}, u32[]{:S(2)}) collective-permute-start(bf16[256,384]{1,0:T(8,128)(2,1)S(1)} %get-tuple-element.3.refs_0_), channel_id=1, source_target_pairs={{0,1},{1,2},{2,3},{3,0},{4,5},{5,6},{6,7},{7,4},{8,9},{9,10},{10,1... | collective-permute-start | bytes 589832 | tf_op jit(solution)/shard_map/ppermute | solution.py:20
  91.2 7.9 %collective-permute-start.15 = (bf16[256,384]{1,0:T(8,128)(2,1)S(1)}, bf16[256,384]{1,0:T(8,128)(2,1)}, u32[]{:S(2)}, u32[]{:S(2)}) collective-permute-start(bf16[256,384]{1,0:T(8,128)(2,1)S(1)} %get-tuple-element.2.refs_4_), channel_id=1, source_target_pairs={{0,3},{1,0},{2,1},{3,2},{4,7},{5,4},{6,5},{7,6},{8,11},{9,8},{10,9... | collective-permute-start | bytes 589832 | tf_op jit(solution)/shard_map/ppermute | solution.py:20
  99.0 21.7 %collective-permute-start.12 = (bf16[256,384]{1,0:T(8,128)(2,1)S(1)}, bf16[256,384]{1,0:T(8,128)(2,1)}, u32[]{:S(2)}, u32[]{:S(2)}) collective-permute-start(bf16[256,384]{1,0:T(8,128)(2,1)S(1)} %get-tuple-element.3.refs_0_), channel_id=1, source_target_pairs={{0,3},{1,0},{2,1},{3,2},{4,7},{5,4},{6,5},{7,6},{8,11},{9,8},{10,9... | collective-permute-start | bytes 589832 | tf_op jit(solution)/shard_map/ppermute | solution.py:20
  99.0 1.0 copy-start.10
  100.0 20.7 %collective-permute-start.14 = (bf16[256,384]{1,0:T(8,128)(2,1)S(1)}, bf16[256,384]{1,0:T(8,128)(2,1)}, u32[]{:S(2)}, u32[]{:S(2)}) collective-permute-start(bf16[256,384]{1,0:T(8,128)(2,1)S(1)} %get-tuple-element.2.refs_4_), channel_id=1, source_target_pairs={{0,1},{1,2},{2,3},{3,0},{4,5},{5,6},{6,7},{7,4},{8,9},{9,10},{10,1... | collective-permute-start | bytes 589832 | tf_op jit(solution)/shard_map/ppermute | solution.py:20
  103.2 1.0 copy-start.12
  104.2 16.5 %collective-permute-start.13 = (bf16[256,384]{1,0:T(8,128)(2,1)}, bf16[256,384]{1,0:T(8,128)(2,1)}, u32[]{:S(2)}, u32[]{:S(2)}) collective-permute-start(bf16[256,384]{1,0:T(8,128)(2,1)} %collective-permute-done.11.refs_1_), channel_id=1, source_target_pairs={{0,1},{1,2},{2,3},{3,0},{4,5},{5,6},{6,7},{7,4},{8,9},{9,10},{10,1... | collective-permute-start | bytes 589832 | tf_op jit(solution)/shard_map/ppermute | solution.py:20
  104.7 1.0 copy-start.14
  105.8 14.9 %collective-permute-start.16 = (bf16[256,384]{1,0:T(8,128)(2,1)}, bf16[256,384]{1,0:T(8,128)(2,1)}, u32[]{:S(2)}, u32[]{:S(2)}) collective-permute-start(bf16[256,384]{1,0:T(8,128)(2,1)} %collective-permute-done.15.refs_6_), channel_id=1, source_target_pairs={{0,3},{1,0},{2,1},{3,2},{4,7},{5,4},{6,5},{7,6},{8,11},{9,8},{10,9... | collective-permute-start | bytes 589832 | tf_op jit(solution)/shard_map/ppermute | solution.py:20
  107.3 1.2 copy-start.6
  108.5 1.2 copy-start.7
  109.7 1.2 copy-start.9
  111.0 1.2 copy-start.11
  112.2 1.2 copy-start.13
  113.4 4.8 %copy-start.15 = (bf16[2048,256]{1,0:T(8,128)(2,1)S(1)}, bf16[2048,256]{1,0:T(8,128)(2,1)}, u32[]{:S(2)}) copy-start(bf16[2048,256]{1,0:T(8,128)(2,1)} %copy-done.14) | copy-start | bytes 3145732
  124.0 41.6 %all-to-all-start.1 = ((bf16[64,8,768]{2,1,0:T(8,128)(2,1)}), bf16[64,8,768]{2,1,0:T(8,128)(2,1)S(1)}, u32[]{:S(2)}, u32[]{:S(2)}) async-start(bf16[64,8,768]{2,1,0:T(8,128)(2,1)} %bitcast.12), calls=%async_computation.1 | async-start | bytes 1572864 | tf_op jit(solution)/shard_map/all_to_all | solution.py:213
  135.3 11.2 %collective-permute-start.17 = (bf16[256,768]{1,0:T(8,128)(2,1)S(1)}, bf16[256,768]{1,0:T(8,128)(2,1)S(1)}, u32[]{:S(2)}, u32[]{:S(2)}) collective-permute-start(bf16[256,768]{1,0:T(8,128)(2,1)S(1)} %slice.58.refs_0_), channel_id=1, source_target_pairs={{0,1},{1,2},{2,3},{3,0},{4,5},{5,6},{6,7},{7,4},{8,9},{9,10},{10,1... | collective-permute-start | bytes 1179656 | tf_op jit(solution)/shard_map/ppermute | solution.py:20
  138.1 11.4 %collective-permute-start.21 = (bf16[256,512]{1,0:T(8,128)(2,1)S(1)}, bf16[256,512]{1,0:T(8,128)(2,1)S(1)}, u32[]{:S(2)}, u32[]{:S(2)}) collective-permute-start(bf16[256,512]{1,0:T(8,128)(2,1)S(1)} %slice.59.refs_4_), channel_id=1, source_target_pairs={{0,3},{1,0},{2,1},{3,2},{4,7},{5,4},{6,5},{7,6},{8,11},{9,8},{10,9... | collective-permute-start | bytes 786440 | tf_op jit(solution)/shard_map/ppermute | solution.py:20
  138.5 24.4 %collective-permute-start.18 = (bf16[256,768]{1,0:T(8,128)(2,1)S(1)}, bf16[256,768]{1,0:T(8,128)(2,1)S(1)}, u32[]{:S(2)}, u32[]{:S(2)}) collective-permute-start(bf16[256,768]{1,0:T(8,128)(2,1)S(1)} %slice.58.refs_0_), channel_id=1, source_target_pairs={{0,3},{1,0},{2,1},{3,2},{4,7},{5,4},{6,5},{7,6},{8,11},{9,8},{10,9... | collective-permute-start | bytes 1179656 | tf_op jit(solution)/shard_map/ppermute | solution.py:20
  146.5 16.4 %collective-permute-start.19 = (bf16[256,768]{1,0:T(8,128)(2,1)S(1)}, bf16[256,768]{1,0:T(8,128)(2,1)S(1)}, u32[]{:S(2)}, u32[]{:S(2)}) collective-permute-start(bf16[256,768]{1,0:T(8,128)(2,1)S(1)} %collective-permute-done.17.refs_1_), channel_id=1, source_target_pairs={{0,1},{1,2},{2,3},{3,0},{4,5},{5,6},{6,7},{7,4},{8,9},{9,10},{10,1... | collective-permute-start | bytes 1179656 | tf_op jit(solution)/shard_map/ppermute | solution.py:20
  149.5 13.4 %collective-permute-start.20 = (bf16[256,512]{1,0:T(8,128)(2,1)S(1)}, bf16[256,512]{1,0:T(8,128)(2,1)S(1)}, u32[]{:S(2)}, u32[]{:S(2)}) collective-permute-start(bf16[256,512]{1,0:T(8,128)(2,1)S(1)} %slice.59.refs_4_), channel_id=1, source_target_pairs={{0,1},{1,2},{2,3},{3,0},{4,5},{5,6},{6,7},{7,4},{8,9},{9,10},{10,1... | collective-permute-start | bytes 786440 | tf_op jit(solution)/shard_map/ppermute | solution.py:20
  149.5 13.4 %collective-permute-start.22 = (bf16[256,512]{1,0:T(8,128)(2,1)S(1)}, bf16[256,512]{1,0:T(8,128)(2,1)S(1)}, u32[]{:S(2)}, u32[]{:S(2)}) collective-permute-start(bf16[256,512]{1,0:T(8,128)(2,1)S(1)} %collective-permute-done.21.refs_6_), channel_id=1, source_target_pairs={{0,3},{1,0},{2,1},{3,2},{4,7},{5,4},{6,5},{7,6},{8,11},{9,8},{10,9... | collective-permute-start | bytes 786440 | tf_op jit(solution)/shard_map/ppermute | solution.py:20
  164.4 1.1 copy-start.1
  165.6 10.4 %copy-start.21 = (bf16[128,2048]{1,0:T(8,128)(2,1)S(1)}, bf16[128,2048]{1,0:T(8,128)(2,1)}, u32[]{:S(2)}) copy-start(bf16[128,2048]{1,0:T(8,128)(2,1)} %param.14) | copy-start | bytes 1572868
  165.6 10.5 %copy-start.22 = (bf16[128,2048]{1,0:T(8,128)(2,1)S(1)}, bf16[128,2048]{1,0:T(8,128)(2,1)}, u32[]{:S(2)}) copy-start(bf16[128,2048]{1,0:T(8,128)(2,1)} %param.13) | copy-start | bytes 1572868
  165.6 72.1 %all-to-all-start.2 = ((bf16[64,8,1280]{2,1,0:T(8,128)(2,1)}), bf16[64,8,1280]{2,1,0:T(8,128)(2,1)S(1)}, u32[]{:S(2)}, u32[]{:S(2)}) async-start(bf16[64,8,1280]{2,1,0:T(8,128)(2,1)} %bitcast.20), calls=%async_computation.2 | async-start | bytes 2621440 | tf_op jit(solution)/shard_map/all_to_all | solution.py:213
  176.0 5.5 %copy-start.24 = (bf16[3,2048]{1,0:T(4,128)(2,1)S(1)}, bf16[3,2048]{1,0:T(4,128)(2,1)}, u32[]{:S(2)}) copy-start(bf16[3,2048]{1,0:T(4,128)(2,1)} %param.15) | copy-start | bytes 36868
  176.0 6.9 %copy-start.23 = (bf16[128,2048]{1,0:T(8,128)(2,1)S(1)}, bf16[128,2048]{1,0:T(8,128)(2,1)}, u32[]{:S(2)}) copy-start(bf16[128,2048]{1,0:T(8,128)(2,1)} %param.12) | copy-start | bytes 1572868
  176.2 6.8 %collective-permute-start = (f32[2,2048]{1,0:T(2,128)S(1)}, f32[2,2048]{1,0:T(2,128)S(1)}, u32[]{:S(2)}, u32[]{:S(2)}) collective-permute-start(f32[2,2048]{1,0:T(2,128)S(1)} %slice.48), channel_id=1, source_target_pairs={{0,1},{1,2},{2,3},{3,4},{4,5},{5,6},{6,7},{7,8},{8,9},{9,10},{10,1... | collective-permute-start | bytes 49160 | tf_op jit(solution)/shard_map/ppermute | solution.py:194
  183.0 40.7 %copy-start.19 = (s32[128,2]{0,1:T(2,128)S(1)}, s32[128,2]{0,1:T(2,128)}, u32[]{:S(2)}) copy-start(s32[128,2]{0,1:T(2,128)} %param.22) | copy-start | bytes 3076
  183.0 40.7 %copy-start.20 = (f32[128,2]{0,1:T(2,128)S(1)}, f32[128,2]{0,1:T(2,128)}, u32[]{:S(2)}) copy-start(f32[128,2]{0,1:T(2,128)} %param.23) | copy-start | bytes 3076
  183.4 34.3 %collective-permute-start.1 = (bf16[128,2048]{1,0:T(8,128)(2,1)S(1)}, bf16[128,2048]{1,0:T(8,128)(2,1)S(1)}, u32[]{:S(2)}, u32[]{:S(2)}) collective-permute-start(bf16[128,2048]{1,0:T(8,128)(2,1)S(1)} %fusion.5.own_ref), channel_id=1, source_target_pairs={{0,1},{1,2},{2,3},{3,0},{4,5},{5,6},{6,7},{7,4},{8,9},{9,10},{10,1... | collective-permute-start | bytes 1572872 | tf_op jit(solution)/shard_map/ppermute | solution.py:20
  211.0 11.1 %collective-permute-start.2 = (bf16[128,2048]{1,0:T(8,128)(2,1)S(1)}, bf16[128,2048]{1,0:T(8,128)(2,1)S(1)}, u32[]{:S(2)}, u32[]{:S(2)}) collective-permute-start(bf16[128,2048]{1,0:T(8,128)(2,1)S(1)} %fusion.5.own_ref), channel_id=1, source_target_pairs={{0,3},{1,0},{2,1},{3,2},{4,7},{5,4},{6,5},{7,6},{8,11},{9,8},{10,9... | collective-permute-start | bytes 1572872 | tf_op jit(solution)/shard_map/ppermute | solution.py:20
  218.4 7.9 %collective-permute-start.3 = (bf16[64,2048]{1,0:T(8,128)(2,1)}, bf16[64,2048]{1,0:T(8,128)(2,1)}, u32[]{:S(2)}, u32[]{:S(2)}) collective-permute-start(bf16[64,2048]{1,0:T(8,128)(2,1)} %slice.54), channel_id=1, source_target_pairs={{0,1},{1,2},{2,3},{3,0},{4,5},{5,6},{6,7},{7,4},{8,9},{9,10},{10,1... | collective-permute-start | bytes 786440 | tf_op jit(solution)/shard_map/ppermute | solution.py:20
  223.7 7.9 %collective-permute-start.4 = (bf16[64,2048]{1,0:T(8,128)(2,1)}, bf16[64,2048]{1,0:T(8,128)(2,1)}, u32[]{:S(2)}, u32[]{:S(2)}) collective-permute-start(bf16[64,2048]{1,0:T(8,128)(2,1)} %slice.55), channel_id=1, source_target_pairs={{0,3},{1,0},{2,1},{3,2},{4,7},{5,4},{6,5},{7,6},{8,11},{9,8},{10,9... | collective-permute-start | bytes 786440 | tf_op jit(solution)/shard_map/ppermute | solution.py:20
  231.6 1.6 copy-start.2
  233.1 1.0 copy-start.4
  (3 other events, 2.2 us)

commit v3 on v2

--- a/solution.py
+++ b/solution.py
@@ -83,33 +83,65 @@
         copy.wait()
 
 
-def hidden_kernel(rows_ref, *refs):
-    weights, out_ref = refs[:-1], refs[-1]
-    units = weights[0].shape[1]
-    for i in range(len(weights) // 2):
-        gate = dot32(rows_ref[...], weights[2 * i][...])
-        up = dot32(rows_ref[...], weights[2 * i + 1][...])
-        out_ref[:, i * units : (i + 1) * units] = (gate / (1.0 + jnp.exp(-gate)) * up).astype(jnp.bfloat16)
-
-
-def down_kernel(near_ref, far_ref, *refs):
-    downs, (out_ref, hidden, weight) = refs[:-3], refs[-3:]
-    middle, units, at = near_ref.shape[1], far_ref.shape[1], 0
-    hidden[:, :middle] = near_ref[...]
-    hidden[:, middle:] = far_ref[...]
-    for i in range(0, len(downs), 4):
-        width = downs[i].shape[1]
-        for k in range(4):
-            weight[k * units : (k + 1) * units, at : at + width] = downs[i + k][...]
+def fetch(pairs, sems):
+    copies = [pltpu.make_async_copy(s, t, sems.at[i]) for i, (s, t) in enumerate(pairs)]
+    for copy in copies:
+        copy.start()
+    return copies
+
+
+def hidden_kernel(rows_ref, *refs, count):
+    weights, (out_ref, here, sems) = refs[: 2 * count], refs[2 * count :]
+    depth, units = weights[0].shape
+    half = depth // 2
+    parts = [(i, pl.ds(s * half, half)) for shard in range(count) for s in (0, 1) for i in (2 * shard, 2 * shard + 1)]
+    copies = fetch([(weights[i].at[p], here.at[i, p]) for i, p in parts], sems)
+    for shard in range(count):
+        sums = [0.0, 0.0]
+        for s in (0, 1):
+            for k in (0, 1):
+                copies[4 * shard + 2 * s + k].wait()
+            rows = rows_ref[:, s * half : (s + 1) * half]
+            sums = [total + dot32(rows, here[2 * shard + k, pl.ds(s * half, half)]) for k, total in enumerate(sums)]
+        gate, up = sums
+        out_ref[:, shard * units : (shard + 1) * units] = (gate / (1.0 + jnp.exp(-gate)) * up).astype(jnp.bfloat16)
+
+
+def stack_kernel(*refs, widths):
+    pieces, (out_ref, sems) = refs[:-2], refs[-2:]
+    units, at, pairs = pieces[0].shape[0], 0, []
+    for i, width in enumerate(widths):
+        for k in range(3):
+            pairs.append((pieces[3 * i + k], out_ref.at[pl.ds(k * units, units), pl.ds(at, width)]))
         at += width
-    out_ref[...] = dot32(hidden[...], weight[...]).astype(jnp.bfloat16)
-
-
-def on_core(kernel, shape, operands, mib, scratch=(), out=pltpu.VMEM):
+    for copy in fetch(pairs, sems):
+        copy.wait()
+
+
+def down_kernel(near_ref, far_ref, stacked_ref, *refs):
+    pieces, (out_ref, far_weight, made, came, sent) = refs[:-5], refs[-5:]
+    at, pairs, copies = 0, [], []
+    for piece in pieces:
+        pairs.append((piece, far_weight.at[:, pl.ds(at, piece.shape[1])]))
+        at += piece.shape[1]
+    for copy in fetch(pairs, came):
+        copy.wait()
+    for i in range(at // COLUMNS):
+        place = pl.ds(i * COLUMNS, COLUMNS)
+        total = dot32(near_ref[...], stacked_ref[:, place]) + dot32(far_ref[...], far_weight[:, place])
+        made[:, place] = total.astype(jnp.bfloat16)
+        copies.append(pltpu.make_async_copy(made.at[:, place], out_ref.at[:, place], sent.at[i]))
+        copies[-1].start()
+    for copy in copies:
+        copy.wait()
+
+
+def on_core(kernel, shape, operands, mib, scratch=(), out=pltpu.VMEM, away=0):
+    count = len(operands) - away
     return pl.pallas_call(
         kernel,
         out_shape=jax.ShapeDtypeStruct(shape, jnp.bfloat16),
-        in_specs=[pl.BlockSpec(memory_space=pltpu.VMEM)] * len(operands),
+        in_specs=[pl.BlockSpec(memory_space=pltpu.VMEM)] * count + [pl.BlockSpec(memory_space=pltpu.HBM)] * away,
         out_specs=pl.BlockSpec(memory_space=out),
         scratch_shapes=list(scratch),
         compiler_params=pltpu.CompilerParams(vmem_limit_bytes=mib * MIB),
@@ -200,16 +232,46 @@
     gated = (out_gate.astype(jnp.float32) * smoothed).astype(jnp.bfloat16)
 
     units = gate.shape[1]
-    near_weights = (gate, up, gates[0], ups[0], gates[1], ups[1])
-    near = on_core(hidden_kernel, (slots, 3 * units), (arrived, *near_weights), 12)
-    far = on_core(hidden_kernel, (slots, units), (arrived, gate_far, up_far), 8)
+
+    def hidden(shards):
+        weights = [w for shard in shards for w in shard]
+        scratch = (
+            pltpu.VMEM((len(weights), model_width, units), jnp.bfloat16),
+            pltpu.SemaphoreType.DMA((2 * len(weights),)),
+        )
+        return on_core(
+            lambda *refs: hidden_kernel(*refs, count=len(shards)),
+            (slots, len(shards) * units),
+            (arrived, *weights),
+            4 * len(shards) + 6,
+            scratch,
+            away=len(weights),
+        )
+
+    near = hidden(((gate, up), (gates[0], ups[0]), (gates[1], ups[1])))
+    far = hidden(((gate_far, up_far),))
 
     returned = []
     for chunk in CHUNKS:
-        width = sum(PIECES[piece] for piece in chunk)
-        operands = (near, far, *[d for piece in chunk for d in downs[piece]])
-        scratch = (pltpu.VMEM((slots, 4 * units), jnp.bfloat16), pltpu.VMEM((4 * units, width), jnp.bfloat16))
-        result = on_core(down_kernel, (slots, width), operands, 14, scratch)
+        widths = [PIECES[piece] for piece in chunk]
+        width = sum(widths)
+        sides = [d for piece in chunk for d in downs[piece][:3]]
+        stacked = on_core(
+            lambda *refs, widths=widths: stack_kernel(*refs, widths=widths),
+            (3 * units, width),
+            sides,
+            6,
+            (pltpu.SemaphoreType.DMA((len(sides),)),),
+            away=len(sides),
+        )
+        scratch = (
+            pltpu.VMEM((units, width), jnp.bfloat16),
+            pltpu.VMEM((slots, width), jnp.bfloat16),
+            pltpu.SemaphoreType.DMA((len(chunk),)),
+            pltpu.SemaphoreType.DMA((width // COLUMNS,)),
+        )
+        operands = (near, far, stacked, *[downs[piece][3] for piece in chunk])
+        result = on_core(down_kernel, (slots, width), operands, 12, scratch, pltpu.HBM, away=len(chunk))
         back = lax.all_to_all(result.reshape(expert_count, slot_cap, width), "ep", 0, 0, tiled=True)
         returned.append(back.reshape(slots, width))
 
@@ -228,7 +290,7 @@
         pltpu.VMEM((token_count, model_width), jnp.bfloat16),
         pltpu.SemaphoreType.DMA((model_width // COLUMNS,)),
     )
-    experts_out = on_core(combine_kernel, (token_count, model_width), (mix, *returned), 8, scratch, pl.ANY)
+    experts_out = on_core(combine_kernel, (token_count, model_width), (mix, *returned), 8, scratch, pltpu.HBM)
     return (mixer_out, experts_out)
 
 

time: 240 us -> 249 us (1.038)
  waiting for transfers between devices: 107 us -> 118 us
  local copies, waits for them, and re-layouts: 22.9 us -> 19.9 us
    ppermute x22, waiting for transfers between devices: 105 us -> 116 us  [turn(): return lax.ppermute(value, 'tp', pairs)]
    unnamed x50 -> x46, local copies, waits for them, and re-layouts: 18.4 us -> 15.3 us
    pallas_call x7 -> x9, Pallas kernels: 14.7 us -> 16.9 us  [on_core(): pl.pallas_call(kernel, out_shape=jax.ShapeDtypeStruct(shape, jnp.bfloat16...]
  transfers between devices with their start and end apart: 26 -> 26, of which waited for: 9 -> 12; matrix products, arithmetic and copies ran while one was open for 2% -> 2% of each run, Pallas kernels for 5% -> 6%
where the time goes in v3:
time: 249 us; the launch traced here: 248 us
  waiting for transfers between devices  118 us (47%)
  starting transfers between devices  88.5 us (36%)
  Pallas kernels  20.4 us (8%)
  local copies, waits for them, and re-layouts  19.9 us (8%)
    ppermute x22, waiting for transfers between devices, turn(): return lax.ppermute(value, 'tp', pairs)  116 us
    ppermute x22, starting transfers between devices, turn(): return lax.ppermute(value, 'tp', pairs)  51.6 us
    all_to_all x2, starting transfers between devices, local(): lax.all_to_all(result.reshape(expert_count, slot_cap, width), 'ep', 0, 0,...  20.7 us
    pallas_call x9, Pallas kernels, on_core(): pl.pallas_call(kernel, out_shape=jax.ShapeDtypeStruct(shape, jnp.bfloat16...  16.9 us
    unnamed x46, local copies, waits for them, and re-layouts  15.3 us
    all_to_all x1, starting transfers between devices, local(): lax.all_to_all(outgoing.reshape(expert_count, slot_cap, model_width), 'ep...  10.9 us
    ppermute x1, starting transfers between devices, local(): lax.ppermute(product[row_count - tap_span:], ('ep', 'tp'), [(i, i + 1) fo...  5.32 us
  transfers between devices with their start and end apart: 26, of which 12 were waited for; matrix products, arithmetic and copies ran while one was open for 2% of the time, Pallas kernels for 6%

profile of v3, /device:TPU:120, one launch (start us, length us, event | category | flops | bytes accessed | tf_op | source)
XLA Modules:
  0.0 248.1 jit_solution(10476761087526038429)
XLA Ops:
  0.6 1.0 copy-done.14
  3.0 0.9 shard_map.132
  4.0 1.3 copy-done
  5.3 10.9 %all-to-all-start = ((bf16[64,8,2048]{2,1,0:T(8,128)(2,1)}), bf16[64,8,2048]{2,1,0:T(8,128)(2,1)S(1)}, u32[]{:S(2)}, u32[]{:S(2)}) async-start(bf16[64,8,2048]{2,1,0:T(8,128)(2,1)} %bitcast.18), calls=%async_computation | async-start | bytes 4194304 | tf_op jit(solution)/shard_map/all_to_all | solution.py:213
  16.5 1.8 collective-permute-start.8
  18.3 1.4 collective-permute-start.6
  20.3 22.1 %collective-permute-done.5.refs_3_ = bf16[2048,256]{1,0:T(8,128)(2,1)} collective-permute-done((bf16[2048,256]{1,0:T(8,128)(2,1)S(1)}, bf16[2048,256]{1,0:T(8,128)(2,1)}, u32[]{:S(2)}, u32[]{:S(2)}) %collective-permute-start.5) | collective-permute-done | bytes 1048608 | tf_op jit(solution)/shard_map/ppermute | solution.py:20
  42.4 1.4 collective-permute-start.9
  44.6 1.1 fusion.7
  45.7 2.7 %collective-permute-start.11 = (bf16[256,384]{1,0:T(8,128)(2,1)S(1)}, bf16[256,384]{1,0:T(8,128)(2,1)S(1)}, u32[]{:S(2)}, u32[]{:S(2)}) collective-permute-start(bf16[256,384]{1,0:T(8,128)(2,1)S(1)} %get-tuple-element.3.refs_0_), channel_id=1, source_target_pairs={{0,1},{1,2},{2,3},{3,0},{4,5},{5,6},{6,7},{7,4},{8,9},{9,10},{10,1... | collective-permute-start | bytes 589832 | tf_op jit(solution)/shard_map/ppermute | solution.py:20
  48.4 42.2 %collective-permute-done.11.refs_1_ = bf16[256,384]{1,0:T(8,128)(2,1)S(1)} collective-permute-done((bf16[256,384]{1,0:T(8,128)(2,1)S(1)}, bf16[256,384]{1,0:T(8,128)(2,1)S(1)}, u32[]{:S(2)}, u32[]{:S(2)}) %collective-permute-start.11) | collective-permute-done | bytes 196640 | tf_op jit(solution)/shard_map/ppermute | solution.py:20
  90.6 0.7 collective-permute-start.12
  91.3 6.5 %collective-permute-done.12.refs_2_ = bf16[256,384]{1,0:T(8,128)(2,1)S(1)} collective-permute-done((bf16[256,384]{1,0:T(8,128)(2,1)S(1)}, bf16[256,384]{1,0:T(8,128)(2,1)S(1)}, u32[]{:S(2)}, u32[]{:S(2)}) %collective-permute-start.12) | collective-permute-done | bytes 196640 | tf_op jit(solution)/shard_map/ppermute | solution.py:20
  98.2 5.3 %collective-permute-done.13.refs_4_ = bf16[256,384]{1,0:T(8,128)(2,1)S(1)} collective-permute-done((bf16[256,384]{1,0:T(8,128)(2,1)S(1)}, bf16[256,384]{1,0:T(8,128)(2,1)S(1)}, u32[]{:S(2)}, u32[]{:S(2)}) %collective-permute-start.13) | collective-permute-done | bytes 196640 | tf_op jit(solution)/shard_map/ppermute | solution.py:20
  103.5 6.9 %collective-permute-done.14.refs_5_ = bf16[256,384]{1,0:T(8,128)(2,1)S(1)} collective-permute-done((bf16[256,384]{1,0:T(8,128)(2,1)S(1)}, bf16[256,384]{1,0:T(8,128)(2,1)S(1)}, u32[]{:S(2)}, u32[]{:S(2)}) %collective-permute-start.14) | collective-permute-done | bytes 196640 | tf_op jit(solution)/shard_map/ppermute | solution.py:20
  110.4 1.3 collective-permute-start.15
  112.8 1.0 copy-done.2
  113.8 1.0 copy-done.12
  114.8 1.2 copy-done.8
  116.0 1.2 copy-done.9
  117.3 1.2 copy-done.11
  118.5 1.2 copy-done.13
  119.7 4.7 %shard_map.133.near_ref = bf16[512,768]{1,0:T(8,128)(2,1)S(1)} custom-call(bf16[512,2048]{1,0:T(8,128)(2,1)S(1)} %bitcast.16, bf16[2048,256]{1,0:T(8,128)(2,1)S(1)} %bitcast.24, bf16[2048,256]{1,0:T(8,128)(2,1)S(1)} %bitcast.27, bf16[2048,256]{1,0:T(8,128)(2,1)} %collective-permute-done.5.refs_3_, bf16[2048,256]{1,0:T(8,128)(2,1)S(1)} %copy-done.11, ...), custom_call_target="tpu_custom_call" | custom-call | tf_op jit(solution)/shard_map/pallas_call | solution.py:141
  124.4 2.9 %shard_map.134.far_ref = bf16[512,256]{1,0:T(8,128)(2,1)S(1)} custom-call(bf16[512,2048]{1,0:T(8,128)(2,1)S(1)} %bitcast.17, bf16[2048,256]{1,0:T(8,128)(2,1)} %collective-permute-done.9.refs_1_, bf16[2048,256]{1,0:T(8,128)(2,1)} %collective-permute-done.10.refs_2_), custom_call_target="tpu_custom_call" | custom-call | tf_op jit(solution)/shard_map/pallas_call | solution.py:141
  127.4 2.9 %shard_map.136 = bf16[512,768]{1,0:T(8,128)(2,1)} custom-call(bf16[512,768]{1,0:T(8,128)(2,1)S(1)} %shard_map.133.near_ref, bf16[512,256]{1,0:T(8,128)(2,1)S(1)} %shard_map.134.far_ref, bf16[768,768]{1,0:T(8,128)(2,1)S(1)} %copy-done.3, bf16[256,384]{1,0:T(8,128)(2,1)} %collective-permute-done.15.refs_0_, bf16[256,384]{1,0:T(8,128)(2,1)} %collective-permute-done.16.refs_1_), custom_call_target="tpu_custom_call" | custom-call | tf_op jit(solution)/shard_map/pallas_call | solution.py:141
  130.3 10.3 %all-to-all-start.1 = ((bf16[64,8,768]{2,1,0:T(8,128)(2,1)}), bf16[64,8,768]{2,1,0:T(8,128)(2,1)S(1)}, u32[]{:S(2)}, u32[]{:S(2)}) async-start(bf16[64,8,768]{2,1,0:T(8,128)(2,1)} %bitcast.12), calls=%async_computation.1 | async-start | bytes 1572864 | tf_op jit(solution)/shard_map/all_to_all | solution.py:275
  140.6 1.0 slice.58.refs_0_
  141.6 2.5 collective-permute-start.17
  144.0 1.0 slice.59.refs_3_
  145.5 7.4 %collective-permute-done.17.refs_1_ = bf16[256,768]{1,0:T(8,128)(2,1)S(1)} collective-permute-done((bf16[256,768]{1,0:T(8,128)(2,1)S(1)}, bf16[256,768]{1,0:T(8,128)(2,1)S(1)}, u32[]{:S(2)}, u32[]{:S(2)}) %collective-permute-start.17) | collective-permute-done | bytes 393248 | tf_op jit(solution)/shard_map/ppermute | solution.py:20
  152.8 3.6 %collective-permute-start.21 = (bf16[256,768]{1,0:T(8,128)(2,1)S(1)}, bf16[256,768]{1,0:T(8,128)(2,1)S(1)}, u32[]{:S(2)}, u32[]{:S(2)}) collective-permute-start(bf16[256,768]{1,0:T(8,128)(2,1)S(1)} %collective-permute-done.17.refs_1_), channel_id=1, source_target_pairs={{0,1},{1,2},{2,3},{3,0},{4,5},{5,6},{6,7},{7,4},{8,9},{9,10},{10,1... | collective-permute-start | bytes 1179656 | tf_op jit(solution)/shard_map/ppermute | solution.py:20
  156.4 2.0 collective-permute-start.22
  158.4 11.4 %collective-permute-done.19.refs_4_ = bf16[256,512]{1,0:T(8,128)(2,1)S(1)} collective-permute-done((bf16[256,512]{1,0:T(8,128)(2,1)S(1)}, bf16[256,512]{1,0:T(8,128)(2,1)S(1)}, u32[]{:S(2)}, u32[]{:S(2)}) %collective-permute-start.19) | collective-permute-done | bytes 262176 | tf_op jit(solution)/shard_map/ppermute | solution.py:20
  170.1 3.4 %shard_map.138 = bf16[512,1280]{1,0:T(8,128)(2,1)S(1)} custom-call(bf16[512,768]{1,0:T(8,128)(2,1)S(1)} %shard_map.133.near_ref, bf16[512,256]{1,0:T(8,128)(2,1)S(1)} %shard_map.134.far_ref, bf16[768,1280]{1,0:T(8,128)(2,1)S(1)} %shard_map.137.stacked_ref, bf16[256,768]{1,0:T(8,128)(2,1)S(1)} %collective-permute-done.21.refs_0_, ...), custom_call_target="tpu_custom_call" | custom-call | tf_op jit(solution)/shard_map/pallas_call | solution.py:141
  173.5 1.1 copy-done.1
  174.6 10.4 %all-to-all-start.2 = ((bf16[64,8,1280]{2,1,0:T(8,128)(2,1)}), bf16[64,8,1280]{2,1,0:T(8,128)(2,1)S(1)}, u32[]{:S(2)}, u32[]{:S(2)}) async-start(bf16[64,8,1280]{2,1,0:T(8,128)(2,1)} %bitcast.20), calls=%async_computation.2 | async-start | bytes 2621440 | tf_op jit(solution)/shard_map/all_to_all | solution.py:275
  185.2 5.3 %collective-permute-start = (f32[2,2048]{1,0:T(2,128)S(1)}, f32[2,2048]{1,0:T(2,128)S(1)}, u32[]{:S(2)}, u32[]{:S(2)}) collective-permute-start(f32[2,2048]{1,0:T(2,128)S(1)} %slice.48), channel_id=1, source_target_pairs={{0,1},{1,2},{2,3},{3,4},{4,5},{5,6},{6,7},{7,8},{8,9},{9,10},{10,1... | collective-permute-start | bytes 49160 | tf_op jit(solution)/shard_map/ppermute | solution.py:226
  190.6 1.4 collective-permute-done
  192.4 27.4 %collective-permute-start.1 = (bf16[128,2048]{1,0:T(8,128)(2,1)S(1)}, bf16[128,2048]{1,0:T(8,128)(2,1)S(1)}, u32[]{:S(2)}, u32[]{:S(2)}) collective-permute-start(bf16[128,2048]{1,0:T(8,128)(2,1)S(1)} %fusion.5.own_ref), channel_id=1, source_target_pairs={{0,1},{1,2},{2,3},{3,0},{4,5},{5,6},{6,7},{7,4},{8,9},{9,10},{10,1... | collective-permute-start | bytes 1572872 | tf_op jit(solution)/shard_map/ppermute | solution.py:20
  219.8 6.7 %collective-permute-done.1.left_ref = bf16[128,2048]{1,0:T(8,128)(2,1)S(1)} collective-permute-done((bf16[128,2048]{1,0:T(8,128)(2,1)S(1)}, bf16[128,2048]{1,0:T(8,128)(2,1)S(1)}, u32[]{:S(2)}, u32[]{:S(2)}) %collective-permute-start.1) | collective-permute-done | bytes 524320 | tf_op jit(solution)/shard_map/ppermute | solution.py:20
  227.2 3.7 %collective-permute-start.3 = (bf16[64,2048]{1,0:T(8,128)(2,1)}, bf16[64,2048]{1,0:T(8,128)(2,1)}, u32[]{:S(2)}, u32[]{:S(2)}) collective-permute-start(bf16[64,2048]{1,0:T(8,128)(2,1)} %slice.54), channel_id=1, source_target_pairs={{0,1},{1,2},{2,3},{3,0},{4,5},{5,6},{6,7},{7,4},{8,9},{9,10},{10,1... | collective-permute-start | bytes 786440 | tf_op jit(solution)/shard_map/ppermute | solution.py:20
  231.7 0.8 copy-done.5
  232.8 2.4 collective-permute-done.3.first_ref
  235.1 5.2 %collective-permute-done.4.second_ref = bf16[64,2048]{1,0:T(8,128)(2,1)} collective-permute-done((bf16[64,2048]{1,0:T(8,128)(2,1)}, bf16[64,2048]{1,0:T(8,128)(2,1)}, u32[]{:S(2)}, u32[]{:S(2)}) %collective-permute-start.4) | collective-permute-done | bytes 262176 | tf_op jit(solution)/shard_map/ppermute | solution.py:20
  240.3 1.6 copy-done.4
  241.9 1.0 copy-done.6
  243.0 3.5 %mixer.1 = bf16[512,512]{1,0:T(8,128)(2,1)} custom-call(s32[1]{0:T(128)} %bitcast.place_ref, bf16[128,2048]{1,0:T(8,128)(2,1)S(1)} %fusion.5.own_ref, bf16[128,2048]{1,0:T(8,128)(2,1)S(1)} %collective-permute-done.1.left_ref, bf16[128,2048]{1,0:T(8,128)(2,1)S(1)} %copy-done.6, bf16[64,2048]{1,0:T(8,128)(2,1)} %collective-permute-done.3.first_ref, ...), custom_call_target="tpu_custom_call" | custom-call | tf_op jit(solution)/shard_map/mixer/pallas_call | solution.py:280
  246.5 1.4 shard_map.139
  (69 shorter events, 7.5 us)
Async XLA Ops:
  0.6 1.0 copy-start.14
  1.7 0.7 copy-start.15
  4.0 1.3 copy-start
  5.3 10.9 %copy-start.7 = (bf16[1,2048,256]{2,1,0:T(8,128)(2,1)S(1)}, bf16[1,2048,256]{2,1,0:T(8,128)(2,1)}, u32[]{:S(2)}) copy-start(bf16[1,2048,256]{2,1,0:T(8,128)(2,1)} %param.19) | copy-start | bytes 3145732
  5.3 109.5 %all-to-all-start = ((bf16[64,8,2048]{2,1,0:T(8,128)(2,1)}), bf16[64,8,2048]{2,1,0:T(8,128)(2,1)S(1)}, u32[]{:S(2)}, u32[]{:S(2)}) async-start(bf16[64,8,2048]{2,1,0:T(8,128)(2,1)} %bitcast.18), calls=%async_computation | async-start | bytes 4194304 | tf_op jit(solution)/shard_map/all_to_all | solution.py:213
  16.2 26.2 %collective-permute-start.5 = (bf16[2048,256]{1,0:T(8,128)(2,1)S(1)}, bf16[2048,256]{1,0:T(8,128)(2,1)}, u32[]{:S(2)}, u32[]{:S(2)}) collective-permute-start(bf16[2048,256]{1,0:T(8,128)(2,1)S(1)} %bitcast.22), channel_id=1, source_target_pairs={{0,1},{1,2},{2,3},{3,0},{4,5},{5,6},{6,7},{7,4},{8,9},{9,10},{10,1... | collective-permute-start | bytes 3145736 | tf_op jit(solution)/shard_map/ppermute | solution.py:20
  16.5 27.6 %collective-permute-start.8 = (bf16[2048,256]{1,0:T(8,128)(2,1)}, bf16[2048,256]{1,0:T(8,128)(2,1)}, u32[]{:S(2)}, u32[]{:S(2)}) collective-permute-start(bf16[2048,256]{1,0:T(8,128)(2,1)} %bitcast.25), channel_id=1, source_target_pairs={{0,3},{1,0},{2,1},{3,2},{4,7},{5,4},{6,5},{7,6},{8,11},{9,8},{10,9... | collective-permute-start | bytes 3145736 | tf_op jit(solution)/shard_map/ppermute | solution.py:20
  18.3 93.5 %collective-permute-start.6 = (bf16[2048,256]{1,0:T(8,128)(2,1)}, bf16[2048,256]{1,0:T(8,128)(2,1)S(1)}, u32[]{:S(2)}, u32[]{:S(2)}) collective-permute-start(bf16[2048,256]{1,0:T(8,128)(2,1)} %bitcast.26), channel_id=1, source_target_pairs={{0,1},{1,2},{2,3},{3,0},{4,5},{5,6},{6,7},{7,4},{8,9},{9,10},{10,1... | collective-permute-start | bytes 3145736 | tf_op jit(solution)/shard_map/ppermute | solution.py:20
  19.7 94.1 %collective-permute-start.7 = (bf16[2048,256]{1,0:T(8,128)(2,1)S(1)}, bf16[2048,256]{1,0:T(8,128)(2,1)S(1)}, u32[]{:S(2)}, u32[]{:S(2)}) collective-permute-start(bf16[2048,256]{1,0:T(8,128)(2,1)S(1)} %bitcast.23), channel_id=1, source_target_pairs={{0,3},{1,0},{2,1},{3,2},{4,7},{5,4},{6,5},{7,6},{8,11},{9,8},{10,9... | collective-permute-start | bytes 3145736 | tf_op jit(solution)/shard_map/ppermute | solution.py:20
  42.4 82.0 %collective-permute-start.9 = (bf16[2048,256]{1,0:T(8,128)(2,1)}, bf16[2048,256]{1,0:T(8,128)(2,1)}, u32[]{:S(2)}, u32[]{:S(2)}) collective-permute-start(bf16[2048,256]{1,0:T(8,128)(2,1)} %collective-permute-done.5.refs_3_), channel_id=1, source_target_pairs={{0,1},{1,2},{2,3},{3,0},{4,5},{5,6},{6,7},{7,4},{8,9},{9,10},{10,1... | collective-permute-start | bytes 3145736 | tf_op jit(solution)/shard_map/ppermute | solution.py:20
  44.0 80.4 %collective-permute-start.10 = (bf16[2048,256]{1,0:T(8,128)(2,1)}, bf16[2048,256]{1,0:T(8,128)(2,1)}, u32[]{:S(2)}, u32[]{:S(2)}) collective-permute-start(bf16[2048,256]{1,0:T(8,128)(2,1)} %collective-permute-done.8.refs_6_), channel_id=1, source_target_pairs={{0,3},{1,0},{2,1},{3,2},{4,7},{5,4},{6,5},{7,6},{8,11},{9,8},{10,9... | collective-permute-start | bytes 3145736 | tf_op jit(solution)/shard_map/ppermute | solution.py:20
  45.7 44.9 %collective-permute-start.11 = (bf16[256,384]{1,0:T(8,128)(2,1)S(1)}, bf16[256,384]{1,0:T(8,128)(2,1)S(1)}, u32[]{:S(2)}, u32[]{:S(2)}) collective-permute-start(bf16[256,384]{1,0:T(8,128)(2,1)S(1)} %get-tuple-element.3.refs_0_), channel_id=1, source_target_pairs={{0,1},{1,2},{2,3},{3,0},{4,5},{5,6},{6,7},{7,4},{8,9},{9,10},{10,1... | collective-permute-start | bytes 589832 | tf_op jit(solution)/shard_map/ppermute | solution.py:20
  90.6 7.3 %collective-permute-start.12 = (bf16[256,384]{1,0:T(8,128)(2,1)S(1)}, bf16[256,384]{1,0:T(8,128)(2,1)S(1)}, u32[]{:S(2)}, u32[]{:S(2)}) collective-permute-start(bf16[256,384]{1,0:T(8,128)(2,1)S(1)} %get-tuple-element.3.refs_0_), channel_id=1, source_target_pairs={{0,3},{1,0},{2,1},{3,2},{4,7},{5,4},{6,5},{7,6},{8,11},{9,8},{10,9... | collective-permute-start | bytes 589832 | tf_op jit(solution)/shard_map/ppermute | solution.py:20
  97.9 5.7 %collective-permute-start.13 = (bf16[256,384]{1,0:T(8,128)(2,1)S(1)}, bf16[256,384]{1,0:T(8,128)(2,1)S(1)}, u32[]{:S(2)}, u32[]{:S(2)}) collective-permute-start(bf16[256,384]{1,0:T(8,128)(2,1)S(1)} %get-tuple-element.2.refs_3_), channel_id=1, source_target_pairs={{0,1},{1,2},{2,3},{3,0},{4,5},{5,6},{6,7},{7,4},{8,9},{9,10},{10,1... | collective-permute-start | bytes 589832 | tf_op jit(solution)/shard_map/ppermute | solution.py:20
  103.5 6.9 %collective-permute-start.14 = (bf16[256,384]{1,0:T(8,128)(2,1)S(1)}, bf16[256,384]{1,0:T(8,128)(2,1)S(1)}, u32[]{:S(2)}, u32[]{:S(2)}) collective-permute-start(bf16[256,384]{1,0:T(8,128)(2,1)S(1)} %get-tuple-element.2.refs_3_), channel_id=1, source_target_pairs={{0,3},{1,0},{2,1},{3,2},{4,7},{5,4},{6,5},{7,6},{8,11},{9,8},{10,9... | collective-permute-start | bytes 589832 | tf_op jit(solution)/shard_map/ppermute | solution.py:20
  110.4 16.9 %collective-permute-start.15 = (bf16[256,384]{1,0:T(8,128)(2,1)S(1)}, bf16[256,384]{1,0:T(8,128)(2,1)}, u32[]{:S(2)}, u32[]{:S(2)}) collective-permute-start(bf16[256,384]{1,0:T(8,128)(2,1)S(1)} %collective-permute-done.11.refs_1_), channel_id=1, source_target_pairs={{0,1},{1,2},{2,3},{3,0},{4,5},{5,6},{6,7},{7,4},{8,9},{9,10},{10,1... | collective-permute-start | bytes 589832 | tf_op jit(solution)/shard_map/ppermute | solution.py:20
  111.7 1.1 copy-start.10
  111.7 15.6 %collective-permute-start.16 = (bf16[256,384]{1,0:T(8,128)(2,1)S(1)}, bf16[256,384]{1,0:T(8,128)(2,1)}, u32[]{:S(2)}, u32[]{:S(2)}) collective-permute-start(bf16[256,384]{1,0:T(8,128)(2,1)S(1)} %collective-permute-done.14.refs_5_), channel_id=1, source_target_pairs={{0,3},{1,0},{2,1},{3,2},{4,7},{5,4},{6,5},{7,6},{8,11},{9,8},{10,9... | collective-permute-start | bytes 589832 | tf_op jit(solution)/shard_map/ppermute | solution.py:20
  112.8 1.0 copy-start.2
  113.8 1.0 copy-start.12
  114.8 1.2 copy-start.8
  116.0 1.2 copy-start.9
  117.3 1.2 copy-start.11
  118.5 1.2 copy-start.13
  124.4 3.0 %copy-start.3 = (bf16[768,768]{1,0:T(8,128)(2,1)S(1)}, bf16[768,768]{1,0:T(8,128)(2,1)}, u32[]{:S(2)}) copy-start(bf16[768,768]{1,0:T(8,128)(2,1)} %copy-done.2) | copy-start | bytes 3538948
  130.3 44.3 %all-to-all-start.1 = ((bf16[64,8,768]{2,1,0:T(8,128)(2,1)}), bf16[64,8,768]{2,1,0:T(8,128)(2,1)S(1)}, u32[]{:S(2)}, u32[]{:S(2)}) async-start(bf16[64,8,768]{2,1,0:T(8,128)(2,1)} %bitcast.12), calls=%async_computation.1 | async-start | bytes 1572864 | tf_op jit(solution)/shard_map/all_to_all | solution.py:275
  141.6 11.2 %collective-permute-start.17 = (bf16[256,768]{1,0:T(8,128)(2,1)S(1)}, bf16[256,768]{1,0:T(8,128)(2,1)S(1)}, u32[]{:S(2)}, u32[]{:S(2)}) collective-permute-start(bf16[256,768]{1,0:T(8,128)(2,1)S(1)} %slice.58.refs_0_), channel_id=1, source_target_pairs={{0,1},{1,2},{2,3},{3,0},{4,5},{5,6},{6,7},{7,4},{8,9},{9,10},{10,1... | collective-permute-start | bytes 1179656 | tf_op jit(solution)/shard_map/ppermute | solution.py:20
  145.0 11.4 %collective-permute-start.20 = (bf16[256,512]{1,0:T(8,128)(2,1)S(1)}, bf16[256,512]{1,0:T(8,128)(2,1)S(1)}, u32[]{:S(2)}, u32[]{:S(2)}) collective-permute-start(bf16[256,512]{1,0:T(8,128)(2,1)S(1)} %slice.59.refs_3_), channel_id=1, source_target_pairs={{0,3},{1,0},{2,1},{3,2},{4,7},{5,4},{6,5},{7,6},{8,11},{9,8},{10,9... | collective-permute-start | bytes 786440 | tf_op jit(solution)/shard_map/ppermute | solution.py:20
  145.1 24.7 %collective-permute-start.18 = (bf16[256,768]{1,0:T(8,128)(2,1)S(1)}, bf16[256,768]{1,0:T(8,128)(2,1)S(1)}, u32[]{:S(2)}, u32[]{:S(2)}) collective-permute-start(bf16[256,768]{1,0:T(8,128)(2,1)S(1)} %slice.58.refs_0_), channel_id=1, source_target_pairs={{0,3},{1,0},{2,1},{3,2},{4,7},{5,4},{6,5},{7,6},{8,11},{9,8},{10,9... | collective-permute-start | bytes 1179656 | tf_op jit(solution)/shard_map/ppermute | solution.py:20
  152.8 17.2 %collective-permute-start.21 = (bf16[256,768]{1,0:T(8,128)(2,1)S(1)}, bf16[256,768]{1,0:T(8,128)(2,1)S(1)}, u32[]{:S(2)}, u32[]{:S(2)}) collective-permute-start(bf16[256,768]{1,0:T(8,128)(2,1)S(1)} %collective-permute-done.17.refs_1_), channel_id=1, source_target_pairs={{0,1},{1,2},{2,3},{3,0},{4,5},{5,6},{6,7},{7,4},{8,9},{9,10},{10,1... | collective-permute-start | bytes 1179656 | tf_op jit(solution)/shard_map/ppermute | solution.py:20
  156.4 13.4 %collective-permute-start.19 = (bf16[256,512]{1,0:T(8,128)(2,1)S(1)}, bf16[256,512]{1,0:T(8,128)(2,1)S(1)}, u32[]{:S(2)}, u32[]{:S(2)}) collective-permute-start(bf16[256,512]{1,0:T(8,128)(2,1)S(1)} %slice.59.refs_3_), channel_id=1, source_target_pairs={{0,1},{1,2},{2,3},{3,0},{4,5},{5,6},{6,7},{7,4},{8,9},{9,10},{10,1... | collective-permute-start | bytes 786440 | tf_op jit(solution)/shard_map/ppermute | solution.py:20
  156.4 13.6 %collective-permute-start.22 = (bf16[256,512]{1,0:T(8,128)(2,1)S(1)}, bf16[256,512]{1,0:T(8,128)(2,1)S(1)}, u32[]{:S(2)}, u32[]{:S(2)}) collective-permute-start(bf16[256,512]{1,0:T(8,128)(2,1)S(1)} %collective-permute-done.20.refs_5_), channel_id=1, source_target_pairs={{0,3},{1,0},{2,1},{3,2},{4,7},{5,4},{6,5},{7,6},{8,11},{9,8},{10,9... | collective-permute-start | bytes 786440 | tf_op jit(solution)/shard_map/ppermute | solution.py:20
  173.5 1.1 copy-start.1
  174.6 10.4 %copy-start.19 = (bf16[128,2048]{1,0:T(8,128)(2,1)S(1)}, bf16[128,2048]{1,0:T(8,128)(2,1)}, u32[]{:S(2)}) copy-start(bf16[128,2048]{1,0:T(8,128)(2,1)} %param.14) | copy-start | bytes 1572868
  174.6 10.4 %copy-start.20 = (bf16[128,2048]{1,0:T(8,128)(2,1)S(1)}, bf16[128,2048]{1,0:T(8,128)(2,1)}, u32[]{:S(2)}) copy-start(bf16[128,2048]{1,0:T(8,128)(2,1)} %param.13) | copy-start | bytes 1572868
  174.6 71.9 %all-to-all-start.2 = ((bf16[64,8,1280]{2,1,0:T(8,128)(2,1)}), bf16[64,8,1280]{2,1,0:T(8,128)(2,1)S(1)}, u32[]{:S(2)}, u32[]{:S(2)}) async-start(bf16[64,8,1280]{2,1,0:T(8,128)(2,1)} %bitcast.20), calls=%async_computation.2 | async-start | bytes 2621440 | tf_op jit(solution)/shard_map/all_to_all | solution.py:275
  185.0 5.5 %copy-start.22 = (bf16[3,2048]{1,0:T(4,128)(2,1)S(1)}, bf16[3,2048]{1,0:T(4,128)(2,1)}, u32[]{:S(2)}) copy-start(bf16[3,2048]{1,0:T(4,128)(2,1)} %param.15) | copy-start | bytes 36868
  185.1 6.9 %copy-start.21 = (bf16[128,2048]{1,0:T(8,128)(2,1)S(1)}, bf16[128,2048]{1,0:T(8,128)(2,1)}, u32[]{:S(2)}) copy-start(bf16[128,2048]{1,0:T(8,128)(2,1)} %param.12) | copy-start | bytes 1572868
  185.2 6.8 %collective-permute-start = (f32[2,2048]{1,0:T(2,128)S(1)}, f32[2,2048]{1,0:T(2,128)S(1)}, u32[]{:S(2)}, u32[]{:S(2)}) collective-permute-start(f32[2,2048]{1,0:T(2,128)S(1)} %slice.48), channel_id=1, source_target_pairs={{0,1},{1,2},{2,3},{3,4},{4,5},{5,6},{6,7},{7,8},{8,9},{9,10},{10,1... | collective-permute-start | bytes 49160 | tf_op jit(solution)/shard_map/ppermute | solution.py:226
  192.0 40.5 %copy-start.17 = (s32[128,2]{0,1:T(2,128)S(1)}, s32[128,2]{0,1:T(2,128)}, u32[]{:S(2)}) copy-start(s32[128,2]{0,1:T(2,128)} %param.22) | copy-start | bytes 3076
  192.0 40.5 %copy-start.18 = (f32[128,2]{0,1:T(2,128)S(1)}, f32[128,2]{0,1:T(2,128)}, u32[]{:S(2)}) copy-start(f32[128,2]{0,1:T(2,128)} %param.23) | copy-start | bytes 3076
  192.4 34.1 %collective-permute-start.1 = (bf16[128,2048]{1,0:T(8,128)(2,1)S(1)}, bf16[128,2048]{1,0:T(8,128)(2,1)S(1)}, u32[]{:S(2)}, u32[]{:S(2)}) collective-permute-start(bf16[128,2048]{1,0:T(8,128)(2,1)S(1)} %fusion.5.own_ref), channel_id=1, source_target_pairs={{0,1},{1,2},{2,3},{3,0},{4,5},{5,6},{6,7},{7,4},{8,9},{9,10},{10,1... | collective-permute-start | bytes 1572872 | tf_op jit(solution)/shard_map/ppermute | solution.py:20
  219.8 11.1 %collective-permute-start.2 = (bf16[128,2048]{1,0:T(8,128)(2,1)S(1)}, bf16[128,2048]{1,0:T(8,128)(2,1)S(1)}, u32[]{:S(2)}, u32[]{:S(2)}) collective-permute-start(bf16[128,2048]{1,0:T(8,128)(2,1)S(1)} %fusion.5.own_ref), channel_id=1, source_target_pairs={{0,3},{1,0},{2,1},{3,2},{4,7},{5,4},{6,5},{7,6},{8,11},{9,8},{10,9... | collective-permute-start | bytes 1572872 | tf_op jit(solution)/shard_map/ppermute | solution.py:20
  227.2 7.9 %collective-permute-start.3 = (bf16[64,2048]{1,0:T(8,128)(2,1)}, bf16[64,2048]{1,0:T(8,128)(2,1)}, u32[]{:S(2)}, u32[]{:S(2)}) collective-permute-start(bf16[64,2048]{1,0:T(8,128)(2,1)} %slice.54), channel_id=1, source_target_pairs={{0,1},{1,2},{2,3},{3,0},{4,5},{5,6},{6,7},{7,4},{8,9},{9,10},{10,1... | collective-permute-start | bytes 786440 | tf_op jit(solution)/shard_map/ppermute | solution.py:20
  231.7 0.8 copy-start.5
  232.4 7.9 %collective-permute-start.4 = (bf16[64,2048]{1,0:T(8,128)(2,1)}, bf16[64,2048]{1,0:T(8,128)(2,1)}, u32[]{:S(2)}, u32[]{:S(2)}) collective-permute-start(bf16[64,2048]{1,0:T(8,128)(2,1)} %slice.55), channel_id=1, source_target_pairs={{0,3},{1,0},{2,1},{3,2},{4,7},{5,4},{6,5},{7,6},{8,11},{9,8},{10,9... | collective-permute-start | bytes 786440 | tf_op jit(solution)/shard_map/ppermute | solution.py:20
  240.3 1.6 copy-start.4
  241.9 1.0 copy-start.6
  (1 other events, 0.7 us)

commit v4 on v3

--- a/solution.py
+++ b/solution.py
@@ -8,7 +8,7 @@
 
 CONV = 3
 NORM_EPS = 1e-06
-PIECES = (384, 384, 768, 512)
+PIECES = (512, 512, 512, 512)
 CHUNKS = ((0, 1), (2, 3))
 COLUMNS = 256
 MIB = 1 << 20
@@ -29,9 +29,9 @@
     return turn(left[:half], 1), turn(right[half:], -1)
 
 
-def slot_table(ids, expert_count, slot_cap):
+def slot_table(ids, expert_count, slot_cap, number=lambda i: i):
     tokens = ids.shape[1]
-    expert = lax.broadcasted_iota(jnp.int32, (expert_count, tokens), 0)
+    expert = number(lax.broadcasted_iota(jnp.int32, (expert_count, tokens), 0))
     chosen = [ids[k : k + 1] == expert for k in range(ids.shape[0])]
     member = jnp.where(chosen[0] | chosen[1], 1.0, 0.0).astype(jnp.bfloat16)
     row = lax.broadcasted_iota(jnp.int32, (tokens, tokens), 0)
@@ -57,28 +57,55 @@
     out_ref[...] = jnp.dot(table, normed, preferred_element_type=jnp.float32).astype(jnp.bfloat16)
 
 
-def mix_kernel(ids_ref, weight_ref, out_ref, *, expert_count, slot_cap):
-    weight = weight_ref[...]
+def mix_kernel(place_ref, ids_ref, weight_ref, out_ref, *, expert_count, slot_cap):
+    weight, ids = weight_ref[...], ids_ref[...]
     tokens = weight.shape[1]
     share = weight / (weight[0:1] + weight[1:2])
-    tables = slot_table(ids_ref[...], expert_count, slot_cap)
-    mix = (tables[0] * share[0:1] + tables[1] * share[1:2]).T
-    high = mix.astype(jnp.bfloat16)
-    out_ref[:tokens] = high
-    out_ref[tokens:] = (mix - high.astype(jnp.float32)).astype(jnp.bfloat16)
-
-
-def combine_kernel(mix_ref, *refs):
-    chunks, out_ref, made, sent = refs[:-3], refs[-3], refs[-2], refs[-1]
-    tokens, at, copies = made.shape[0], 0, []
-    for chunk in chunks:
-        for first in range(0, chunk.shape[1], COLUMNS):
-            both = dot32(mix_ref[...], chunk[:, first : first + COLUMNS])
-            made[:, at : at + COLUMNS] = (both[:tokens] + both[tokens:]).astype(jnp.bfloat16)
-            place = pl.ds(at, COLUMNS)
-            copies.append(pltpu.make_async_copy(made.at[:, place], out_ref.at[:, place], sent.at[len(copies)]))
+    z, member = place_ref[0], place_ref[1]
+
+    def stepped(i):
+        return ((z - (i & 7)) & 7) * 8 + (member ^ lax.shift_right_logical(i, 3))
+
+    for t, number in enumerate((stepped, lambda i: i)):
+        tables = slot_table(ids, expert_count, slot_cap, number)
+        mix = (tables[0] * share[0:1] + tables[1] * share[1:2]).T
+        high = mix.astype(jnp.bfloat16)
+        out_ref[2 * t * tokens : (2 * t + 1) * tokens] = high
+        out_ref[(2 * t + 1) * tokens : (2 * t + 2) * tokens] = (mix - high.astype(jnp.float32)).astype(jnp.bfloat16)
+
+
+def early_kernel(mix_ref, *refs):
+    blocks, (out_ref, rows) = refs[:-2], refs[-2:]
+    tokens, count = out_ref.shape[0], blocks[0].shape[0]
+    for i, block in enumerate(blocks):
+        rows[i * count : (i + 1) * count, :] = block[...]
+    both = dot32(mix_ref[: 2 * tokens], rows[...])
+    out_ref[...] = (both[:tokens] + both[tokens:]).astype(jnp.bfloat16)
+
+
+def combine_kernel(mix_ref, early_ref, rows_ref, out_ref, made, sent):
+    tokens, at = early_ref.shape
+    copies = [pltpu.make_async_copy(early_ref, out_ref.at[:, pl.ds(0, at)], sent.at[0])]
+    copies[0].start()
+    for first in range(0, rows_ref.shape[1], COLUMNS):
+        both = dot32(mix_ref[2 * tokens :], rows_ref[:, first : first + COLUMNS])
+        made[:, first : first + COLUMNS] = (both[:tokens] + both[tokens:]).astype(jnp.bfloat16)
+        here, there = made.at[:, pl.ds(first, COLUMNS)], out_ref.at[:, pl.ds(at + first, COLUMNS)]
+        copies.append(pltpu.make_async_copy(here, there, sent.at[len(copies)]))
+        copies[-1].start()
+    for copy in copies:
+        copy.wait()
+
+
+def spread_kernel(place_ref, *refs):
+    planes, blocks, sems = refs[:8], refs[8:16], refs[16]
+    rows, copies = planes[0].shape[0] // 8, []
+    for k in range(8):
+        start = pl.multiple_of((place_ref[1] ^ k) * rows, rows)
+        for z in range(8):
+            here, there = planes[z].at[pl.ds(start, rows)], blocks[k].at[pl.ds(z * rows, rows)]
+            copies.append(pltpu.make_async_copy(here, there, sems.at[len(copies)]))
             copies[-1].start()
-            at += COLUMNS
     for copy in copies:
         copy.wait()
 
@@ -95,16 +122,23 @@
     depth, units = weights[0].shape
     half = depth // 2
     parts = [(i, pl.ds(s * half, half)) for shard in range(count) for s in (0, 1) for i in (2 * shard, 2 * shard + 1)]
-    copies = fetch([(weights[i].at[p], here.at[i, p]) for i, p in parts], sems)
-    for shard in range(count):
+    fetch([(weights[i].at[p], here.at[i, p]) for i, p in parts], sems)
+
+    def shard_of(shard, _):
         sums = [0.0, 0.0]
         for s in (0, 1):
+            part = pl.ds(s * half, half)
             for k in (0, 1):
-                copies[4 * shard + 2 * s + k].wait()
+                there = here.at[2 * shard + k, part]
+                pltpu.make_async_copy(there, there, sems.at[4 * shard + 2 * s + k]).wait()
             rows = rows_ref[:, s * half : (s + 1) * half]
-            sums = [total + dot32(rows, here[2 * shard + k, pl.ds(s * half, half)]) for k, total in enumerate(sums)]
+            sums = [total + dot32(rows, here[2 * shard + k, part]) for k, total in enumerate(sums)]
         gate, up = sums
-        out_ref[:, shard * units : (shard + 1) * units] = (gate / (1.0 + jnp.exp(-gate)) * up).astype(jnp.bfloat16)
+        columns = pl.ds(pl.multiple_of(shard * units, units), units)
+        out_ref[:, columns] = (gate / (1.0 + jnp.exp(-gate)) * up).astype(jnp.bfloat16)
+        return _
+
+    lax.fori_loop(0, count, shard_of, 0)
 
 
 def stack_kernel(*refs, widths):
@@ -118,31 +152,44 @@
         copy.wait()
 
 
-def down_kernel(near_ref, far_ref, stacked_ref, *refs):
-    pieces, (out_ref, far_weight, made, came, sent) = refs[:-5], refs[-5:]
+def down_kernel(place_ref, near_ref, far_ref, stacked_ref, *refs, planes):
+    pieces, outs, (far_weight, made, came, sent) = refs[:2], refs[2:-4], refs[-4:]
     at, pairs, copies = 0, [], []
     for piece in pieces:
         pairs.append((piece, far_weight.at[:, pl.ds(at, piece.shape[1])]))
         at += piece.shape[1]
     for copy in fetch(pairs, came):
         copy.wait()
-    for i in range(at // COLUMNS):
-        place = pl.ds(i * COLUMNS, COLUMNS)
+
+    def block(i, _):
+        place = pl.ds(pl.multiple_of(i * COLUMNS, COLUMNS), COLUMNS)
         total = dot32(near_ref[...], stacked_ref[:, place]) + dot32(far_ref[...], far_weight[:, place])
         made[:, place] = total.astype(jnp.bfloat16)
-        copies.append(pltpu.make_async_copy(made.at[:, place], out_ref.at[:, place], sent.at[i]))
-        copies[-1].start()
+        if not planes:
+            pltpu.make_async_copy(made.at[:, place], outs[0].at[:, place], sent.at[i]).start()
+        return _
+
+    lax.fori_loop(0, at // COLUMNS, block, 0)
+    for i in range(0 if planes else at // COLUMNS):
+        place = pl.ds(i * COLUMNS, COLUMNS)
+        copies.append(pltpu.make_async_copy(made.at[:, place], outs[0].at[:, place], sent.at[i]))
+    if planes:
+        rows = outs[0].shape[0]
+        starts = [pl.multiple_of(((place_ref[0] + d) & 7) * rows, rows) for d in range(8)]
+        copies = fetch([(made.at[pl.ds(s, rows)], out) for s, out in zip(starts, outs)], sent)
     for copy in copies:
         copy.wait()
 
 
-def on_core(kernel, shape, operands, mib, scratch=(), out=pltpu.VMEM, away=0):
-    count = len(operands) - away
+def on_core(kernel, shape, operands, mib, scratch=(), out=pltpu.VMEM, away=0, scalars=0, several=0):
+    count = len(operands) - away - scalars
+    space = [pltpu.SMEM] * scalars + [pltpu.VMEM] * count + [pltpu.HBM] * away
+    result, placed = jax.ShapeDtypeStruct(shape, jnp.bfloat16), pl.BlockSpec(memory_space=out)
     return pl.pallas_call(
         kernel,
-        out_shape=jax.ShapeDtypeStruct(shape, jnp.bfloat16),
-        in_specs=[pl.BlockSpec(memory_space=pltpu.VMEM)] * count + [pl.BlockSpec(memory_space=pltpu.HBM)] * away,
-        out_specs=pl.BlockSpec(memory_space=out),
+        out_shape=[result] * several if several else result,
+        in_specs=[pl.BlockSpec(memory_space=s) for s in space],
+        out_specs=[placed] * several if several else placed,
         scratch_shapes=list(scratch),
         compiler_params=pltpu.CompilerParams(vmem_limit_bytes=mib * MIB),
     )(*operands)
@@ -213,11 +260,14 @@
     arrived = lax.all_to_all(
         outgoing.reshape(expert_count, slot_cap, model_width), "ep", 0, 0, tiled=True
     ).reshape(slots, model_width)
+    ep = lax.axis_index("ep")
+    place = jnp.stack([ep // 8, ep % 8]).astype(jnp.int32)
     mix = on_core(
         lambda *refs: mix_kernel(*refs, expert_count=expert_count, slot_cap=slot_cap),
-        (2 * token_count, slots),
-        (ids_t, weight_t),
+        (4 * token_count, slots),
+        (place, ids_t, weight_t),
         8,
+        scalars=1,
     )
 
     tap_span = CONV - 1
@@ -251,8 +301,8 @@
     near = hidden(((gate, up), (gates[0], ups[0]), (gates[1], ups[1])))
     far = hidden(((gate_far, up_far),))
 
-    returned = []
-    for chunk in CHUNKS:
+    results = []
+    for i, chunk in enumerate(CHUNKS):
         widths = [PIECES[piece] for piece in chunk]
         width = sum(widths)
         sides = [d for piece in chunk for d in downs[piece][:3]]
@@ -267,13 +317,51 @@
         scratch = (
             pltpu.VMEM((units, width), jnp.bfloat16),
             pltpu.VMEM((slots, width), jnp.bfloat16),
-            pltpu.SemaphoreType.DMA((len(chunk),)),
-            pltpu.SemaphoreType.DMA((width // COLUMNS,)),
-        )
-        operands = (near, far, stacked, *[downs[piece][3] for piece in chunk])
-        result = on_core(down_kernel, (slots, width), operands, 12, scratch, pltpu.HBM, away=len(chunk))
-        back = lax.all_to_all(result.reshape(expert_count, slot_cap, width), "ep", 0, 0, tiled=True)
-        returned.append(back.reshape(slots, width))
+            pltpu.SemaphoreType.DMA((2,)),
+            pltpu.SemaphoreType.DMA((8,)),
+        )
+        results.append(
+            on_core(
+                lambda *refs, i=i: down_kernel(*refs, planes=i == 0),
+                (slots // 8, width) if i == 0 else (slots, width),
+                (place, near, far, stacked, *[downs[piece][3] for piece in chunk]),
+                12,
+                scratch,
+                pltpu.HBM,
+                away=2,
+                scalars=1,
+                several=8 if i == 0 else 0,
+            )
+        )
+
+    planes, last = results
+    width = last.shape[1]
+
+    def hop(value, target):
+        return lax.ppermute(value, "ep", [(p, target(p // 8, p % 8)) for p in range(expert_count)])
+
+    planes = [planes[0]] + [hop(planes[d], lambda z, m, d=d: (z + d) % 8 * 8 + m) for d in range(1, 8)]
+    blocks = on_core(
+        spread_kernel,
+        planes[0].shape,
+        (place, *planes),
+        4,
+        (pltpu.SemaphoreType.DMA((64,)),),
+        pltpu.HBM,
+        away=8,
+        scalars=1,
+        several=8,
+    )
+    blocks = [blocks[0]] + [hop(blocks[k], lambda z, m, k=k: z * 8 + (m ^ k)) for k in range(1, 8)]
+    early = on_core(
+        early_kernel,
+        (token_count, planes[0].shape[1]),
+        (mix, *blocks),
+        8,
+        (pltpu.VMEM((slots, planes[0].shape[1]), jnp.bfloat16),),
+    )
+    back = lax.all_to_all(last.reshape(expert_count, slot_cap, width), "ep", 0, 0, tiled=True)
+    back = back.reshape(slots, width)
 
     gated_sides = from_sides(gated)
     gated_far = from_opposite(*gated_sides)
@@ -286,11 +374,8 @@
         name="mixer",
     )(lax.axis_index("tp").reshape(1), gated, *gated_sides, *gated_far, mixer_weight)
 
-    scratch = (
-        pltpu.VMEM((token_count, model_width), jnp.bfloat16),
-        pltpu.SemaphoreType.DMA((model_width // COLUMNS,)),
-    )
-    experts_out = on_core(combine_kernel, (token_count, model_width), (mix, *returned), 8, scratch, pltpu.HBM)
+    scratch = (pltpu.VMEM((token_count, width), jnp.bfloat16), pltpu.SemaphoreType.DMA((1 + width // COLUMNS,)))
+    experts_out = on_core(combine_kernel, (token_count, model_width), (mix, early, back), 8, scratch, pltpu.HBM)
     return (mixer_out, experts_out)
 
 

time: 249 us -> 248 us (level)
  the two profiles are of different devices: /device:TPU:120 before, /device:TPU:2 now
where the time goes in v4:
time: 248 us; the launch traced here: 244 us
  waiting for transfers between devices  115 us (46%)
  starting transfers between devices  76.6 us (31%)
  Pallas kernels  27.3 us (11%)
  local copies, waits for them, and re-layouts  23.5 us (9%)
    ppermute x22, waiting for transfers between devices, turn(): return lax.ppermute(value, 'tp', pairs)  88.6 us
    ppermute x22, starting transfers between devices, turn(): return lax.ppermute(value, 'tp', pairs)  32.1 us
    pallas_call x11, Pallas kernels, on_core(): pl.pallas_call(kernel, out_shape=[result] * several if several else resul...  24.9 us
    ppermute x14, waiting for transfers between devices, hop(): lax.ppermute(value, 'ep', [(p, target(p // 8, p % 8)) for p in range(expe...  24 us
    unnamed x74, local copies, waits for them, and re-layouts  21.5 us
    ppermute x14, starting transfers between devices, hop(): lax.ppermute(value, 'ep', [(p, target(p // 8, p % 8)) for p in range(expe...  20 us
    all_to_all x1, starting transfers between devices, local(): lax.all_to_all(outgoing.reshape(expert_count, slot_cap, model_width), 'ep...  12.2 us
    all_to_all x1, starting transfers between devices, local(): lax.all_to_all(last.reshape(expert_count, slot_cap, width), 'ep', 0, 0, t...  10.5 us
  transfers between devices with their start and end apart: 39, of which 15 were waited for; matrix products, arithmetic and copies ran while one was open for 1% of the time, Pallas kernels for 10%

profile of v4, /device:TPU:2, one launch (start us, length us, event | category | flops | bytes accessed | tf_op | source)
XLA Modules:
  0.0 244.2 jit_solution(2562842165300607025)
XLA Ops:
  4.0 1.3 copy-done
  5.3 12.2 %all-to-all-start = ((bf16[64,8,2048]{2,1,0:T(8,128)(2,1)}), bf16[64,8,2048]{2,1,0:T(8,128)(2,1)S(1)}, u32[]{:S(2)}, u32[]{:S(2)}) async-start(bf16[64,8,2048]{2,1,0:T(8,128)(2,1)} %bitcast.18), calls=%async_computation | async-start | bytes 4194304 | tf_op jit(solution)/shard_map/all_to_all | solution.py:260
  17.5 1.7 collective-permute-start.5
  19.1 1.7 collective-permute-start.8
  20.8 2.0 fusion.7
  23.1 1.6 collective-permute-start.6
  24.7 1.7 collective-permute-start.7
  26.4 24.1 %collective-permute-done.31.refs_1_ = bf16[256,512]{1,0:T(8,128)(2,1)} collective-permute-done((bf16[256,512]{1,0:T(8,128)(2,1)S(1)}, bf16[256,512]{1,0:T(8,128)(2,1)}, u32[]{:S(2)}, u32[]{:S(2)}) %collective-permute-start.31) | collective-permute-done | bytes 262176 | tf_op jit(solution)/shard_map/ppermute | solution.py:20
  50.5 1.8 collective-permute-start.32
  53.2 3.0 %collective-permute-start.10 = (bf16[2048,256]{1,0:T(8,128)(2,1)}, bf16[2048,256]{1,0:T(8,128)(2,1)}, u32[]{:S(2)}, u32[]{:S(2)}) collective-permute-start(bf16[2048,256]{1,0:T(8,128)(2,1)} %collective-permute-done.8.refs_6_), channel_id=1, source_target_pairs={{0,3},{1,0},{2,1},{3,2},{4,7},{5,4},{6,5},{7,6},{8,11},{9,8},{10,9... | collective-permute-start | bytes 3145736 | tf_op jit(solution)/shard_map/ppermute | solution.py:20
  56.2 17.2 %collective-permute-done.32.refs_2_ = bf16[256,512]{1,0:T(8,128)(2,1)S(1)} collective-permute-done((bf16[256,512]{1,0:T(8,128)(2,1)S(1)}, bf16[256,512]{1,0:T(8,128)(2,1)S(1)}, u32[]{:S(2)}, u32[]{:S(2)}) %collective-permute-start.32) | collective-permute-done | bytes 262176 | tf_op jit(solution)/shard_map/ppermute | solution.py:20
  74.1 1.6 collective-permute-start.33
  75.7 24.4 %collective-permute-done.33.refs_4_ = bf16[256,512]{1,0:T(8,128)(2,1)S(1)} collective-permute-done((bf16[256,512]{1,0:T(8,128)(2,1)S(1)}, bf16[256,512]{1,0:T(8,128)(2,1)S(1)}, u32[]{:S(2)}, u32[]{:S(2)}) %collective-permute-start.33) | collective-permute-done | bytes 262176 | tf_op jit(solution)/shard_map/ppermute | solution.py:20
  100.9 1.7 collective-permute-start.34
  103.3 5.2 %collective-permute-done.34.refs_5_ = bf16[256,512]{1,0:T(8,128)(2,1)} collective-permute-done((bf16[256,512]{1,0:T(8,128)(2,1)S(1)}, bf16[256,512]{1,0:T(8,128)(2,1)}, u32[]{:S(2)}, u32[]{:S(2)}) %collective-permute-start.34) | collective-permute-done | bytes 262176 | tf_op jit(solution)/shard_map/ppermute | solution.py:20
  109.7 3.0 %collective-permute-start.36 = (bf16[256,512]{1,0:T(8,128)(2,1)}, bf16[256,512]{1,0:T(8,128)(2,1)}, u32[]{:S(2)}, u32[]{:S(2)}) collective-permute-start(bf16[256,512]{1,0:T(8,128)(2,1)} %collective-permute-done.34.refs_5_), channel_id=1, source_target_pairs={{0,3},{1,0},{2,1},{3,2},{4,7},{5,4},{6,5},{7,6},{8,11},{9,8},{10,9... | collective-permute-start | bytes 786440 | tf_op jit(solution)/shard_map/ppermute | solution.py:20
  122.5 4.5 %shard_map.133.refs_1_ = bf16[512,768]{1,0:T(8,128)(2,1)S(1)} custom-call(bf16[512,2048]{1,0:T(8,128)(2,1)S(1)} %bitcast.16, bf16[2048,256]{1,0:T(8,128)(2,1)S(1)} %bitcast.22, bf16[2048,256]{1,0:T(8,128)(2,1)S(1)} %bitcast.25, bf16[2048,256]{1,0:T(8,128)(2,1)} %collective-permute-done.5.refs_3_, bf16[2048,256]{1,0:T(8,128)(2,1)S(1)} %copy-done.13, ...), custom_call_target="tpu_custom_call" | custom-call | tf_op jit(solution)/shard_map/pallas_call | solution.py:188
  127.1 3.3 %collective-permute-start.12 = (bf16[256,512]{1,0:T(8,128)(2,1)}, bf16[256,512]{1,0:T(8,128)(2,1)}, u32[]{:S(2)}, u32[]{:S(2)}) collective-permute-start(bf16[256,512]{1,0:T(8,128)(2,1)} %get-tuple-element.37.refs_0_), channel_id=1, source_target_pairs={{0,3},{1,0},{2,1},{3,2},{4,7},{5,4},{6,5},{7,6},{8,11},{9,8},{10,9... | collective-permute-start | bytes 786440 | tf_op jit(solution)/shard_map/ppermute | solution.py:20
  130.4 2.8 %shard_map.134.refs_2_ = bf16[512,256]{1,0:T(8,128)(2,1)S(1)} custom-call(bf16[512,2048]{1,0:T(8,128)(2,1)S(1)} %bitcast.17, bf16[2048,256]{1,0:T(8,128)(2,1)} %collective-permute-done.9.refs_1_, bf16[2048,256]{1,0:T(8,128)(2,1)} %collective-permute-done.10.refs_2_), custom_call_target="tpu_custom_call" | custom-call | tf_op jit(solution)/shard_map/pallas_call | solution.py:188
  133.3 4.2 %shard_map.140 = bf16[512,1024]{1,0:T(8,128)(2,1)} custom-call(s32[2]{0:T(128)S(1)} %pad_add_fusion.refs_0_.place_ref, bf16[512,768]{1,0:T(8,128)(2,1)S(1)} %shard_map.133.refs_1_, bf16[512,256]{1,0:T(8,128)(2,1)S(1)} %shard_map.134.refs_2_, bf16[768,1024]{1,0:T(8,128)(2,1)S(1)} %copy-done.2, bf16[256,512]{1,0:T(8,128)(2,1)} %collective-permute-done.35.refs_4_, ...), custom_call_target="tpu_custom_call" | custom-call | tf_op jit(solution)/shard_map/pallas_call | solution.py:188
  137.6 10.5 %all-to-all-start.1 = ((bf16[64,8,1024]{2,1,0:T(8,128)(2,1)}), bf16[64,8,1024]{2,1,0:T(8,128)(2,1)S(1)}, u32[]{:S(2)}, u32[]{:S(2)}) async-start(bf16[64,8,1024]{2,1,0:T(8,128)(2,1)} %bitcast.14), calls=%async_computation.1 | async-start | bytes 2097152 | tf_op jit(solution)/shard_map/all_to_all | solution.py:363
  148.2 1.9 collective-permute-start
  150.1 3.0 %collective-permute-start.14 = (bf16[256,512]{1,0:T(8,128)(2,1)S(1)}, bf16[256,512]{1,0:T(8,128)(2,1)S(1)}, u32[]{:S(2)}, u32[]{:S(2)}) collective-permute-start(bf16[256,512]{1,0:T(8,128)(2,1)S(1)} %get-tuple-element.36.refs_3_), channel_id=1, source_target_pairs={{0,3},{1,0},{2,1},{3,2},{4,7},{5,4},{6,5},{7,6},{8,11},{9,8},{10,9... | collective-permute-start | bytes 786440 | tf_op jit(solution)/shard_map/ppermute | solution.py:20
  153.2 2.2 collective-permute-done
  155.9 3.2 %collective-permute-start.2 = (bf16[128,2048]{1,0:T(8,128)(2,1)S(1)}, bf16[128,2048]{1,0:T(8,128)(2,1)S(1)}, u32[]{:S(2)}, u32[]{:S(2)}) collective-permute-start(bf16[128,2048]{1,0:T(8,128)(2,1)S(1)} %fusion.5.own_ref), channel_id=1, source_target_pairs={{0,3},{1,0},{2,1},{3,2},{4,7},{5,4},{6,5},{7,6},{8,11},{9,8},{10,9... | collective-permute-start | bytes 1572872 | tf_op jit(solution)/shard_map/ppermute | solution.py:20
  159.5 3.7 %collective-permute-start.16 = (bf16[256,512]{1,0:T(8,128)(2,1)S(1)}, bf16[256,512]{1,0:T(8,128)(2,1)S(1)}, u32[]{:S(2)}, u32[]{:S(2)}) collective-permute-start(bf16[256,512]{1,0:T(8,128)(2,1)S(1)} %collective-permute-done.14.refs_5_), channel_id=1, source_target_pairs={{0,3},{1,0},{2,1},{3,2},{4,7},{5,4},{6,5},{7,6},{8,11},{9,8},{10,9... | collective-permute-start | bytes 786440 | tf_op jit(solution)/shard_map/ppermute | solution.py:20
  163.2 14.3 %collective-permute-done.13.refs_4_ = bf16[256,512]{1,0:T(8,128)(2,1)S(1)} collective-permute-done((bf16[256,512]{1,0:T(8,128)(2,1)S(1)}, bf16[256,512]{1,0:T(8,128)(2,1)S(1)}, u32[]{:S(2)}, u32[]{:S(2)}) %collective-permute-start.13) | collective-permute-done | bytes 262176 | tf_op jit(solution)/shard_map/ppermute | solution.py:20
  178.7 3.0 %collective-permute-done.15.refs_4_ = bf16[256,512]{1,0:T(8,128)(2,1)S(1)} collective-permute-done((bf16[256,512]{1,0:T(8,128)(2,1)}, bf16[256,512]{1,0:T(8,128)(2,1)S(1)}, u32[]{:S(2)}, u32[]{:S(2)}) %collective-permute-start.15) | collective-permute-done | bytes 262176 | tf_op jit(solution)/shard_map/ppermute | solution.py:20
  181.7 3.9 %shard_map.136 = (bf16[64,1024]{1,0:T(8,128)(2,1)S(1)}, bf16[64,1024]{1,0:T(8,128)(2,1)S(1)}, bf16[64,1024]{1,0:T(8,128)(2,1)S(1)}, bf16[64,1024]{1,0:T(8,128)(2...) custom-call(s32[2]{0:T(128)S(1)} %pad_add_fusion.refs_0_.place_ref, ...), custom_call_target="tpu_custom_call" | custom-call | tf_op jit(solution)/shard_map/pallas_call | solution.py:188
  185.6 1.5 collective-permute-start.17
  187.1 2.4 collective-permute-start.18
  189.5 2.8 %collective-permute-start.19 = (bf16[64,1024]{1,0:T(8,128)(2,1)S(1)}, bf16[64,1024]{1,0:T(8,128)(2,1)S(1)}, u32[]{:S(2)}, u32[]{:S(2)}) collective-permute-start(bf16[64,1024]{1,0:T(8,128)(2,1)S(1)} %get-tuple-element.21), channel_id=1, source_target_pairs={{0,96},{4,100},{8,104},{12,108},{16,112},{20,116},{24,120},{28,124... | collective-permute-start | bytes 393224 | tf_op jit(solution)/shard_map/ppermute | solution.py:341
  192.4 2.1 collective-permute-start.20
  195.5 2.9 %collective-permute-start.21 = (bf16[64,1024]{1,0:T(8,128)(2,1)S(1)}, bf16[64,1024]{1,0:T(8,128)(2,1)S(1)}, u32[]{:S(2)}, u32[]{:S(2)}) collective-permute-start(bf16[64,1024]{1,0:T(8,128)(2,1)S(1)} %get-tuple-element.23), channel_id=1, source_target_pairs={{0,160},{4,164},{8,168},{12,172},{16,176},{20,180},{24,184},{28,18... | collective-permute-start | bytes 393224 | tf_op jit(solution)/shard_map/ppermute | solution.py:341
  198.4 4.7 %collective-permute-done.18.refs_2_ = bf16[64,1024]{1,0:T(8,128)(2,1)S(1)} collective-permute-done((bf16[64,1024]{1,0:T(8,128)(2,1)S(1)}, bf16[64,1024]{1,0:T(8,128)(2,1)S(1)}, u32[]{:S(2)}, u32[]{:S(2)}) %collective-permute-start.18) | collective-permute-done | bytes 131104 | tf_op jit(solution)/shard_map/ppermute | solution.py:341
  203.9 6.2 %collective-permute-done.19.refs_3_ = bf16[64,1024]{1,0:T(8,128)(2,1)S(1)} collective-permute-done((bf16[64,1024]{1,0:T(8,128)(2,1)S(1)}, bf16[64,1024]{1,0:T(8,128)(2,1)S(1)}, u32[]{:S(2)}, u32[]{:S(2)}) %collective-permute-start.19) | collective-permute-done | bytes 131104 | tf_op jit(solution)/shard_map/ppermute | solution.py:341
  210.2 3.1 %collective-permute-done.21.refs_5_ = bf16[64,1024]{1,0:T(8,128)(2,1)S(1)} collective-permute-done((bf16[64,1024]{1,0:T(8,128)(2,1)S(1)}, bf16[64,1024]{1,0:T(8,128)(2,1)S(1)}, u32[]{:S(2)}, u32[]{:S(2)}) %collective-permute-start.21) | collective-permute-done | bytes 131104 | tf_op jit(solution)/shard_map/ppermute | solution.py:341
  213.3 2.1 collective-permute-done.22.refs_6_
  215.4 2.5 %collective-permute-done.23.refs_7_ = bf16[64,1024]{1,0:T(8,128)(2,1)S(1)} collective-permute-done((bf16[64,1024]{1,0:T(8,128)(2,1)S(1)}, bf16[64,1024]{1,0:T(8,128)(2,1)S(1)}, u32[]{:S(2)}, u32[]{:S(2)}) %collective-permute-start.23) | collective-permute-done | bytes 131104 | tf_op jit(solution)/shard_map/ppermute | solution.py:341
  217.8 2.5 %shard_map.137 = (bf16[64,1024]{1,0:T(8,128)(2,1)S(1)}, bf16[64,1024]{1,0:T(8,128)(2,1)S(1)}, bf16[64,1024]{1,0:T(8,128)(2,1)S(1)}, bf16[64,1024]{1,0:T(8,128)(2...) custom-call(s32[2]{0:T(128)S(1)} %pad_add_fusion.refs_0_.place_ref, ...), custom_call_target="tpu_custom_call" | custom-call | tf_op jit(solution)/shard_map/pallas_call | solution.py:188
  220.4 2.3 collective-permute-start.25
  222.7 2.2 collective-permute-start.27
  227.1 1.3 collective-permute-start.29
  230.8 1.6 copy-done.3
  233.3 2.5 %mixer.1 = bf16[512,512]{1,0:T(8,128)(2,1)} custom-call(s32[1]{0:T(128)} %bitcast.place_ref, bf16[128,2048]{1,0:T(8,128)(2,1)S(1)} %fusion.5.own_ref, bf16[128,2048]{1,0:T(8,128)(2,1)S(1)} %copy-done.5, bf16[128,2048]{1,0:T(8,128)(2,1)S(1)} %copy-done.7, bf16[64,2048]{1,0:T(8,128)(2,1)S(1)} %collective-permute-done.3.first_ref, ...), custom_call_target="tpu_custom_call" | custom-call | tf_op jit(solution)/shard_map/mixer/pallas_call | solution.py:368
  235.8 3.0 %collective-permute-done.29.refs_6_ = bf16[64,1024]{1,0:T(8,128)(2,1)} collective-permute-done((bf16[64,1024]{1,0:T(8,128)(2,1)}, bf16[64,1024]{1,0:T(8,128)(2,1)}, u32[]{:S(2)}, u32[]{:S(2)}) %collective-permute-start.29) | collective-permute-done | bytes 131104 | tf_op jit(solution)/shard_map/ppermute | solution.py:341
  238.8 2.5 %collective-permute-done.30.refs_7_ = bf16[64,1024]{1,0:T(8,128)(2,1)} collective-permute-done((bf16[64,1024]{1,0:T(8,128)(2,1)}, bf16[64,1024]{1,0:T(8,128)(2,1)}, u32[]{:S(2)}, u32[]{:S(2)}) %collective-permute-start.30) | collective-permute-done | bytes 131104 | tf_op jit(solution)/shard_map/ppermute | solution.py:341
  241.2 1.6 shard_map.138.early_ref
  (124 shorter events, 28.5 us)
Async XLA Ops:
  5.3 12.2 %copy-start.8 = (bf16[1,2048,256]{2,1,0:T(8,128)(2,1)S(1)}, bf16[1,2048,256]{2,1,0:T(8,128)(2,1)}, u32[]{:S(2)}) copy-start(bf16[1,2048,256]{2,1,0:T(8,128)(2,1)} %param.19) | copy-start | bytes 3145732
  5.3 113.6 %all-to-all-start = ((bf16[64,8,2048]{2,1,0:T(8,128)(2,1)}), bf16[64,8,2048]{2,1,0:T(8,128)(2,1)S(1)}, u32[]{:S(2)}, u32[]{:S(2)}) async-start(bf16[64,8,2048]{2,1,0:T(8,128)(2,1)} %bitcast.18), calls=%async_computation | async-start | bytes 4194304 | tf_op jit(solution)/shard_map/all_to_all | solution.py:260
  17.5 35.5 %collective-permute-start.5 = (bf16[2048,256]{1,0:T(8,128)(2,1)S(1)}, bf16[2048,256]{1,0:T(8,128)(2,1)}, u32[]{:S(2)}, u32[]{:S(2)}) collective-permute-start(bf16[2048,256]{1,0:T(8,128)(2,1)S(1)} %bitcast.20), channel_id=1, source_target_pairs={{0,1},{1,2},{2,3},{3,0},{4,5},{5,6},{6,7},{7,4},{8,9},{9,10},{10,1... | collective-permute-start | bytes 3145736 | tf_op jit(solution)/shard_map/ppermute | solution.py:20
  19.1 34.1 %collective-permute-start.8 = (bf16[2048,256]{1,0:T(8,128)(2,1)}, bf16[2048,256]{1,0:T(8,128)(2,1)}, u32[]{:S(2)}, u32[]{:S(2)}) collective-permute-start(bf16[2048,256]{1,0:T(8,128)(2,1)} %bitcast.23), channel_id=1, source_target_pairs={{0,3},{1,0},{2,1},{3,2},{4,7},{5,4},{6,5},{7,6},{8,11},{9,8},{10,9... | collective-permute-start | bytes 3145736 | tf_op jit(solution)/shard_map/ppermute | solution.py:20
  22.8 27.7 %collective-permute-start.31 = (bf16[256,512]{1,0:T(8,128)(2,1)S(1)}, bf16[256,512]{1,0:T(8,128)(2,1)}, u32[]{:S(2)}, u32[]{:S(2)}) collective-permute-start(bf16[256,512]{1,0:T(8,128)(2,1)S(1)} %get-tuple-element.35.refs_0_), channel_id=1, source_target_pairs={{0,1},{1,2},{2,3},{3,0},{4,5},{5,6},{6,7},{7,4},{8,9},{9,10},{10,1... | collective-permute-start | bytes 786440 | tf_op jit(solution)/shard_map/ppermute | solution.py:20
  23.1 85.6 %collective-permute-start.6 = (bf16[2048,256]{1,0:T(8,128)(2,1)S(1)}, bf16[2048,256]{1,0:T(8,128)(2,1)S(1)}, u32[]{:S(2)}, u32[]{:S(2)}) collective-permute-start(bf16[2048,256]{1,0:T(8,128)(2,1)S(1)} %bitcast.24), channel_id=1, source_target_pairs={{0,1},{1,2},{2,3},{3,0},{4,5},{5,6},{6,7},{7,4},{8,9},{9,10},{10,1... | collective-permute-start | bytes 3145736 | tf_op jit(solution)/shard_map/ppermute | solution.py:20
  24.7 94.2 %collective-permute-start.7 = (bf16[2048,256]{1,0:T(8,128)(2,1)S(1)}, bf16[2048,256]{1,0:T(8,128)(2,1)}, u32[]{:S(2)}, u32[]{:S(2)}) collective-permute-start(bf16[2048,256]{1,0:T(8,128)(2,1)S(1)} %bitcast.21), channel_id=1, source_target_pairs={{0,3},{1,0},{2,1},{3,2},{4,7},{5,4},{6,5},{7,6},{8,11},{9,8},{10,9... | collective-permute-start | bytes 3145736 | tf_op jit(solution)/shard_map/ppermute | solution.py:20
  50.5 22.9 %collective-permute-start.32 = (bf16[256,512]{1,0:T(8,128)(2,1)S(1)}, bf16[256,512]{1,0:T(8,128)(2,1)S(1)}, u32[]{:S(2)}, u32[]{:S(2)}) collective-permute-start(bf16[256,512]{1,0:T(8,128)(2,1)S(1)} %get-tuple-element.35.refs_0_), channel_id=1, source_target_pairs={{0,3},{1,0},{2,1},{3,2},{4,7},{5,4},{6,5},{7,6},{8,11},{9,8},{10,9... | collective-permute-start | bytes 786440 | tf_op jit(solution)/shard_map/ppermute | solution.py:20
  53.0 74.1 %collective-permute-start.9 = (bf16[2048,256]{1,0:T(8,128)(2,1)}, bf16[2048,256]{1,0:T(8,128)(2,1)}, u32[]{:S(2)}, u32[]{:S(2)}) collective-permute-start(bf16[2048,256]{1,0:T(8,128)(2,1)} %collective-permute-done.5.refs_3_), channel_id=1, source_target_pairs={{0,1},{1,2},{2,3},{3,0},{4,5},{5,6},{6,7},{7,4},{8,9},{9,10},{10,1... | collective-permute-start | bytes 3145736 | tf_op jit(solution)/shard_map/ppermute | solution.py:20
  53.2 77.2 %collective-permute-start.10 = (bf16[2048,256]{1,0:T(8,128)(2,1)}, bf16[2048,256]{1,0:T(8,128)(2,1)}, u32[]{:S(2)}, u32[]{:S(2)}) collective-permute-start(bf16[2048,256]{1,0:T(8,128)(2,1)} %collective-permute-done.8.refs_6_), channel_id=1, source_target_pairs={{0,3},{1,0},{2,1},{3,2},{4,7},{5,4},{6,5},{7,6},{8,11},{9,8},{10,9... | collective-permute-start | bytes 3145736 | tf_op jit(solution)/shard_map/ppermute | solution.py:20
  74.1 26.0 %collective-permute-start.33 = (bf16[256,512]{1,0:T(8,128)(2,1)S(1)}, bf16[256,512]{1,0:T(8,128)(2,1)S(1)}, u32[]{:S(2)}, u32[]{:S(2)}) collective-permute-start(bf16[256,512]{1,0:T(8,128)(2,1)S(1)} %get-tuple-element.34.refs_3_), channel_id=1, source_target_pairs={{0,1},{1,2},{2,3},{3,0},{4,5},{5,6},{6,7},{7,4},{8,9},{9,10},{10,1... | collective-permute-start | bytes 786440 | tf_op jit(solution)/shard_map/ppermute | solution.py:20
  100.9 7.6 %collective-permute-start.34 = (bf16[256,512]{1,0:T(8,128)(2,1)S(1)}, bf16[256,512]{1,0:T(8,128)(2,1)}, u32[]{:S(2)}, u32[]{:S(2)}) collective-permute-start(bf16[256,512]{1,0:T(8,128)(2,1)S(1)} %get-tuple-element.34.refs_3_), channel_id=1, source_target_pairs={{0,3},{1,0},{2,1},{3,2},{4,7},{5,4},{6,5},{7,6},{8,11},{9,8},{10,9... | collective-permute-start | bytes 786440 | tf_op jit(solution)/shard_map/ppermute | solution.py:20
  108.5 24.8 %collective-permute-start.35 = (bf16[256,512]{1,0:T(8,128)(2,1)}, bf16[256,512]{1,0:T(8,128)(2,1)}, u32[]{:S(2)}, u32[]{:S(2)}) collective-permute-start(bf16[256,512]{1,0:T(8,128)(2,1)} %collective-permute-done.31.refs_1_), channel_id=1, source_target_pairs={{0,1},{1,2},{2,3},{3,0},{4,5},{5,6},{6,7},{7,4},{8,9},{9,10},{10,1... | collective-permute-start | bytes 786440 | tf_op jit(solution)/shard_map/ppermute | solution.py:20
  109.7 23.6 %collective-permute-start.36 = (bf16[256,512]{1,0:T(8,128)(2,1)}, bf16[256,512]{1,0:T(8,128)(2,1)}, u32[]{:S(2)}, u32[]{:S(2)}) collective-permute-start(bf16[256,512]{1,0:T(8,128)(2,1)} %collective-permute-done.34.refs_5_), channel_id=1, source_target_pairs={{0,3},{1,0},{2,1},{3,2},{4,7},{5,4},{6,5},{7,6},{8,11},{9,8},{10,9... | collective-permute-start | bytes 786440 | tf_op jit(solution)/shard_map/ppermute | solution.py:20
  118.9 40.3 %collective-permute-start.11 = (bf16[256,512]{1,0:T(8,128)(2,1)}, bf16[256,512]{1,0:T(8,128)(2,1)}, u32[]{:S(2)}, u32[]{:S(2)}) collective-permute-start(bf16[256,512]{1,0:T(8,128)(2,1)} %get-tuple-element.37.refs_0_), channel_id=1, source_target_pairs={{0,1},{1,2},{2,3},{3,0},{4,5},{5,6},{6,7},{7,4},{8,9},{9,10},{10,1... | collective-permute-start | bytes 786440 | tf_op jit(solution)/shard_map/ppermute | solution.py:20
  127.1 32.0 %collective-permute-start.12 = (bf16[256,512]{1,0:T(8,128)(2,1)}, bf16[256,512]{1,0:T(8,128)(2,1)}, u32[]{:S(2)}, u32[]{:S(2)}) collective-permute-start(bf16[256,512]{1,0:T(8,128)(2,1)} %get-tuple-element.37.refs_0_), channel_id=1, source_target_pairs={{0,3},{1,0},{2,1},{3,2},{4,7},{5,4},{6,5},{7,6},{8,11},{9,8},{10,9... | collective-permute-start | bytes 786440 | tf_op jit(solution)/shard_map/ppermute | solution.py:20
  137.5 10.5 %copy-start.33 = (bf16[128,2048]{1,0:T(8,128)(2,1)S(1)}, bf16[128,2048]{1,0:T(8,128)(2,1)}, u32[]{:S(2)}) copy-start(bf16[128,2048]{1,0:T(8,128)(2,1)} %param.14) | copy-start | bytes 1572868
  137.5 10.5 %copy-start.34 = (bf16[128,2048]{1,0:T(8,128)(2,1)S(1)}, bf16[128,2048]{1,0:T(8,128)(2,1)}, u32[]{:S(2)}) copy-start(bf16[128,2048]{1,0:T(8,128)(2,1)} %param.13) | copy-start | bytes 1572868
  137.6 105.3 %all-to-all-start.1 = ((bf16[64,8,1024]{2,1,0:T(8,128)(2,1)}), bf16[64,8,1024]{2,1,0:T(8,128)(2,1)S(1)}, u32[]{:S(2)}, u32[]{:S(2)}) async-start(bf16[64,8,1024]{2,1,0:T(8,128)(2,1)} %bitcast.14), calls=%async_computation.1 | async-start | bytes 2097152 | tf_op jit(solution)/shard_map/all_to_all | solution.py:363
  148.2 7.2 %collective-permute-start = (f32[2,2048]{1,0:T(2,128)S(1)}, f32[2,2048]{1,0:T(2,128)S(1)}, u32[]{:S(2)}, u32[]{:S(2)}) collective-permute-start(f32[2,2048]{1,0:T(2,128)S(1)} %slice.48), channel_id=1, source_target_pairs={{0,1},{1,2},{2,3},{3,4},{4,5},{5,6},{6,7},{7,8},{8,9},{9,10},{10,1... | collective-permute-start | bytes 49160 | tf_op jit(solution)/shard_map/ppermute | solution.py:276
  150.1 9.4 %collective-permute-start.14 = (bf16[256,512]{1,0:T(8,128)(2,1)S(1)}, bf16[256,512]{1,0:T(8,128)(2,1)S(1)}, u32[]{:S(2)}, u32[]{:S(2)}) collective-permute-start(bf16[256,512]{1,0:T(8,128)(2,1)S(1)} %get-tuple-element.36.refs_3_), channel_id=1, source_target_pairs={{0,3},{1,0},{2,1},{3,2},{4,7},{5,4},{6,5},{7,6},{8,11},{9,8},{10,9... | collective-permute-start | bytes 786440 | tf_op jit(solution)/shard_map/ppermute | solution.py:20
  155.8 36.6 %collective-permute-start.1 = (bf16[128,2048]{1,0:T(8,128)(2,1)S(1)}, bf16[128,2048]{1,0:T(8,128)(2,1)S(1)}, u32[]{:S(2)}, u32[]{:S(2)}) collective-permute-start(bf16[128,2048]{1,0:T(8,128)(2,1)S(1)} %fusion.5.own_ref), channel_id=1, source_target_pairs={{0,1},{1,2},{2,3},{3,0},{4,5},{5,6},{6,7},{7,4},{8,9},{9,10},{10,1... | collective-permute-start | bytes 1572872 | tf_op jit(solution)/shard_map/ppermute | solution.py:20
  155.9 38.7 %collective-permute-start.2 = (bf16[128,2048]{1,0:T(8,128)(2,1)S(1)}, bf16[128,2048]{1,0:T(8,128)(2,1)S(1)}, u32[]{:S(2)}, u32[]{:S(2)}) collective-permute-start(bf16[128,2048]{1,0:T(8,128)(2,1)S(1)} %fusion.5.own_ref), channel_id=1, source_target_pairs={{0,3},{1,0},{2,1},{3,2},{4,7},{5,4},{6,5},{7,6},{8,11},{9,8},{10,9... | collective-permute-start | bytes 1572872 | tf_op jit(solution)/shard_map/ppermute | solution.py:20
  159.1 18.4 %collective-permute-start.13 = (bf16[256,512]{1,0:T(8,128)(2,1)S(1)}, bf16[256,512]{1,0:T(8,128)(2,1)S(1)}, u32[]{:S(2)}, u32[]{:S(2)}) collective-permute-start(bf16[256,512]{1,0:T(8,128)(2,1)S(1)} %get-tuple-element.36.refs_3_), channel_id=1, source_target_pairs={{0,1},{1,2},{2,3},{3,0},{4,5},{5,6},{6,7},{7,4},{8,9},{9,10},{10,1... | collective-permute-start | bytes 786440 | tf_op jit(solution)/shard_map/ppermute | solution.py:20
  159.1 22.5 %collective-permute-start.15 = (bf16[256,512]{1,0:T(8,128)(2,1)}, bf16[256,512]{1,0:T(8,128)(2,1)S(1)}, u32[]{:S(2)}, u32[]{:S(2)}) collective-permute-start(bf16[256,512]{1,0:T(8,128)(2,1)} %collective-permute-done.11.refs_1_), channel_id=1, source_target_pairs={{0,1},{1,2},{2,3},{3,0},{4,5},{5,6},{6,7},{7,4},{8,9},{9,10},{10,1... | collective-permute-start | bytes 786440 | tf_op jit(solution)/shard_map/ppermute | solution.py:20
  159.5 22.1 %collective-permute-start.16 = (bf16[256,512]{1,0:T(8,128)(2,1)S(1)}, bf16[256,512]{1,0:T(8,128)(2,1)S(1)}, u32[]{:S(2)}, u32[]{:S(2)}) collective-permute-start(bf16[256,512]{1,0:T(8,128)(2,1)S(1)} %collective-permute-done.14.refs_5_), channel_id=1, source_target_pairs={{0,3},{1,0},{2,1},{3,2},{4,7},{5,4},{6,5},{7,6},{8,11},{9,8},{10,9... | collective-permute-start | bytes 786440 | tf_op jit(solution)/shard_map/ppermute | solution.py:20
  185.5 44.2 %copy-start.31 = (s32[128,2]{0,1:T(2,128)S(1)}, s32[128,2]{0,1:T(2,128)}, u32[]{:S(2)}) copy-start(s32[128,2]{0,1:T(2,128)} %param.22) | copy-start | bytes 3076
  185.6 44.2 %copy-start.32 = (f32[128,2]{0,1:T(2,128)S(1)}, f32[128,2]{0,1:T(2,128)}, u32[]{:S(2)}) copy-start(f32[128,2]{0,1:T(2,128)} %param.23) | copy-start | bytes 3076
  185.6 9.9 %collective-permute-start.17 = (bf16[64,1024]{1,0:T(8,128)(2,1)S(1)}, bf16[64,1024]{1,0:T(8,128)(2,1)S(1)}, u32[]{:S(2)}, u32[]{:S(2)}) collective-permute-start(bf16[64,1024]{1,0:T(8,128)(2,1)S(1)} %get-tuple-element.19), channel_id=1, source_target_pairs={{0,32},{4,36},{8,40},{12,44},{16,48},{20,52},{24,56},{28,60},{32,6... | collective-permute-start | bytes 393224 | tf_op jit(solution)/shard_map/ppermute | solution.py:341
  187.1 16.0 %collective-permute-start.18 = (bf16[64,1024]{1,0:T(8,128)(2,1)S(1)}, bf16[64,1024]{1,0:T(8,128)(2,1)S(1)}, u32[]{:S(2)}, u32[]{:S(2)}) collective-permute-start(bf16[64,1024]{1,0:T(8,128)(2,1)S(1)} %get-tuple-element.20), channel_id=1, source_target_pairs={{0,64},{4,68},{8,72},{12,76},{16,80},{20,84},{24,88},{28,92},{32,9... | collective-permute-start | bytes 393224 | tf_op jit(solution)/shard_map/ppermute | solution.py:341
  189.5 20.5 %collective-permute-start.19 = (bf16[64,1024]{1,0:T(8,128)(2,1)S(1)}, bf16[64,1024]{1,0:T(8,128)(2,1)S(1)}, u32[]{:S(2)}, u32[]{:S(2)}) collective-permute-start(bf16[64,1024]{1,0:T(8,128)(2,1)S(1)} %get-tuple-element.21), channel_id=1, source_target_pairs={{0,96},{4,100},{8,104},{12,108},{16,112},{20,116},{24,120},{28,124... | collective-permute-start | bytes 393224 | tf_op jit(solution)/shard_map/ppermute | solution.py:341
  192.4 17.7 %collective-permute-start.20 = (bf16[64,1024]{1,0:T(8,128)(2,1)S(1)}, bf16[64,1024]{1,0:T(8,128)(2,1)S(1)}, u32[]{:S(2)}, u32[]{:S(2)}) collective-permute-start(bf16[64,1024]{1,0:T(8,128)(2,1)S(1)} %get-tuple-element.22), channel_id=1, source_target_pairs={{0,128},{4,132},{8,136},{12,140},{16,144},{20,148},{24,152},{28,15... | collective-permute-start | bytes 393224 | tf_op jit(solution)/shard_map/ppermute | solution.py:341
  194.6 28.2 %collective-permute-start.3 = (bf16[64,2048]{1,0:T(8,128)(2,1)S(1)}, bf16[64,2048]{1,0:T(8,128)(2,1)S(1)}, u32[]{:S(2)}, u32[]{:S(2)}) collective-permute-start(bf16[64,2048]{1,0:T(8,128)(2,1)S(1)} %slice.54), channel_id=1, source_target_pairs={{0,1},{1,2},{2,3},{3,0},{4,5},{5,6},{6,7},{7,4},{8,9},{9,10},{10,1... | collective-permute-start | bytes 786440 | tf_op jit(solution)/shard_map/ppermute | solution.py:20
  194.6 36.1 %copy-start.5 = (bf16[128,2048]{1,0:T(8,128)(2,1)S(1)}, bf16[128,2048]{1,0:T(8,128)(2,1)}, u32[]{:S(2)}) copy-start(bf16[128,2048]{1,0:T(8,128)(2,1)} %copy-done.4) | copy-start | bytes 1572868
  195.5 35.2 %copy-start.7 = (bf16[128,2048]{1,0:T(8,128)(2,1)S(1)}, bf16[128,2048]{1,0:T(8,128)(2,1)}, u32[]{:S(2)}) copy-start(bf16[128,2048]{1,0:T(8,128)(2,1)} %copy-done.6) | copy-start | bytes 1572868
  195.5 17.8 %collective-permute-start.21 = (bf16[64,1024]{1,0:T(8,128)(2,1)S(1)}, bf16[64,1024]{1,0:T(8,128)(2,1)S(1)}, u32[]{:S(2)}, u32[]{:S(2)}) collective-permute-start(bf16[64,1024]{1,0:T(8,128)(2,1)S(1)} %get-tuple-element.23), channel_id=1, source_target_pairs={{0,160},{4,164},{8,168},{12,172},{16,176},{20,180},{24,184},{28,18... | collective-permute-start | bytes 393224 | tf_op jit(solution)/shard_map/ppermute | solution.py:341
  203.2 12.2 %collective-permute-start.22 = (bf16[64,1024]{1,0:T(8,128)(2,1)S(1)}, bf16[64,1024]{1,0:T(8,128)(2,1)S(1)}, u32[]{:S(2)}, u32[]{:S(2)}) collective-permute-start(bf16[64,1024]{1,0:T(8,128)(2,1)S(1)} %get-tuple-element.24), channel_id=1, source_target_pairs={{0,192},{4,196},{8,200},{12,204},{16,208},{20,212},{24,216},{28,22... | collective-permute-start | bytes 393224 | tf_op jit(solution)/shard_map/ppermute | solution.py:341
  210.0 7.8 %collective-permute-start.23 = (bf16[64,1024]{1,0:T(8,128)(2,1)S(1)}, bf16[64,1024]{1,0:T(8,128)(2,1)S(1)}, u32[]{:S(2)}, u32[]{:S(2)}) collective-permute-start(bf16[64,1024]{1,0:T(8,128)(2,1)S(1)} %get-tuple-element.25), channel_id=1, source_target_pairs={{0,224},{4,228},{8,232},{12,236},{16,240},{20,244},{24,248},{28,25... | collective-permute-start | bytes 393224 | tf_op jit(solution)/shard_map/ppermute | solution.py:341
  210.0 14.9 %collective-permute-start.4 = (bf16[64,2048]{1,0:T(8,128)(2,1)S(1)}, bf16[64,2048]{1,0:T(8,128)(2,1)S(1)}, u32[]{:S(2)}, u32[]{:S(2)}) collective-permute-start(bf16[64,2048]{1,0:T(8,128)(2,1)S(1)} %slice.55), channel_id=1, source_target_pairs={{0,3},{1,0},{2,1},{3,2},{4,7},{5,4},{6,5},{7,6},{8,11},{9,8},{10,9... | collective-permute-start | bytes 786440 | tf_op jit(solution)/shard_map/ppermute | solution.py:20
  220.3 6.2 %collective-permute-start.24 = (bf16[64,1024]{1,0:T(8,128)(2,1)S(1)}, bf16[64,1024]{1,0:T(8,128)(2,1)S(1)}, u32[]{:S(2)}, u32[]{:S(2)}) collective-permute-start(bf16[64,1024]{1,0:T(8,128)(2,1)S(1)} %get-tuple-element.27), channel_id=1, source_target_pairs={{0,4},{4,0},{8,12},{12,8},{16,20},{20,16},{24,28},{28,24},{32,36},... | collective-permute-start | bytes 393224 | tf_op jit(solution)/shard_map/ppermute | solution.py:341
  220.4 8.0 %collective-permute-start.25 = (bf16[64,1024]{1,0:T(8,128)(2,1)S(1)}, bf16[64,1024]{1,0:T(8,128)(2,1)S(1)}, u32[]{:S(2)}, u32[]{:S(2)}) collective-permute-start(bf16[64,1024]{1,0:T(8,128)(2,1)S(1)} %get-tuple-element.28), channel_id=1, source_target_pairs={{0,8},{4,12},{8,0},{12,4},{16,24},{20,28},{24,16},{28,20},{32,40},... | collective-permute-start | bytes 393224 | tf_op jit(solution)/shard_map/ppermute | solution.py:341
  222.7 13.1 %collective-permute-start.26 = (bf16[64,1024]{1,0:T(8,128)(2,1)}, bf16[64,1024]{1,0:T(8,128)(2,1)}, u32[]{:S(2)}, u32[]{:S(2)}) collective-permute-start(bf16[64,1024]{1,0:T(8,128)(2,1)} %get-tuple-element.29), channel_id=1, source_target_pairs={{0,12},{4,8},{8,4},{12,0},{16,28},{20,24},{24,20},{28,16},{32,44},... | collective-permute-start | bytes 393224 | tf_op jit(solution)/shard_map/ppermute | solution.py:341
  222.7 13.0 %collective-permute-start.27 = (bf16[64,1024]{1,0:T(8,128)(2,1)}, bf16[64,1024]{1,0:T(8,128)(2,1)}, u32[]{:S(2)}, u32[]{:S(2)}) collective-permute-start(bf16[64,1024]{1,0:T(8,128)(2,1)} %get-tuple-element.30), channel_id=1, source_target_pairs={{0,16},{4,20},{8,24},{12,28},{16,0},{20,4},{24,8},{28,12},{32,48},... | collective-permute-start | bytes 393224 | tf_op jit(solution)/shard_map/ppermute | solution.py:341
  225.7 10.1 %collective-permute-start.28 = (bf16[64,1024]{1,0:T(8,128)(2,1)}, bf16[64,1024]{1,0:T(8,128)(2,1)}, u32[]{:S(2)}, u32[]{:S(2)}) collective-permute-start(bf16[64,1024]{1,0:T(8,128)(2,1)} %get-tuple-element.31), channel_id=1, source_target_pairs={{0,20},{4,16},{8,28},{12,24},{16,4},{20,0},{24,12},{28,8},{32,52},... | collective-permute-start | bytes 393224 | tf_op jit(solution)/shard_map/ppermute | solution.py:341
  227.1 11.6 %collective-permute-start.29 = (bf16[64,1024]{1,0:T(8,128)(2,1)}, bf16[64,1024]{1,0:T(8,128)(2,1)}, u32[]{:S(2)}, u32[]{:S(2)}) collective-permute-start(bf16[64,1024]{1,0:T(8,128)(2,1)} %get-tuple-element.32), channel_id=1, source_target_pairs={{0,24},{4,28},{8,16},{12,20},{16,8},{20,12},{24,0},{28,4},{32,56},... | collective-permute-start | bytes 393224 | tf_op jit(solution)/shard_map/ppermute | solution.py:341
  229.1 12.1 %collective-permute-start.30 = (bf16[64,1024]{1,0:T(8,128)(2,1)}, bf16[64,1024]{1,0:T(8,128)(2,1)}, u32[]{:S(2)}, u32[]{:S(2)}) collective-permute-start(bf16[64,1024]{1,0:T(8,128)(2,1)} %get-tuple-element.33), channel_id=1, source_target_pairs={{0,28},{4,24},{8,20},{12,16},{16,12},{20,8},{24,4},{28,0},{32,60},... | collective-permute-start | bytes 393224 | tf_op jit(solution)/shard_map/ppermute | solution.py:341
  233.3 7.9 %copy-start.26 = (bf16[64,1024]{1,0:T(8,128)(2,1)S(1)}, bf16[64,1024]{1,0:T(8,128)(2,1)}, u32[]{:S(2)}) copy-start(bf16[64,1024]{1,0:T(8,128)(2,1)} %copy-done.25) | copy-start | bytes 393220
  233.3 7.9 %copy-start.28 = (bf16[64,1024]{1,0:T(8,128)(2,1)S(1)}, bf16[64,1024]{1,0:T(8,128)(2,1)}, u32[]{:S(2)}) copy-start(bf16[64,1024]{1,0:T(8,128)(2,1)} %copy-done.27) | copy-start | bytes 393220
  (28 other events, 48.0 us)

commit v5 on v3

--- a/solution.py
+++ b/solution.py
@@ -12,6 +12,7 @@
 CHUNKS = ((0, 1), (2, 3))
 COLUMNS = 256
 MIB = 1 << 20
+DOWN_MIB = 12
 
 
 def turn(value, steps):
@@ -95,52 +96,72 @@
     depth, units = weights[0].shape
     half = depth // 2
     parts = [(i, pl.ds(s * half, half)) for shard in range(count) for s in (0, 1) for i in (2 * shard, 2 * shard + 1)]
-    copies = fetch([(weights[i].at[p], here.at[i, p]) for i, p in parts], sems)
-    for shard in range(count):
+    fetch([(weights[i].at[p], here.at[i, p]) for i, p in parts], sems)
+
+    def shard_of(shard, _):
         sums = [0.0, 0.0]
         for s in (0, 1):
+            part = pl.ds(s * half, half)
             for k in (0, 1):
-                copies[4 * shard + 2 * s + k].wait()
+                there = here.at[2 * shard + k, part]
+                pltpu.make_async_copy(there, there, sems.at[4 * shard + 2 * s + k]).wait()
             rows = rows_ref[:, s * half : (s + 1) * half]
-            sums = [total + dot32(rows, here[2 * shard + k, pl.ds(s * half, half)]) for k, total in enumerate(sums)]
+            sums = [total + dot32(rows, here[2 * shard + k, part]) for k, total in enumerate(sums)]
         gate, up = sums
-        out_ref[:, shard * units : (shard + 1) * units] = (gate / (1.0 + jnp.exp(-gate)) * up).astype(jnp.bfloat16)
-
-
-def stack_kernel(*refs, widths):
-    pieces, (out_ref, sems) = refs[:-2], refs[-2:]
+        columns = pl.ds(pl.multiple_of(shard * units, units), units)
+        out_ref[:, columns] = (gate / (1.0 + jnp.exp(-gate)) * up).astype(jnp.bfloat16)
+        return _
+
+    lax.fori_loop(0, count, shard_of, 0)
+
+
+def lead_kernel(near_ref, *refs, widths):
+    pieces, (out_ref, stacked, sems) = refs[:-3], refs[-3:]
     units, at, pairs = pieces[0].shape[0], 0, []
     for i, width in enumerate(widths):
         for k in range(3):
-            pairs.append((pieces[3 * i + k], out_ref.at[pl.ds(k * units, units), pl.ds(at, width)]))
+            pairs.append((pieces[3 * i + k], stacked.at[pl.ds(k * units, units), pl.ds(at, width)]))
         at += width
     for copy in fetch(pairs, sems):
         copy.wait()
 
-
-def down_kernel(near_ref, far_ref, stacked_ref, *refs):
+    def block(i, _):
+        place = pl.ds(pl.multiple_of(i * COLUMNS, COLUMNS), COLUMNS)
+        out_ref[:, place] = dot32(near_ref[...], stacked[:, place])
+        return _
+
+    lax.fori_loop(0, at // COLUMNS, block, 0)
+
+
+def down_kernel(lead_ref, far_ref, *refs):
     pieces, (out_ref, far_weight, made, came, sent) = refs[:-5], refs[-5:]
-    at, pairs, copies = 0, [], []
+    at, pairs = 0, []
     for piece in pieces:
         pairs.append((piece, far_weight.at[:, pl.ds(at, piece.shape[1])]))
         at += piece.shape[1]
     for copy in fetch(pairs, came):
         copy.wait()
+
+    def outward(i):
+        place = pl.ds(pl.multiple_of(i * COLUMNS, COLUMNS), COLUMNS)
+        return place, pltpu.make_async_copy(made.at[:, place], out_ref.at[:, place], sent.at[i])
+
+    def block(i, _):
+        place, copy = outward(i)
+        made[:, place] = (lead_ref[:, place] + dot32(far_ref[...], far_weight[:, place])).astype(jnp.bfloat16)
+        copy.start()
+        return _
+
+    lax.fori_loop(0, at // COLUMNS, block, 0)
     for i in range(at // COLUMNS):
-        place = pl.ds(i * COLUMNS, COLUMNS)
-        total = dot32(near_ref[...], stacked_ref[:, place]) + dot32(far_ref[...], far_weight[:, place])
-        made[:, place] = total.astype(jnp.bfloat16)
-        copies.append(pltpu.make_async_copy(made.at[:, place], out_ref.at[:, place], sent.at[i]))
-        copies[-1].start()
-    for copy in copies:
-        copy.wait()
-
-
-def on_core(kernel, shape, operands, mib, scratch=(), out=pltpu.VMEM, away=0):
+        outward(i)[1].wait()
+
+
+def on_core(kernel, shape, operands, mib, scratch=(), out=pltpu.VMEM, away=0, kind=jnp.bfloat16):
     count = len(operands) - away
     return pl.pallas_call(
         kernel,
-        out_shape=jax.ShapeDtypeStruct(shape, jnp.bfloat16),
+        out_shape=jax.ShapeDtypeStruct(shape, kind),
         in_specs=[pl.BlockSpec(memory_space=pltpu.VMEM)] * count + [pl.BlockSpec(memory_space=pltpu.HBM)] * away,
         out_specs=pl.BlockSpec(memory_space=out),
         scratch_shapes=list(scratch),
@@ -256,13 +277,14 @@
         widths = [PIECES[piece] for piece in chunk]
         width = sum(widths)
         sides = [d for piece in chunk for d in downs[piece][:3]]
-        stacked = on_core(
-            lambda *refs, widths=widths: stack_kernel(*refs, widths=widths),
-            (3 * units, width),
-            sides,
-            6,
-            (pltpu.SemaphoreType.DMA((len(sides),)),),
+        lead = on_core(
+            lambda *refs, widths=widths: lead_kernel(*refs, widths=widths),
+            (slots, width),
+            (near, *sides),
+            12,
+            (pltpu.VMEM((3 * units, width), jnp.bfloat16), pltpu.SemaphoreType.DMA((len(sides),))),
             away=len(sides),
+            kind=jnp.float32,
         )
         scratch = (
             pltpu.VMEM((units, width), jnp.bfloat16),
@@ -270,8 +292,8 @@
             pltpu.SemaphoreType.DMA((len(chunk),)),
             pltpu.SemaphoreType.DMA((width // COLUMNS,)),
         )
-        operands = (near, far, stacked, *[downs[piece][3] for piece in chunk])
-        result = on_core(down_kernel, (slots, width), operands, 12, scratch, pltpu.HBM, away=len(chunk))
+        operands = (lead, far, *[downs[piece][3] for piece in chunk])
+        result = on_core(down_kernel, (slots, width), operands, DOWN_MIB, scratch, pltpu.HBM, away=len(chunk))
         back = lax.all_to_all(result.reshape(expert_count, slot_cap, width), "ep", 0, 0, tiled=True)
         returned.append(back.reshape(slots, width))
 

time: 249 us -> 242 us (0.972)
  waiting for transfers between devices: 118 us -> 108 us
    ppermute x22, waiting for transfers between devices: 116 us -> 106 us  [turn(): return lax.ppermute(value, 'tp', pairs)]
    unnamed x46 -> x48, local copies, waits for them, and re-layouts: 15.3 us -> 17.3 us
  transfers between devices with their start and end apart: 26 -> 26, of which waited for: 12 -> 9; matrix products, arithmetic and copies ran while one was open for 2% -> 2% of each run, Pallas kernels for 6% -> 7%
where the time goes in v5:
time: 242 us; the launch traced here: 241 us
  waiting for transfers between devices  108 us (45%)
  starting transfers between devices  87.5 us (36%)
  Pallas kernels  22.4 us (9%)
  local copies, waits for them, and re-layouts  21.9 us (9%)
    ppermute x22, waiting for transfers between devices, turn(): return lax.ppermute(value, 'tp', pairs)  106 us
    ppermute x22, starting transfers between devices, turn(): return lax.ppermute(value, 'tp', pairs)  50.6 us
    all_to_all x2, starting transfers between devices, local(): lax.all_to_all(result.reshape(expert_count, slot_cap, width), 'ep', 0, 0,...  20.7 us
    pallas_call x9, Pallas kernels, on_core(): pl.pallas_call(kernel, out_shape=jax.ShapeDtypeStruct(shape, kind), in_sp...  18.9 us
    unnamed x48, local copies, waits for them, and re-layouts  17.3 us
    all_to_all x1, starting transfers between devices, local(): lax.all_to_all(outgoing.reshape(expert_count, slot_cap, model_width), 'ep...  10.9 us
    ppermute x1, starting transfers between devices, local(): lax.ppermute(product[row_count - tap_span:], ('ep', 'tp'), [(i, i + 1) fo...  5.32 us
  transfers between devices with their start and end apart: 26, of which 9 were waited for; matrix products, arithmetic and copies ran while one was open for 2% of the time, Pallas kernels for 7%

profile of v5, /device:TPU:120, one launch (start us, length us, event | category | flops | bytes accessed | tf_op | source)
XLA Modules:
  0.0 241.3 jit_solution(17035740162165185677)
XLA Ops:
  0.6 1.0 copy-done.15
  3.0 0.9 shard_map.132
  4.0 1.3 copy-done
  5.3 10.9 %all-to-all-start = ((bf16[64,8,2048]{2,1,0:T(8,128)(2,1)}), bf16[64,8,2048]{2,1,0:T(8,128)(2,1)S(1)}, u32[]{:S(2)}, u32[]{:S(2)}) async-start(bf16[64,8,2048]{2,1,0:T(8,128)(2,1)} %bitcast.18), calls=%async_computation | async-start | bytes 4194304 | tf_op jit(solution)/shard_map/all_to_all | solution.py:234
  16.5 1.8 collective-permute-start.8
  18.3 1.4 collective-permute-start.6
  20.3 22.0 %collective-permute-done.5.refs_3_ = bf16[2048,256]{1,0:T(8,128)(2,1)S(1)} collective-permute-done((bf16[2048,256]{1,0:T(8,128)(2,1)S(1)}, bf16[2048,256]{1,0:T(8,128)(2,1)S(1)}, u32[]{:S(2)}, u32[]{:S(2)}) %collective-permute-start.5) | collective-permute-done | bytes 1048608 | tf_op jit(solution)/shard_map/ppermute | solution.py:21
  42.3 1.4 collective-permute-start.13
  43.7 1.0 copy-done.7
  45.3 1.1 fusion.7
  47.2 45.0 %collective-permute-done.12.refs_6_ = bf16[256,384]{1,0:T(8,128)(2,1)} collective-permute-done((bf16[256,384]{1,0:T(8,128)(2,1)S(1)}, bf16[256,384]{1,0:T(8,128)(2,1)}, u32[]{:S(2)}, u32[]{:S(2)}) %collective-permute-start.12) | collective-permute-done | bytes 196640 | tf_op jit(solution)/shard_map/ppermute | solution.py:21
  92.4 5.8 %collective-permute-done.9.refs_2_ = bf16[256,384]{1,0:T(8,128)(2,1)} collective-permute-done((bf16[256,384]{1,0:T(8,128)(2,1)S(1)}, bf16[256,384]{1,0:T(8,128)(2,1)}, u32[]{:S(2)}, u32[]{:S(2)}) %collective-permute-start.9) | collective-permute-done | bytes 196640 | tf_op jit(solution)/shard_map/ppermute | solution.py:21
  98.6 1.0 copy-done.9
  99.6 2.9 %collective-permute-start.11 = (bf16[256,384]{1,0:T(8,128)(2,1)S(1)}, bf16[256,384]{1,0:T(8,128)(2,1)}, u32[]{:S(2)}, u32[]{:S(2)}) collective-permute-start(bf16[256,384]{1,0:T(8,128)(2,1)S(1)} %get-tuple-element.2.refs_4_), channel_id=1, source_target_pairs={{0,1},{1,2},{2,3},{3,0},{4,5},{5,6},{6,7},{7,4},{8,9},{9,10},{10,1... | collective-permute-start | bytes 589832 | tf_op jit(solution)/shard_map/ppermute | solution.py:21
  102.5 1.0 copy-done.11
  103.8 1.0 copy-done.13
  104.8 1.7 collective-permute-start.16
  106.6 1.2 copy-done.5
  107.8 1.2 copy-done.6
  109.0 1.2 copy-done.8
  110.2 1.2 copy-done.10
  111.5 1.2 copy-done.12
  112.7 4.7 %shard_map.133.refs_0_ = bf16[512,768]{1,0:T(8,128)(2,1)S(1)} custom-call(bf16[512,2048]{1,0:T(8,128)(2,1)S(1)} %bitcast.16, bf16[2048,256]{1,0:T(8,128)(2,1)S(1)} %bitcast.23, bf16[2048,256]{1,0:T(8,128)(2,1)S(1)} %bitcast.26, bf16[2048,256]{1,0:T(8,128)(2,1)S(1)} %copy-done.8, bf16[2048,256]{1,0:T(8,128)(2,1)S(1)} %copy-done.10, ...), custom_call_target="tpu_custom_call" | custom-call | tf_op jit(solution)/shard_map/pallas_call | solution.py:162
  117.4 2.5 %shard_map.135.far_ref = bf16[512,256]{1,0:T(8,128)(2,1)S(1)} custom-call(bf16[512,2048]{1,0:T(8,128)(2,1)S(1)} %bitcast.17, bf16[2048,256]{1,0:T(8,128)(2,1)S(1)} %copy-done.14, bf16[2048,256]{1,0:T(8,128)(2,1)} %collective-permute-done.14.refs_2_), custom_call_target="tpu_custom_call" | custom-call | tf_op jit(solution)/shard_map/pallas_call | solution.py:162
  120.0 2.4 %shard_map.134.lead_ref = f32[512,768]{1,0:T(8,128)S(1)} custom-call(bf16[512,768]{1,0:T(8,128)(2,1)S(1)} %shard_map.133.refs_0_, bf16[256,384]{1,0:T(8,128)(2,1)S(1)} %get-tuple-element.3.refs_1_, bf16[256,384]{1,0:T(8,128)(2,1)} %collective-permute-done.9.refs_2_, bf16[256,384]{1,0:T(8,128)(2,1)} %collective-permute-done.10.refs_3_, ...), custom_call_target="tpu_custom_call" | custom-call | tf_op jit(solution)/shard_map/pallas_call | solution.py:162
  122.4 2.5 %shard_map.136 = bf16[512,768]{1,0:T(8,128)(2,1)} custom-call(f32[512,768]{1,0:T(8,128)S(1)} %shard_map.134.lead_ref, bf16[512,256]{1,0:T(8,128)(2,1)S(1)} %shard_map.135.far_ref, bf16[256,384]{1,0:T(8,128)(2,1)} %collective-permute-done.15.refs_0_, bf16[256,384]{1,0:T(8,128)(2,1)} %collective-permute-done.16.refs_1_), custom_call_target="tpu_custom_call" | custom-call | tf_op jit(solution)/shard_map/pallas_call | solution.py:162
  124.9 10.3 %all-to-all-start.1 = ((bf16[64,8,768]{2,1,0:T(8,128)(2,1)}), bf16[64,8,768]{2,1,0:T(8,128)(2,1)S(1)}, u32[]{:S(2)}, u32[]{:S(2)}) async-start(bf16[64,8,768]{2,1,0:T(8,128)(2,1)} %bitcast.12), calls=%async_computation.1 | async-start | bytes 1572864 | tf_op jit(solution)/shard_map/all_to_all | solution.py:297
  135.2 1.0 slice.58.refs_1_
  136.3 1.6 collective-permute-start.17
  137.8 1.0 slice.59.refs_4_
  139.5 8.0 %collective-permute-done.17.refs_2_ = bf16[256,768]{1,0:T(8,128)(2,1)S(1)} collective-permute-done((bf16[256,768]{1,0:T(8,128)(2,1)S(1)}, bf16[256,768]{1,0:T(8,128)(2,1)S(1)}, u32[]{:S(2)}, u32[]{:S(2)}) %collective-permute-start.17) | collective-permute-done | bytes 393248 | tf_op jit(solution)/shard_map/ppermute | solution.py:21
  147.5 2.7 %collective-permute-start.21 = (bf16[256,768]{1,0:T(8,128)(2,1)S(1)}, bf16[256,768]{1,0:T(8,128)(2,1)S(1)}, u32[]{:S(2)}, u32[]{:S(2)}) collective-permute-start(bf16[256,768]{1,0:T(8,128)(2,1)S(1)} %collective-permute-done.17.refs_2_), channel_id=1, source_target_pairs={{0,1},{1,2},{2,3},{3,0},{4,5},{5,6},{6,7},{7,4},{8,9},{9,10},{10,1... | collective-permute-start | bytes 1179656 | tf_op jit(solution)/shard_map/ppermute | solution.py:21
  150.2 2.0 collective-permute-start.22
  152.2 11.4 %collective-permute-done.19.refs_5_ = bf16[256,512]{1,0:T(8,128)(2,1)S(1)} collective-permute-done((bf16[256,512]{1,0:T(8,128)(2,1)S(1)}, bf16[256,512]{1,0:T(8,128)(2,1)S(1)}, u32[]{:S(2)}, u32[]{:S(2)}) %collective-permute-start.19) | collective-permute-done | bytes 262176 | tf_op jit(solution)/shard_map/ppermute | solution.py:21
  163.6 2.1 shard_map.137.lead_ref
  165.7 2.0 shard_map.138
  167.8 10.4 %all-to-all-start.2 = ((bf16[64,8,1280]{2,1,0:T(8,128)(2,1)}), bf16[64,8,1280]{2,1,0:T(8,128)(2,1)S(1)}, u32[]{:S(2)}, u32[]{:S(2)}) async-start(bf16[64,8,1280]{2,1,0:T(8,128)(2,1)} %bitcast.14), calls=%async_computation.2 | async-start | bytes 2621440 | tf_op jit(solution)/shard_map/all_to_all | solution.py:297
  178.5 5.3 %collective-permute-start = (f32[2,2048]{1,0:T(2,128)S(1)}, f32[2,2048]{1,0:T(2,128)S(1)}, u32[]{:S(2)}, u32[]{:S(2)}) collective-permute-start(f32[2,2048]{1,0:T(2,128)S(1)} %slice.48), channel_id=1, source_target_pairs={{0,1},{1,2},{2,3},{3,4},{4,5},{5,6},{6,7},{7,8},{8,9},{9,10},{10,1... | collective-permute-start | bytes 49160 | tf_op jit(solution)/shard_map/ppermute | solution.py:247
  183.8 1.4 collective-permute-done
  185.6 27.4 %collective-permute-start.1 = (bf16[128,2048]{1,0:T(8,128)(2,1)S(1)}, bf16[128,2048]{1,0:T(8,128)(2,1)S(1)}, u32[]{:S(2)}, u32[]{:S(2)}) collective-permute-start(bf16[128,2048]{1,0:T(8,128)(2,1)S(1)} %fusion.5.own_ref), channel_id=1, source_target_pairs={{0,1},{1,2},{2,3},{3,0},{4,5},{5,6},{6,7},{7,4},{8,9},{9,10},{10,1... | collective-permute-start | bytes 1572872 | tf_op jit(solution)/shard_map/ppermute | solution.py:21
  213.1 6.7 %collective-permute-done.1.left_ref = bf16[128,2048]{1,0:T(8,128)(2,1)S(1)} collective-permute-done((bf16[128,2048]{1,0:T(8,128)(2,1)S(1)}, bf16[128,2048]{1,0:T(8,128)(2,1)S(1)}, u32[]{:S(2)}, u32[]{:S(2)}) %collective-permute-start.1) | collective-permute-done | bytes 524320 | tf_op jit(solution)/shard_map/ppermute | solution.py:21
  220.5 3.7 %collective-permute-start.3 = (bf16[64,2048]{1,0:T(8,128)(2,1)}, bf16[64,2048]{1,0:T(8,128)(2,1)}, u32[]{:S(2)}, u32[]{:S(2)}) collective-permute-start(bf16[64,2048]{1,0:T(8,128)(2,1)} %slice.54), channel_id=1, source_target_pairs={{0,1},{1,2},{2,3},{3,0},{4,5},{5,6},{6,7},{7,4},{8,9},{9,10},{10,1... | collective-permute-start | bytes 786440 | tf_op jit(solution)/shard_map/ppermute | solution.py:21
  226.0 2.4 collective-permute-done.3.first_ref
  228.4 5.2 %collective-permute-done.4.second_ref = bf16[64,2048]{1,0:T(8,128)(2,1)} collective-permute-done((bf16[64,2048]{1,0:T(8,128)(2,1)}, bf16[64,2048]{1,0:T(8,128)(2,1)}, u32[]{:S(2)}, u32[]{:S(2)}) %collective-permute-start.4) | collective-permute-done | bytes 262176 | tf_op jit(solution)/shard_map/ppermute | solution.py:21
  233.6 1.6 copy-done.1
  235.2 1.0 copy-done.3
  236.2 3.5 %mixer.1 = bf16[512,512]{1,0:T(8,128)(2,1)} custom-call(s32[1]{0:T(128)} %bitcast.place_ref, bf16[128,2048]{1,0:T(8,128)(2,1)S(1)} %fusion.5.own_ref, bf16[128,2048]{1,0:T(8,128)(2,1)S(1)} %collective-permute-done.1.left_ref, bf16[128,2048]{1,0:T(8,128)(2,1)S(1)} %copy-done.3, bf16[64,2048]{1,0:T(8,128)(2,1)} %collective-permute-done.3.first_ref, ...), custom_call_target="tpu_custom_call" | custom-call | tf_op jit(solution)/shard_map/mixer/pallas_call | solution.py:302
  239.7 1.4 shard_map.139
  (71 shorter events, 8.4 us)
Async XLA Ops:
  0.6 1.0 copy-start.15
  4.0 1.3 copy-start
  5.3 10.9 %copy-start.4 = (bf16[1,2048,256]{2,1,0:T(8,128)(2,1)S(1)}, bf16[1,2048,256]{2,1,0:T(8,128)(2,1)}, u32[]{:S(2)}) copy-start(bf16[1,2048,256]{2,1,0:T(8,128)(2,1)} %param.19) | copy-start | bytes 3145732
  5.3 101.2 %all-to-all-start = ((bf16[64,8,2048]{2,1,0:T(8,128)(2,1)}), bf16[64,8,2048]{2,1,0:T(8,128)(2,1)S(1)}, u32[]{:S(2)}, u32[]{:S(2)}) async-start(bf16[64,8,2048]{2,1,0:T(8,128)(2,1)} %bitcast.18), calls=%async_computation | async-start | bytes 4194304 | tf_op jit(solution)/shard_map/all_to_all | solution.py:234
  16.2 26.1 %collective-permute-start.5 = (bf16[2048,256]{1,0:T(8,128)(2,1)S(1)}, bf16[2048,256]{1,0:T(8,128)(2,1)S(1)}, u32[]{:S(2)}, u32[]{:S(2)}) collective-permute-start(bf16[2048,256]{1,0:T(8,128)(2,1)S(1)} %bitcast.21), channel_id=1, source_target_pairs={{0,1},{1,2},{2,3},{3,0},{4,5},{5,6},{6,7},{7,4},{8,9},{9,10},{10,1... | collective-permute-start | bytes 3145736 | tf_op jit(solution)/shard_map/ppermute | solution.py:21
  16.5 28.2 %collective-permute-start.8 = (bf16[2048,256]{1,0:T(8,128)(2,1)}, bf16[2048,256]{1,0:T(8,128)(2,1)}, u32[]{:S(2)}, u32[]{:S(2)}) collective-permute-start(bf16[2048,256]{1,0:T(8,128)(2,1)} %bitcast.24), channel_id=1, source_target_pairs={{0,3},{1,0},{2,1},{3,2},{4,7},{5,4},{6,5},{7,6},{8,11},{9,8},{10,9... | collective-permute-start | bytes 3145736 | tf_op jit(solution)/shard_map/ppermute | solution.py:21
  18.3 80.3 %collective-permute-start.6 = (bf16[2048,256]{1,0:T(8,128)(2,1)}, bf16[2048,256]{1,0:T(8,128)(2,1)S(1)}, u32[]{:S(2)}, u32[]{:S(2)}) collective-permute-start(bf16[2048,256]{1,0:T(8,128)(2,1)} %bitcast.25), channel_id=1, source_target_pairs={{0,1},{1,2},{2,3},{3,0},{4,5},{5,6},{6,7},{7,4},{8,9},{9,10},{10,1... | collective-permute-start | bytes 3145736 | tf_op jit(solution)/shard_map/ppermute | solution.py:21
  19.7 82.8 %collective-permute-start.7 = (bf16[2048,256]{1,0:T(8,128)(2,1)S(1)}, bf16[2048,256]{1,0:T(8,128)(2,1)S(1)}, u32[]{:S(2)}, u32[]{:S(2)}) collective-permute-start(bf16[2048,256]{1,0:T(8,128)(2,1)S(1)} %bitcast.22), channel_id=1, source_target_pairs={{0,3},{1,0},{2,1},{3,2},{4,7},{5,4},{6,5},{7,6},{8,11},{9,8},{10,9... | collective-permute-start | bytes 3145736 | tf_op jit(solution)/shard_map/ppermute | solution.py:21
  42.3 61.5 %collective-permute-start.13 = (bf16[2048,256]{1,0:T(8,128)(2,1)S(1)}, bf16[2048,256]{1,0:T(8,128)(2,1)S(1)}, u32[]{:S(2)}, u32[]{:S(2)}) collective-permute-start(bf16[2048,256]{1,0:T(8,128)(2,1)S(1)} %collective-permute-done.5.refs_3_), channel_id=1, source_target_pairs={{0,1},{1,2},{2,3},{3,0},{4,5},{5,6},{6,7},{7,4},{8,9},{9,10},{10,1... | collective-permute-start | bytes 3145736 | tf_op jit(solution)/shard_map/ppermute | solution.py:21
  43.7 1.0 copy-start.7
  44.7 72.6 %collective-permute-start.14 = (bf16[2048,256]{1,0:T(8,128)(2,1)}, bf16[2048,256]{1,0:T(8,128)(2,1)}, u32[]{:S(2)}, u32[]{:S(2)}) collective-permute-start(bf16[2048,256]{1,0:T(8,128)(2,1)} %collective-permute-done.8.refs_6_), channel_id=1, source_target_pairs={{0,3},{1,0},{2,1},{3,2},{4,7},{5,4},{6,5},{7,6},{8,11},{9,8},{10,9... | collective-permute-start | bytes 3145736 | tf_op jit(solution)/shard_map/ppermute | solution.py:21
  46.4 45.8 %collective-permute-start.12 = (bf16[256,384]{1,0:T(8,128)(2,1)S(1)}, bf16[256,384]{1,0:T(8,128)(2,1)}, u32[]{:S(2)}, u32[]{:S(2)}) collective-permute-start(bf16[256,384]{1,0:T(8,128)(2,1)S(1)} %get-tuple-element.2.refs_4_), channel_id=1, source_target_pairs={{0,3},{1,0},{2,1},{3,2},{4,7},{5,4},{6,5},{7,6},{8,11},{9,8},{10,9... | collective-permute-start | bytes 589832 | tf_op jit(solution)/shard_map/ppermute | solution.py:21
  92.2 6.0 %collective-permute-start.9 = (bf16[256,384]{1,0:T(8,128)(2,1)S(1)}, bf16[256,384]{1,0:T(8,128)(2,1)}, u32[]{:S(2)}, u32[]{:S(2)}) collective-permute-start(bf16[256,384]{1,0:T(8,128)(2,1)S(1)} %get-tuple-element.3.refs_1_), channel_id=1, source_target_pairs={{0,1},{1,2},{2,3},{3,0},{4,5},{5,6},{6,7},{7,4},{8,9},{9,10},{10,1... | collective-permute-start | bytes 589832 | tf_op jit(solution)/shard_map/ppermute | solution.py:21
  98.3 21.7 %collective-permute-start.10 = (bf16[256,384]{1,0:T(8,128)(2,1)S(1)}, bf16[256,384]{1,0:T(8,128)(2,1)}, u32[]{:S(2)}, u32[]{:S(2)}) collective-permute-start(bf16[256,384]{1,0:T(8,128)(2,1)S(1)} %get-tuple-element.3.refs_1_), channel_id=1, source_target_pairs={{0,3},{1,0},{2,1},{3,2},{4,7},{5,4},{6,5},{7,6},{8,11},{9,8},{10,9... | collective-permute-start | bytes 589832 | tf_op jit(solution)/shard_map/ppermute | solution.py:21
  98.6 1.0 copy-start.9
  99.6 20.4 %collective-permute-start.11 = (bf16[256,384]{1,0:T(8,128)(2,1)S(1)}, bf16[256,384]{1,0:T(8,128)(2,1)}, u32[]{:S(2)}, u32[]{:S(2)}) collective-permute-start(bf16[256,384]{1,0:T(8,128)(2,1)S(1)} %get-tuple-element.2.refs_4_), channel_id=1, source_target_pairs={{0,1},{1,2},{2,3},{3,0},{4,5},{5,6},{6,7},{7,4},{8,9},{9,10},{10,1... | collective-permute-start | bytes 589832 | tf_op jit(solution)/shard_map/ppermute | solution.py:21
  102.5 1.0 copy-start.11
  103.5 18.9 %collective-permute-start.15 = (bf16[256,384]{1,0:T(8,128)(2,1)}, bf16[256,384]{1,0:T(8,128)(2,1)}, u32[]{:S(2)}, u32[]{:S(2)}) collective-permute-start(bf16[256,384]{1,0:T(8,128)(2,1)} %collective-permute-done.9.refs_2_), channel_id=1, source_target_pairs={{0,1},{1,2},{2,3},{3,0},{4,5},{5,6},{6,7},{7,4},{8,9},{9,10},{10,1... | collective-permute-start | bytes 589832 | tf_op jit(solution)/shard_map/ppermute | solution.py:21
  103.8 1.0 copy-start.13
  104.8 17.6 %collective-permute-start.16 = (bf16[256,384]{1,0:T(8,128)(2,1)}, bf16[256,384]{1,0:T(8,128)(2,1)}, u32[]{:S(2)}, u32[]{:S(2)}) collective-permute-start(bf16[256,384]{1,0:T(8,128)(2,1)} %collective-permute-done.12.refs_6_), channel_id=1, source_target_pairs={{0,3},{1,0},{2,1},{3,2},{4,7},{5,4},{6,5},{7,6},{8,11},{9,8},{10,9... | collective-permute-start | bytes 589832 | tf_op jit(solution)/shard_map/ppermute | solution.py:21
  106.6 1.2 copy-start.5
  107.8 1.2 copy-start.6
  109.0 1.2 copy-start.8
  110.2 1.2 copy-start.10
  111.5 1.2 copy-start.12
  112.7 4.7 %copy-start.14 = (bf16[2048,256]{1,0:T(8,128)(2,1)S(1)}, bf16[2048,256]{1,0:T(8,128)(2,1)}, u32[]{:S(2)}) copy-start(bf16[2048,256]{1,0:T(8,128)(2,1)} %copy-done.13) | copy-start | bytes 3145732
  124.9 42.9 %all-to-all-start.1 = ((bf16[64,8,768]{2,1,0:T(8,128)(2,1)}), bf16[64,8,768]{2,1,0:T(8,128)(2,1)S(1)}, u32[]{:S(2)}, u32[]{:S(2)}) async-start(bf16[64,8,768]{2,1,0:T(8,128)(2,1)} %bitcast.12), calls=%async_computation.1 | async-start | bytes 1572864 | tf_op jit(solution)/shard_map/all_to_all | solution.py:297
  136.3 11.2 %collective-permute-start.17 = (bf16[256,768]{1,0:T(8,128)(2,1)S(1)}, bf16[256,768]{1,0:T(8,128)(2,1)S(1)}, u32[]{:S(2)}, u32[]{:S(2)}) collective-permute-start(bf16[256,768]{1,0:T(8,128)(2,1)S(1)} %slice.58.refs_1_), channel_id=1, source_target_pairs={{0,1},{1,2},{2,3},{3,0},{4,5},{5,6},{6,7},{7,4},{8,9},{9,10},{10,1... | collective-permute-start | bytes 1179656 | tf_op jit(solution)/shard_map/ppermute | solution.py:21
  138.8 11.4 %collective-permute-start.20 = (bf16[256,512]{1,0:T(8,128)(2,1)S(1)}, bf16[256,512]{1,0:T(8,128)(2,1)S(1)}, u32[]{:S(2)}, u32[]{:S(2)}) collective-permute-start(bf16[256,512]{1,0:T(8,128)(2,1)S(1)} %slice.59.refs_4_), channel_id=1, source_target_pairs={{0,3},{1,0},{2,1},{3,2},{4,7},{5,4},{6,5},{7,6},{8,11},{9,8},{10,9... | collective-permute-start | bytes 786440 | tf_op jit(solution)/shard_map/ppermute | solution.py:21
  139.4 24.2 %collective-permute-start.18 = (bf16[256,768]{1,0:T(8,128)(2,1)S(1)}, bf16[256,768]{1,0:T(8,128)(2,1)S(1)}, u32[]{:S(2)}, u32[]{:S(2)}) collective-permute-start(bf16[256,768]{1,0:T(8,128)(2,1)S(1)} %slice.58.refs_1_), channel_id=1, source_target_pairs={{0,3},{1,0},{2,1},{3,2},{4,7},{5,4},{6,5},{7,6},{8,11},{9,8},{10,9... | collective-permute-start | bytes 1179656 | tf_op jit(solution)/shard_map/ppermute | solution.py:21
  147.5 18.2 %collective-permute-start.21 = (bf16[256,768]{1,0:T(8,128)(2,1)S(1)}, bf16[256,768]{1,0:T(8,128)(2,1)S(1)}, u32[]{:S(2)}, u32[]{:S(2)}) collective-permute-start(bf16[256,768]{1,0:T(8,128)(2,1)S(1)} %collective-permute-done.17.refs_2_), channel_id=1, source_target_pairs={{0,1},{1,2},{2,3},{3,0},{4,5},{5,6},{6,7},{7,4},{8,9},{9,10},{10,1... | collective-permute-start | bytes 1179656 | tf_op jit(solution)/shard_map/ppermute | solution.py:21
  150.2 13.4 %collective-permute-start.19 = (bf16[256,512]{1,0:T(8,128)(2,1)S(1)}, bf16[256,512]{1,0:T(8,128)(2,1)S(1)}, u32[]{:S(2)}, u32[]{:S(2)}) collective-permute-start(bf16[256,512]{1,0:T(8,128)(2,1)S(1)} %slice.59.refs_4_), channel_id=1, source_target_pairs={{0,1},{1,2},{2,3},{3,0},{4,5},{5,6},{6,7},{7,4},{8,9},{9,10},{10,1... | collective-permute-start | bytes 786440 | tf_op jit(solution)/shard_map/ppermute | solution.py:21
  150.2 15.5 %collective-permute-start.22 = (bf16[256,512]{1,0:T(8,128)(2,1)S(1)}, bf16[256,512]{1,0:T(8,128)(2,1)S(1)}, u32[]{:S(2)}, u32[]{:S(2)}) collective-permute-start(bf16[256,512]{1,0:T(8,128)(2,1)S(1)} %collective-permute-done.20.refs_6_), channel_id=1, source_target_pairs={{0,3},{1,0},{2,1},{3,2},{4,7},{5,4},{6,5},{7,6},{8,11},{9,8},{10,9... | collective-permute-start | bytes 786440 | tf_op jit(solution)/shard_map/ppermute | solution.py:21
  167.8 10.5 %copy-start.20 = (bf16[128,2048]{1,0:T(8,128)(2,1)S(1)}, bf16[128,2048]{1,0:T(8,128)(2,1)}, u32[]{:S(2)}) copy-start(bf16[128,2048]{1,0:T(8,128)(2,1)} %param.14) | copy-start | bytes 1572868
  167.8 10.5 %copy-start.21 = (bf16[128,2048]{1,0:T(8,128)(2,1)S(1)}, bf16[128,2048]{1,0:T(8,128)(2,1)}, u32[]{:S(2)}) copy-start(bf16[128,2048]{1,0:T(8,128)(2,1)} %param.13) | copy-start | bytes 1572868
  167.8 71.9 %all-to-all-start.2 = ((bf16[64,8,1280]{2,1,0:T(8,128)(2,1)}), bf16[64,8,1280]{2,1,0:T(8,128)(2,1)S(1)}, u32[]{:S(2)}, u32[]{:S(2)}) async-start(bf16[64,8,1280]{2,1,0:T(8,128)(2,1)} %bitcast.14), calls=%async_computation.2 | async-start | bytes 2621440 | tf_op jit(solution)/shard_map/all_to_all | solution.py:297
  178.3 5.5 %copy-start.23 = (bf16[3,2048]{1,0:T(4,128)(2,1)S(1)}, bf16[3,2048]{1,0:T(4,128)(2,1)}, u32[]{:S(2)}) copy-start(bf16[3,2048]{1,0:T(4,128)(2,1)} %param.15) | copy-start | bytes 36868
  178.3 6.9 %copy-start.22 = (bf16[128,2048]{1,0:T(8,128)(2,1)S(1)}, bf16[128,2048]{1,0:T(8,128)(2,1)}, u32[]{:S(2)}) copy-start(bf16[128,2048]{1,0:T(8,128)(2,1)} %param.12) | copy-start | bytes 1572868
  178.5 6.8 %collective-permute-start = (f32[2,2048]{1,0:T(2,128)S(1)}, f32[2,2048]{1,0:T(2,128)S(1)}, u32[]{:S(2)}, u32[]{:S(2)}) collective-permute-start(f32[2,2048]{1,0:T(2,128)S(1)} %slice.48), channel_id=1, source_target_pairs={{0,1},{1,2},{2,3},{3,4},{4,5},{5,6},{6,7},{7,8},{8,9},{9,10},{10,1... | collective-permute-start | bytes 49160 | tf_op jit(solution)/shard_map/ppermute | solution.py:247
  185.2 40.5 %copy-start.18 = (s32[128,2]{0,1:T(2,128)S(1)}, s32[128,2]{0,1:T(2,128)}, u32[]{:S(2)}) copy-start(s32[128,2]{0,1:T(2,128)} %param.22) | copy-start | bytes 3076
  185.2 40.5 %copy-start.19 = (f32[128,2]{0,1:T(2,128)S(1)}, f32[128,2]{0,1:T(2,128)}, u32[]{:S(2)}) copy-start(f32[128,2]{0,1:T(2,128)} %param.23) | copy-start | bytes 3076
  185.6 34.1 %collective-permute-start.1 = (bf16[128,2048]{1,0:T(8,128)(2,1)S(1)}, bf16[128,2048]{1,0:T(8,128)(2,1)S(1)}, u32[]{:S(2)}, u32[]{:S(2)}) collective-permute-start(bf16[128,2048]{1,0:T(8,128)(2,1)S(1)} %fusion.5.own_ref), channel_id=1, source_target_pairs={{0,1},{1,2},{2,3},{3,0},{4,5},{5,6},{6,7},{7,4},{8,9},{9,10},{10,1... | collective-permute-start | bytes 1572872 | tf_op jit(solution)/shard_map/ppermute | solution.py:21
  213.1 11.1 %collective-permute-start.2 = (bf16[128,2048]{1,0:T(8,128)(2,1)S(1)}, bf16[128,2048]{1,0:T(8,128)(2,1)S(1)}, u32[]{:S(2)}, u32[]{:S(2)}) collective-permute-start(bf16[128,2048]{1,0:T(8,128)(2,1)S(1)} %fusion.5.own_ref), channel_id=1, source_target_pairs={{0,3},{1,0},{2,1},{3,2},{4,7},{5,4},{6,5},{7,6},{8,11},{9,8},{10,9... | collective-permute-start | bytes 1572872 | tf_op jit(solution)/shard_map/ppermute | solution.py:21
  220.5 7.9 %collective-permute-start.3 = (bf16[64,2048]{1,0:T(8,128)(2,1)}, bf16[64,2048]{1,0:T(8,128)(2,1)}, u32[]{:S(2)}, u32[]{:S(2)}) collective-permute-start(bf16[64,2048]{1,0:T(8,128)(2,1)} %slice.54), channel_id=1, source_target_pairs={{0,1},{1,2},{2,3},{3,0},{4,5},{5,6},{6,7},{7,4},{8,9},{9,10},{10,1... | collective-permute-start | bytes 786440 | tf_op jit(solution)/shard_map/ppermute | solution.py:21
  224.9 0.8 copy-start.2
  225.7 7.9 %collective-permute-start.4 = (bf16[64,2048]{1,0:T(8,128)(2,1)}, bf16[64,2048]{1,0:T(8,128)(2,1)}, u32[]{:S(2)}, u32[]{:S(2)}) collective-permute-start(bf16[64,2048]{1,0:T(8,128)(2,1)} %slice.55), channel_id=1, source_target_pairs={{0,3},{1,0},{2,1},{3,2},{4,7},{5,4},{6,5},{7,6},{8,11},{9,8},{10,9... | collective-permute-start | bytes 786440 | tf_op jit(solution)/shard_map/ppermute | solution.py:21
  233.6 1.6 copy-start.1
  235.2 1.0 copy-start.3
  (2 other events, 1.4 us)

commit v6 on v5

--- a/solution.py
+++ b/solution.py
@@ -8,7 +8,7 @@
 
 CONV = 3
 NORM_EPS = 1e-06
-PIECES = (384, 384, 768, 512)
+PIECES = (384, 256, 768, 640)
 CHUNKS = ((0, 1), (2, 3))
 COLUMNS = 256
 MIB = 1 << 20
@@ -73,13 +73,13 @@
     chunks, out_ref, made, sent = refs[:-3], refs[-3], refs[-2], refs[-1]
     tokens, at, copies = made.shape[0], 0, []
     for chunk in chunks:
-        for first in range(0, chunk.shape[1], COLUMNS):
-            both = dot32(mix_ref[...], chunk[:, first : first + COLUMNS])
-            made[:, at : at + COLUMNS] = (both[:tokens] + both[tokens:]).astype(jnp.bfloat16)
-            place = pl.ds(at, COLUMNS)
+        for span in spans(chunk.shape[1]):
+            both = dot32(mix_ref[...], chunk[:, span])
+            place = pl.ds(at, span.size)
+            made[:, place] = (both[:tokens] + both[tokens:]).astype(jnp.bfloat16)
             copies.append(pltpu.make_async_copy(made.at[:, place], out_ref.at[:, place], sent.at[len(copies)]))
             copies[-1].start()
-            at += COLUMNS
+            at += span.size
     for copy in copies:
         copy.wait()
 
@@ -125,12 +125,8 @@
     for copy in fetch(pairs, sems):
         copy.wait()
 
-    def block(i, _):
-        place = pl.ds(pl.multiple_of(i * COLUMNS, COLUMNS), COLUMNS)
+    for place in spans(at):
         out_ref[:, place] = dot32(near_ref[...], stacked[:, place])
-        return _
-
-    lax.fori_loop(0, at // COLUMNS, block, 0)
 
 
 def down_kernel(lead_ref, far_ref, *refs):
@@ -142,19 +138,13 @@
     for copy in fetch(pairs, came):
         copy.wait()
 
-    def outward(i):
-        place = pl.ds(pl.multiple_of(i * COLUMNS, COLUMNS), COLUMNS)
-        return place, pltpu.make_async_copy(made.at[:, place], out_ref.at[:, place], sent.at[i])
-
-    def block(i, _):
-        place, copy = outward(i)
+    copies = []
+    for i, place in enumerate(spans(at)):
         made[:, place] = (lead_ref[:, place] + dot32(far_ref[...], far_weight[:, place])).astype(jnp.bfloat16)
-        copy.start()
-        return _
-
-    lax.fori_loop(0, at // COLUMNS, block, 0)
-    for i in range(at // COLUMNS):
-        outward(i)[1].wait()
+        copies.append(pltpu.make_async_copy(made.at[:, place], out_ref.at[:, place], sent.at[i]))
+        copies[-1].start()
+    for copy in copies:
+        copy.wait()
 
 
 def on_core(kernel, shape, operands, mib, scratch=(), out=pltpu.VMEM, away=0, kind=jnp.bfloat16):
@@ -183,6 +173,10 @@
     put(right_ref, 1, 0)
     put(first_ref, 2, 0)
     put(second_ref, 2, rows // 2)
+
+
+def spans(width):
+    return [pl.ds(at, min(COLUMNS, width - at)) for at in range(0, width, COLUMNS)]
 
 
 def dot32(a, b):
@@ -290,7 +284,7 @@
             pltpu.VMEM((units, width), jnp.bfloat16),
             pltpu.VMEM((slots, width), jnp.bfloat16),
             pltpu.SemaphoreType.DMA((len(chunk),)),
-            pltpu.SemaphoreType.DMA((width // COLUMNS,)),
+            pltpu.SemaphoreType.DMA((len(spans(width)),)),
         )
         operands = (lead, far, *[downs[piece][3] for piece in chunk])
         result = on_core(down_kernel, (slots, width), operands, DOWN_MIB, scratch, pltpu.HBM, away=len(chunk))
@@ -310,7 +304,7 @@
 
     scratch = (
         pltpu.VMEM((token_count, model_width), jnp.bfloat16),
-        pltpu.SemaphoreType.DMA((model_width // COLUMNS,)),
+        pltpu.SemaphoreType.DMA((model_width // COLUMNS + len(CHUNKS),)),
     )
     experts_out = on_core(combine_kernel, (token_count, model_width), (mix, *returned), 8, scratch, pltpu.HBM)
     return (mixer_out, experts_out)

time: 242 us -> 244 us (level)
  starting transfers between devices: 87.5 us -> 90 us
    ppermute x22, starting transfers between devices: 50.6 us -> 53.1 us  [turn(): return lax.ppermute(value, 'tp', pairs)]
  transfers between devices with their start and end apart: 26 -> 26, of which waited for: 9 -> 10; matrix products, arithmetic and copies ran while one was open for 2% -> 2% of each run, Pallas kernels for 7% -> 7%
where the time goes in v6:
time: 244 us; the launch traced here: 243 us
  waiting for transfers between devices  108 us (44%)
  starting transfers between devices  90 us (37%)
  local copies, waits for them, and re-layouts  22.7 us (9%)
  Pallas kernels  20.8 us (9%)
    ppermute x22, waiting for transfers between devices, turn(): return lax.ppermute(value, 'tp', pairs)  106 us
    ppermute x22, starting transfers between devices, turn(): return lax.ppermute(value, 'tp', pairs)  53.1 us
    all_to_all x2, starting transfers between devices, local(): lax.all_to_all(result.reshape(expert_count, slot_cap, width), 'ep', 0, 0,...  20.7 us
    pallas_call x9, Pallas kernels, on_core(): pl.pallas_call(kernel, out_shape=jax.ShapeDtypeStruct(shape, kind), in_sp...  17.3 us
    unnamed x48, local copies, waits for them, and re-layouts  17.3 us
    all_to_all x1, starting transfers between devices, local(): lax.all_to_all(outgoing.reshape(expert_count, slot_cap, model_width), 'ep...  10.9 us
    ppermute x1, starting transfers between devices, local(): lax.ppermute(product[row_count - tap_span:], ('ep', 'tp'), [(i, i + 1) fo...  5.34 us
  transfers between devices with their start and end apart: 26, of which 10 were waited for; matrix products, arithmetic and copies ran while one was open for 2% of the time, Pallas kernels for 7%

profile of v6, /device:TPU:120, one launch (start us, length us, event | category | flops | bytes accessed | tf_op | source)
XLA Modules:
  0.0 242.7 jit_solution(491450668191828752)
XLA Ops:
  0.6 1.0 copy-done.15
  4.0 1.3 copy-done
  5.3 10.9 %all-to-all-start = ((bf16[64,8,2048]{2,1,0:T(8,128)(2,1)}), bf16[64,8,2048]{2,1,0:T(8,128)(2,1)S(1)}, u32[]{:S(2)}, u32[]{:S(2)}) async-start(bf16[64,8,2048]{2,1,0:T(8,128)(2,1)} %bitcast.18), calls=%async_computation | async-start | bytes 4194304 | tf_op jit(solution)/shard_map/all_to_all | solution.py:228
  16.5 1.8 collective-permute-start.8
  18.3 1.4 collective-permute-start.6
  20.3 22.0 %collective-permute-done.5.refs_3_ = bf16[2048,256]{1,0:T(8,128)(2,1)S(1)} collective-permute-done((bf16[2048,256]{1,0:T(8,128)(2,1)S(1)}, bf16[2048,256]{1,0:T(8,128)(2,1)S(1)}, u32[]{:S(2)}, u32[]{:S(2)}) %collective-permute-start.5) | collective-permute-done | bytes 1048608 | tf_op jit(solution)/shard_map/ppermute | solution.py:21
  42.3 1.4 collective-permute-start.13
  43.7 1.0 copy-done.7
  45.3 0.9 slice.57.refs_4_
  47.0 0.9 slice.56.refs_1_
  48.0 42.8 %collective-permute-done.12.refs_6_ = bf16[256,256]{1,0:T(8,128)(2,1)} collective-permute-done((bf16[256,256]{1,0:T(8,128)(2,1)S(1)}, bf16[256,256]{1,0:T(8,128)(2,1)}, u32[]{:S(2)}, u32[]{:S(2)}) %collective-permute-start.12) | collective-permute-done | bytes 131104 | tf_op jit(solution)/shard_map/ppermute | solution.py:21
  91.0 5.8 %collective-permute-done.9.refs_2_ = bf16[256,384]{1,0:T(8,128)(2,1)} collective-permute-done((bf16[256,384]{1,0:T(8,128)(2,1)S(1)}, bf16[256,384]{1,0:T(8,128)(2,1)}, u32[]{:S(2)}, u32[]{:S(2)}) %collective-permute-start.9) | collective-permute-done | bytes 196640 | tf_op jit(solution)/shard_map/ppermute | solution.py:21
  97.2 1.0 copy-done.9
  98.1 2.9 %collective-permute-start.15 = (bf16[256,384]{1,0:T(8,128)(2,1)}, bf16[256,384]{1,0:T(8,128)(2,1)}, u32[]{:S(2)}, u32[]{:S(2)}) collective-permute-start(bf16[256,384]{1,0:T(8,128)(2,1)} %collective-permute-done.9.refs_2_), channel_id=1, source_target_pairs={{0,1},{1,2},{2,3},{3,0},{4,5},{5,6},{6,7},{7,4},{8,9},{9,10},{10,1... | collective-permute-start | bytes 589832 | tf_op jit(solution)/shard_map/ppermute | solution.py:21
  101.1 1.0 copy-done.11
  102.3 1.0 copy-done.13
  103.4 1.7 collective-permute-start.16
  105.1 1.2 copy-done.5
  106.3 1.2 copy-done.6
  107.6 1.2 copy-done.8
  108.8 1.2 copy-done.10
  110.0 1.2 copy-done.12
  111.2 4.7 %shard_map.133.refs_0_ = bf16[512,768]{1,0:T(8,128)(2,1)S(1)} custom-call(bf16[512,2048]{1,0:T(8,128)(2,1)S(1)} %bitcast.16, bf16[2048,256]{1,0:T(8,128)(2,1)S(1)} %bitcast.23, bf16[2048,256]{1,0:T(8,128)(2,1)S(1)} %bitcast.26, bf16[2048,256]{1,0:T(8,128)(2,1)S(1)} %copy-done.8, bf16[2048,256]{1,0:T(8,128)(2,1)S(1)} %copy-done.10, ...), custom_call_target="tpu_custom_call" | custom-call | tf_op jit(solution)/shard_map/pallas_call | solution.py:152
  115.9 2.5 %shard_map.135.far_ref = bf16[512,256]{1,0:T(8,128)(2,1)S(1)} custom-call(bf16[512,2048]{1,0:T(8,128)(2,1)S(1)} %bitcast.17, bf16[2048,256]{1,0:T(8,128)(2,1)S(1)} %copy-done.14, bf16[2048,256]{1,0:T(8,128)(2,1)} %collective-permute-done.14.refs_2_), custom_call_target="tpu_custom_call" | custom-call | tf_op jit(solution)/shard_map/pallas_call | solution.py:152
  118.5 2.0 shard_map.134.lead_ref
  120.6 2.2 shard_map.136
  122.7 10.3 %all-to-all-start.1 = ((bf16[64,8,640]{2,1,0:T(8,128)(2,1)}), bf16[64,8,640]{2,1,0:T(8,128)(2,1)S(1)}, u32[]{:S(2)}, u32[]{:S(2)}) async-start(bf16[64,8,640]{2,1,0:T(8,128)(2,1)} %bitcast.12), calls=%async_computation.1 | async-start | bytes 1310720 | tf_op jit(solution)/shard_map/all_to_all | solution.py:291
  133.1 1.0 slice.58.refs_1_
  134.1 1.6 collective-permute-start.17
  135.7 1.0 slice.59.refs_4_
  137.4 7.9 %collective-permute-done.17.refs_2_ = bf16[256,768]{1,0:T(8,128)(2,1)S(1)} collective-permute-done((bf16[256,768]{1,0:T(8,128)(2,1)S(1)}, bf16[256,768]{1,0:T(8,128)(2,1)S(1)}, u32[]{:S(2)}, u32[]{:S(2)}) %collective-permute-start.17) | collective-permute-done | bytes 393248 | tf_op jit(solution)/shard_map/ppermute | solution.py:21
  145.3 2.7 %collective-permute-start.21 = (bf16[256,768]{1,0:T(8,128)(2,1)S(1)}, bf16[256,768]{1,0:T(8,128)(2,1)S(1)}, u32[]{:S(2)}, u32[]{:S(2)}) collective-permute-start(bf16[256,768]{1,0:T(8,128)(2,1)S(1)} %collective-permute-done.17.refs_2_), channel_id=1, source_target_pairs={{0,1},{1,2},{2,3},{3,0},{4,5},{5,6},{6,7},{7,4},{8,9},{9,10},{10,1... | collective-permute-start | bytes 1179656 | tf_op jit(solution)/shard_map/ppermute | solution.py:21
  148.5 1.5 collective-permute-start.22
  150.1 12.8 %collective-permute-done.19.refs_5_ = bf16[256,640]{1,0:T(8,128)(2,1)S(1)} collective-permute-done((bf16[256,640]{1,0:T(8,128)(2,1)S(1)}, bf16[256,640]{1,0:T(8,128)(2,1)S(1)}, u32[]{:S(2)}, u32[]{:S(2)}) %collective-permute-start.19) | collective-permute-done | bytes 327712 | tf_op jit(solution)/shard_map/ppermute | solution.py:21
  162.9 1.6 shard_map.137.lead_ref
  164.5 1.6 shard_map.138
  166.1 10.4 %all-to-all-start.2 = ((bf16[64,8,1408]{2,1,0:T(8,128)(2,1)}), bf16[64,8,1408]{2,1,0:T(8,128)(2,1)S(1)}, u32[]{:S(2)}, u32[]{:S(2)}) async-start(bf16[64,8,1408]{2,1,0:T(8,128)(2,1)} %bitcast.14), calls=%async_computation.2 | async-start | bytes 2883584 | tf_op jit(solution)/shard_map/all_to_all | solution.py:291
  176.8 5.3 %collective-permute-start = (f32[2,2048]{1,0:T(2,128)S(1)}, f32[2,2048]{1,0:T(2,128)S(1)}, u32[]{:S(2)}, u32[]{:S(2)}) collective-permute-start(f32[2,2048]{1,0:T(2,128)S(1)} %slice.48), channel_id=1, source_target_pairs={{0,1},{1,2},{2,3},{3,4},{4,5},{5,6},{6,7},{7,8},{8,9},{9,10},{10,1... | collective-permute-start | bytes 49160 | tf_op jit(solution)/shard_map/ppermute | solution.py:241
  182.1 1.4 collective-permute-done
  183.9 30.4 %collective-permute-start.1 = (bf16[128,2048]{1,0:T(8,128)(2,1)S(1)}, bf16[128,2048]{1,0:T(8,128)(2,1)S(1)}, u32[]{:S(2)}, u32[]{:S(2)}) collective-permute-start(bf16[128,2048]{1,0:T(8,128)(2,1)S(1)} %fusion.5.own_ref), channel_id=1, source_target_pairs={{0,1},{1,2},{2,3},{3,0},{4,5},{5,6},{6,7},{7,4},{8,9},{9,10},{10,1... | collective-permute-start | bytes 1572872 | tf_op jit(solution)/shard_map/ppermute | solution.py:21
  214.4 6.7 %collective-permute-done.1.left_ref = bf16[128,2048]{1,0:T(8,128)(2,1)S(1)} collective-permute-done((bf16[128,2048]{1,0:T(8,128)(2,1)S(1)}, bf16[128,2048]{1,0:T(8,128)(2,1)S(1)}, u32[]{:S(2)}, u32[]{:S(2)}) %collective-permute-start.1) | collective-permute-done | bytes 524320 | tf_op jit(solution)/shard_map/ppermute | solution.py:21
  221.8 3.7 %collective-permute-start.3 = (bf16[64,2048]{1,0:T(8,128)(2,1)}, bf16[64,2048]{1,0:T(8,128)(2,1)}, u32[]{:S(2)}, u32[]{:S(2)}) collective-permute-start(bf16[64,2048]{1,0:T(8,128)(2,1)} %slice.54), channel_id=1, source_target_pairs={{0,1},{1,2},{2,3},{3,0},{4,5},{5,6},{6,7},{7,4},{8,9},{9,10},{10,1... | collective-permute-start | bytes 786440 | tf_op jit(solution)/shard_map/ppermute | solution.py:21
  227.3 2.4 collective-permute-done.3.first_ref
  229.7 5.2 %collective-permute-done.4.second_ref = bf16[64,2048]{1,0:T(8,128)(2,1)} collective-permute-done((bf16[64,2048]{1,0:T(8,128)(2,1)}, bf16[64,2048]{1,0:T(8,128)(2,1)}, u32[]{:S(2)}, u32[]{:S(2)}) %collective-permute-start.4) | collective-permute-done | bytes 262176 | tf_op jit(solution)/shard_map/ppermute | solution.py:21
  234.9 1.6 copy-done.1
  236.5 1.0 copy-done.3
  237.5 3.5 %mixer.1 = bf16[512,512]{1,0:T(8,128)(2,1)} custom-call(s32[1]{0:T(128)} %bitcast.place_ref, bf16[128,2048]{1,0:T(8,128)(2,1)S(1)} %fusion.5.own_ref, bf16[128,2048]{1,0:T(8,128)(2,1)S(1)} %collective-permute-done.1.left_ref, bf16[128,2048]{1,0:T(8,128)(2,1)S(1)} %copy-done.3, bf16[64,2048]{1,0:T(8,128)(2,1)} %collective-permute-done.3.first_ref, ...), custom_call_target="tpu_custom_call" | custom-call | tf_op jit(solution)/shard_map/mixer/pallas_call | solution.py:296
  241.0 1.5 shard_map.139
  (72 shorter events, 9.8 us)
Async XLA Ops:
  0.6 1.0 copy-start.15
  4.0 1.3 copy-start
  5.3 10.9 %copy-start.4 = (bf16[1,2048,256]{2,1,0:T(8,128)(2,1)S(1)}, bf16[1,2048,256]{2,1,0:T(8,128)(2,1)}, u32[]{:S(2)}) copy-start(bf16[1,2048,256]{2,1,0:T(8,128)(2,1)} %param.19) | copy-start | bytes 3145732
  5.3 99.8 %all-to-all-start = ((bf16[64,8,2048]{2,1,0:T(8,128)(2,1)}), bf16[64,8,2048]{2,1,0:T(8,128)(2,1)S(1)}, u32[]{:S(2)}, u32[]{:S(2)}) async-start(bf16[64,8,2048]{2,1,0:T(8,128)(2,1)} %bitcast.18), calls=%async_computation | async-start | bytes 4194304 | tf_op jit(solution)/shard_map/all_to_all | solution.py:228
  16.2 26.1 %collective-permute-start.5 = (bf16[2048,256]{1,0:T(8,128)(2,1)S(1)}, bf16[2048,256]{1,0:T(8,128)(2,1)S(1)}, u32[]{:S(2)}, u32[]{:S(2)}) collective-permute-start(bf16[2048,256]{1,0:T(8,128)(2,1)S(1)} %bitcast.21), channel_id=1, source_target_pairs={{0,1},{1,2},{2,3},{3,0},{4,5},{5,6},{6,7},{7,4},{8,9},{9,10},{10,1... | collective-permute-start | bytes 3145736 | tf_op jit(solution)/shard_map/ppermute | solution.py:21
  16.5 28.2 %collective-permute-start.8 = (bf16[2048,256]{1,0:T(8,128)(2,1)}, bf16[2048,256]{1,0:T(8,128)(2,1)}, u32[]{:S(2)}, u32[]{:S(2)}) collective-permute-start(bf16[2048,256]{1,0:T(8,128)(2,1)} %bitcast.24), channel_id=1, source_target_pairs={{0,3},{1,0},{2,1},{3,2},{4,7},{5,4},{6,5},{7,6},{8,11},{9,8},{10,9... | collective-permute-start | bytes 3145736 | tf_op jit(solution)/shard_map/ppermute | solution.py:21
  18.3 78.9 %collective-permute-start.6 = (bf16[2048,256]{1,0:T(8,128)(2,1)}, bf16[2048,256]{1,0:T(8,128)(2,1)S(1)}, u32[]{:S(2)}, u32[]{:S(2)}) collective-permute-start(bf16[2048,256]{1,0:T(8,128)(2,1)} %bitcast.25), channel_id=1, source_target_pairs={{0,1},{1,2},{2,3},{3,0},{4,5},{5,6},{6,7},{7,4},{8,9},{9,10},{10,1... | collective-permute-start | bytes 3145736 | tf_op jit(solution)/shard_map/ppermute | solution.py:21
  19.7 81.4 %collective-permute-start.7 = (bf16[2048,256]{1,0:T(8,128)(2,1)S(1)}, bf16[2048,256]{1,0:T(8,128)(2,1)S(1)}, u32[]{:S(2)}, u32[]{:S(2)}) collective-permute-start(bf16[2048,256]{1,0:T(8,128)(2,1)S(1)} %bitcast.22), channel_id=1, source_target_pairs={{0,3},{1,0},{2,1},{3,2},{4,7},{5,4},{6,5},{7,6},{8,11},{9,8},{10,9... | collective-permute-start | bytes 3145736 | tf_op jit(solution)/shard_map/ppermute | solution.py:21
  42.3 60.1 %collective-permute-start.13 = (bf16[2048,256]{1,0:T(8,128)(2,1)S(1)}, bf16[2048,256]{1,0:T(8,128)(2,1)S(1)}, u32[]{:S(2)}, u32[]{:S(2)}) collective-permute-start(bf16[2048,256]{1,0:T(8,128)(2,1)S(1)} %collective-permute-done.5.refs_3_), channel_id=1, source_target_pairs={{0,1},{1,2},{2,3},{3,0},{4,5},{5,6},{6,7},{7,4},{8,9},{9,10},{10,1... | collective-permute-start | bytes 3145736 | tf_op jit(solution)/shard_map/ppermute | solution.py:21
  43.7 1.0 copy-start.7
  44.7 71.2 %collective-permute-start.14 = (bf16[2048,256]{1,0:T(8,128)(2,1)}, bf16[2048,256]{1,0:T(8,128)(2,1)}, u32[]{:S(2)}, u32[]{:S(2)}) collective-permute-start(bf16[2048,256]{1,0:T(8,128)(2,1)} %collective-permute-done.8.refs_6_), channel_id=1, source_target_pairs={{0,3},{1,0},{2,1},{3,2},{4,7},{5,4},{6,5},{7,6},{8,11},{9,8},{10,9... | collective-permute-start | bytes 3145736 | tf_op jit(solution)/shard_map/ppermute | solution.py:21
  46.2 44.6 %collective-permute-start.12 = (bf16[256,256]{1,0:T(8,128)(2,1)S(1)}, bf16[256,256]{1,0:T(8,128)(2,1)}, u32[]{:S(2)}, u32[]{:S(2)}) collective-permute-start(bf16[256,256]{1,0:T(8,128)(2,1)S(1)} %slice.57.refs_4_), channel_id=1, source_target_pairs={{0,3},{1,0},{2,1},{3,2},{4,7},{5,4},{6,5},{7,6},{8,11},{9,8},{10,9... | collective-permute-start | bytes 393224 | tf_op jit(solution)/shard_map/ppermute | solution.py:21
  90.8 6.0 %collective-permute-start.9 = (bf16[256,384]{1,0:T(8,128)(2,1)S(1)}, bf16[256,384]{1,0:T(8,128)(2,1)}, u32[]{:S(2)}, u32[]{:S(2)}) collective-permute-start(bf16[256,384]{1,0:T(8,128)(2,1)S(1)} %slice.56.refs_1_), channel_id=1, source_target_pairs={{0,1},{1,2},{2,3},{3,0},{4,5},{5,6},{6,7},{7,4},{8,9},{9,10},{10,1... | collective-permute-start | bytes 589832 | tf_op jit(solution)/shard_map/ppermute | solution.py:21
  96.8 21.7 %collective-permute-start.10 = (bf16[256,384]{1,0:T(8,128)(2,1)S(1)}, bf16[256,384]{1,0:T(8,128)(2,1)}, u32[]{:S(2)}, u32[]{:S(2)}) collective-permute-start(bf16[256,384]{1,0:T(8,128)(2,1)S(1)} %slice.56.refs_1_), channel_id=1, source_target_pairs={{0,3},{1,0},{2,1},{3,2},{4,7},{5,4},{6,5},{7,6},{8,11},{9,8},{10,9... | collective-permute-start | bytes 589832 | tf_op jit(solution)/shard_map/ppermute | solution.py:21
  97.1 1.0 copy-start.9
  98.1 22.4 %collective-permute-start.15 = (bf16[256,384]{1,0:T(8,128)(2,1)}, bf16[256,384]{1,0:T(8,128)(2,1)}, u32[]{:S(2)}, u32[]{:S(2)}) collective-permute-start(bf16[256,384]{1,0:T(8,128)(2,1)} %collective-permute-done.9.refs_2_), channel_id=1, source_target_pairs={{0,1},{1,2},{2,3},{3,0},{4,5},{5,6},{6,7},{7,4},{8,9},{9,10},{10,1... | collective-permute-start | bytes 589832 | tf_op jit(solution)/shard_map/ppermute | solution.py:21
  101.1 1.0 copy-start.11
  102.0 16.5 %collective-permute-start.11 = (bf16[256,256]{1,0:T(8,128)(2,1)S(1)}, bf16[256,256]{1,0:T(8,128)(2,1)}, u32[]{:S(2)}, u32[]{:S(2)}) collective-permute-start(bf16[256,256]{1,0:T(8,128)(2,1)S(1)} %slice.57.refs_4_), channel_id=1, source_target_pairs={{0,1},{1,2},{2,3},{3,0},{4,5},{5,6},{6,7},{7,4},{8,9},{9,10},{10,1... | collective-permute-start | bytes 393224 | tf_op jit(solution)/shard_map/ppermute | solution.py:21
  102.3 1.0 copy-start.13
  103.4 17.2 %collective-permute-start.16 = (bf16[256,256]{1,0:T(8,128)(2,1)}, bf16[256,256]{1,0:T(8,128)(2,1)}, u32[]{:S(2)}, u32[]{:S(2)}) collective-permute-start(bf16[256,256]{1,0:T(8,128)(2,1)} %collective-permute-done.12.refs_6_), channel_id=1, source_target_pairs={{0,3},{1,0},{2,1},{3,2},{4,7},{5,4},{6,5},{7,6},{8,11},{9,8},{10,9... | collective-permute-start | bytes 393224 | tf_op jit(solution)/shard_map/ppermute | solution.py:21
  105.1 1.2 copy-start.5
  106.3 1.2 copy-start.6
  107.6 1.2 copy-start.8
  108.8 1.2 copy-start.10
  110.0 1.2 copy-start.12
  111.2 4.7 %copy-start.14 = (bf16[2048,256]{1,0:T(8,128)(2,1)S(1)}, bf16[2048,256]{1,0:T(8,128)(2,1)}, u32[]{:S(2)}) copy-start(bf16[2048,256]{1,0:T(8,128)(2,1)} %copy-done.13) | copy-start | bytes 3145732
  122.7 43.3 %all-to-all-start.1 = ((bf16[64,8,640]{2,1,0:T(8,128)(2,1)}), bf16[64,8,640]{2,1,0:T(8,128)(2,1)S(1)}, u32[]{:S(2)}, u32[]{:S(2)}) async-start(bf16[64,8,640]{2,1,0:T(8,128)(2,1)} %bitcast.12), calls=%async_computation.1 | async-start | bytes 1310720 | tf_op jit(solution)/shard_map/all_to_all | solution.py:291
  134.1 11.2 %collective-permute-start.17 = (bf16[256,768]{1,0:T(8,128)(2,1)S(1)}, bf16[256,768]{1,0:T(8,128)(2,1)S(1)}, u32[]{:S(2)}, u32[]{:S(2)}) collective-permute-start(bf16[256,768]{1,0:T(8,128)(2,1)S(1)} %slice.58.refs_1_), channel_id=1, source_target_pairs={{0,1},{1,2},{2,3},{3,0},{4,5},{5,6},{6,7},{7,4},{8,9},{9,10},{10,1... | collective-permute-start | bytes 1179656 | tf_op jit(solution)/shard_map/ppermute | solution.py:21
  136.7 11.9 %collective-permute-start.20 = (bf16[256,640]{1,0:T(8,128)(2,1)S(1)}, bf16[256,640]{1,0:T(8,128)(2,1)S(1)}, u32[]{:S(2)}, u32[]{:S(2)}) collective-permute-start(bf16[256,640]{1,0:T(8,128)(2,1)S(1)} %slice.59.refs_4_), channel_id=1, source_target_pairs={{0,3},{1,0},{2,1},{3,2},{4,7},{5,4},{6,5},{7,6},{8,11},{9,8},{10,9... | collective-permute-start | bytes 983048 | tf_op jit(solution)/shard_map/ppermute | solution.py:21
  137.3 25.6 %collective-permute-start.18 = (bf16[256,768]{1,0:T(8,128)(2,1)S(1)}, bf16[256,768]{1,0:T(8,128)(2,1)S(1)}, u32[]{:S(2)}, u32[]{:S(2)}) collective-permute-start(bf16[256,768]{1,0:T(8,128)(2,1)S(1)} %slice.58.refs_1_), channel_id=1, source_target_pairs={{0,3},{1,0},{2,1},{3,2},{4,7},{5,4},{6,5},{7,6},{8,11},{9,8},{10,9... | collective-permute-start | bytes 1179656 | tf_op jit(solution)/shard_map/ppermute | solution.py:21
  145.3 19.2 %collective-permute-start.21 = (bf16[256,768]{1,0:T(8,128)(2,1)S(1)}, bf16[256,768]{1,0:T(8,128)(2,1)S(1)}, u32[]{:S(2)}, u32[]{:S(2)}) collective-permute-start(bf16[256,768]{1,0:T(8,128)(2,1)S(1)} %collective-permute-done.17.refs_2_), channel_id=1, source_target_pairs={{0,1},{1,2},{2,3},{3,0},{4,5},{5,6},{6,7},{7,4},{8,9},{9,10},{10,1... | collective-permute-start | bytes 1179656 | tf_op jit(solution)/shard_map/ppermute | solution.py:21
  148.0 14.8 %collective-permute-start.19 = (bf16[256,640]{1,0:T(8,128)(2,1)S(1)}, bf16[256,640]{1,0:T(8,128)(2,1)S(1)}, u32[]{:S(2)}, u32[]{:S(2)}) collective-permute-start(bf16[256,640]{1,0:T(8,128)(2,1)S(1)} %slice.59.refs_4_), channel_id=1, source_target_pairs={{0,1},{1,2},{2,3},{3,0},{4,5},{5,6},{6,7},{7,4},{8,9},{9,10},{10,1... | collective-permute-start | bytes 983048 | tf_op jit(solution)/shard_map/ppermute | solution.py:21
  148.5 15.9 %collective-permute-start.22 = (bf16[256,640]{1,0:T(8,128)(2,1)S(1)}, bf16[256,640]{1,0:T(8,128)(2,1)S(1)}, u32[]{:S(2)}, u32[]{:S(2)}) collective-permute-start(bf16[256,640]{1,0:T(8,128)(2,1)S(1)} %collective-permute-done.20.refs_6_), channel_id=1, source_target_pairs={{0,3},{1,0},{2,1},{3,2},{4,7},{5,4},{6,5},{7,6},{8,11},{9,8},{10,9... | collective-permute-start | bytes 983048 | tf_op jit(solution)/shard_map/ppermute | solution.py:21
  166.1 10.5 %copy-start.20 = (bf16[128,2048]{1,0:T(8,128)(2,1)S(1)}, bf16[128,2048]{1,0:T(8,128)(2,1)}, u32[]{:S(2)}) copy-start(bf16[128,2048]{1,0:T(8,128)(2,1)} %param.14) | copy-start | bytes 1572868
  166.1 10.5 %copy-start.21 = (bf16[128,2048]{1,0:T(8,128)(2,1)S(1)}, bf16[128,2048]{1,0:T(8,128)(2,1)}, u32[]{:S(2)}) copy-start(bf16[128,2048]{1,0:T(8,128)(2,1)} %param.13) | copy-start | bytes 1572868
  166.1 74.9 %all-to-all-start.2 = ((bf16[64,8,1408]{2,1,0:T(8,128)(2,1)}), bf16[64,8,1408]{2,1,0:T(8,128)(2,1)S(1)}, u32[]{:S(2)}, u32[]{:S(2)}) async-start(bf16[64,8,1408]{2,1,0:T(8,128)(2,1)} %bitcast.14), calls=%async_computation.2 | async-start | bytes 2883584 | tf_op jit(solution)/shard_map/all_to_all | solution.py:291
  176.6 5.5 %copy-start.23 = (bf16[3,2048]{1,0:T(4,128)(2,1)S(1)}, bf16[3,2048]{1,0:T(4,128)(2,1)}, u32[]{:S(2)}) copy-start(bf16[3,2048]{1,0:T(4,128)(2,1)} %param.15) | copy-start | bytes 36868
  176.6 6.9 %copy-start.22 = (bf16[128,2048]{1,0:T(8,128)(2,1)S(1)}, bf16[128,2048]{1,0:T(8,128)(2,1)}, u32[]{:S(2)}) copy-start(bf16[128,2048]{1,0:T(8,128)(2,1)} %param.12) | copy-start | bytes 1572868
  176.8 6.8 %collective-permute-start = (f32[2,2048]{1,0:T(2,128)S(1)}, f32[2,2048]{1,0:T(2,128)S(1)}, u32[]{:S(2)}, u32[]{:S(2)}) collective-permute-start(f32[2,2048]{1,0:T(2,128)S(1)} %slice.48), channel_id=1, source_target_pairs={{0,1},{1,2},{2,3},{3,4},{4,5},{5,6},{6,7},{7,8},{8,9},{9,10},{10,1... | collective-permute-start | bytes 49160 | tf_op jit(solution)/shard_map/ppermute | solution.py:241
  183.5 43.5 %copy-start.18 = (s32[128,2]{0,1:T(2,128)S(1)}, s32[128,2]{0,1:T(2,128)}, u32[]{:S(2)}) copy-start(s32[128,2]{0,1:T(2,128)} %param.22) | copy-start | bytes 3076
  183.5 43.5 %copy-start.19 = (f32[128,2]{0,1:T(2,128)S(1)}, f32[128,2]{0,1:T(2,128)}, u32[]{:S(2)}) copy-start(f32[128,2]{0,1:T(2,128)} %param.23) | copy-start | bytes 3076
  183.9 37.1 %collective-permute-start.1 = (bf16[128,2048]{1,0:T(8,128)(2,1)S(1)}, bf16[128,2048]{1,0:T(8,128)(2,1)S(1)}, u32[]{:S(2)}, u32[]{:S(2)}) collective-permute-start(bf16[128,2048]{1,0:T(8,128)(2,1)S(1)} %fusion.5.own_ref), channel_id=1, source_target_pairs={{0,1},{1,2},{2,3},{3,0},{4,5},{5,6},{6,7},{7,4},{8,9},{9,10},{10,1... | collective-permute-start | bytes 1572872 | tf_op jit(solution)/shard_map/ppermute | solution.py:21
  214.4 11.1 %collective-permute-start.2 = (bf16[128,2048]{1,0:T(8,128)(2,1)S(1)}, bf16[128,2048]{1,0:T(8,128)(2,1)S(1)}, u32[]{:S(2)}, u32[]{:S(2)}) collective-permute-start(bf16[128,2048]{1,0:T(8,128)(2,1)S(1)} %fusion.5.own_ref), channel_id=1, source_target_pairs={{0,3},{1,0},{2,1},{3,2},{4,7},{5,4},{6,5},{7,6},{8,11},{9,8},{10,9... | collective-permute-start | bytes 1572872 | tf_op jit(solution)/shard_map/ppermute | solution.py:21
  221.8 7.9 %collective-permute-start.3 = (bf16[64,2048]{1,0:T(8,128)(2,1)}, bf16[64,2048]{1,0:T(8,128)(2,1)}, u32[]{:S(2)}, u32[]{:S(2)}) collective-permute-start(bf16[64,2048]{1,0:T(8,128)(2,1)} %slice.54), channel_id=1, source_target_pairs={{0,1},{1,2},{2,3},{3,0},{4,5},{5,6},{6,7},{7,4},{8,9},{9,10},{10,1... | collective-permute-start | bytes 786440 | tf_op jit(solution)/shard_map/ppermute | solution.py:21
  226.2 0.8 copy-start.2
  227.0 7.9 %collective-permute-start.4 = (bf16[64,2048]{1,0:T(8,128)(2,1)}, bf16[64,2048]{1,0:T(8,128)(2,1)}, u32[]{:S(2)}, u32[]{:S(2)}) collective-permute-start(bf16[64,2048]{1,0:T(8,128)(2,1)} %slice.55), channel_id=1, source_target_pairs={{0,3},{1,0},{2,1},{3,2},{4,7},{5,4},{6,5},{7,6},{8,11},{9,8},{10,9... | collective-permute-start | bytes 786440 | tf_op jit(solution)/shard_map/ppermute | solution.py:21
  234.9 1.6 copy-start.1
  236.5 1.0 copy-start.3
  (2 other events, 1.4 us)
